TPU v7x, 768 devices: a whole 4x8x12 slice. The times are simulated.
768 devices in a mesh: fs: 48 (over z, x), tp: 16 (over y, core).
Axes of the slice: x: 4, y: 8, z: 12, core: 2. Of those that a mesh axis runs over, the one named last changes fastest.
Arguments:
- tokens: bfloat16 [21504, 2304], P('fs'), may hold values from -6 to 6
- norm_gain: float32 [2304], replicated, may hold values from 0.1 to 1.9
- gate_weight: bfloat16 [2304, 6144], P('fs', 'tp'), may hold values from -0.125 to 0.125
- up_weight: bfloat16 [2304, 6144], P('fs', 'tp'), may hold values from -0.125 to 0.125
- down_weight: bfloat16 [6144, 2304], P('tp', 'fs'), may hold values from -0.078125 to 0.078125
- branch_gain: float32 [2304], replicated, may hold values from 0.1 to 1.9
Outputs:
- result: bfloat16 [21504, 2304], P('fs')
All inputs are finite; a program needn't handle non-finite values.
Results may differ from a plain program's by a relative error of at most 0.014.
Values may be sent and summed in bfloat16 or wider, within the bound.
No kernel may reach another device: no remote copies, remote signals or barrier semaphores. Data moves between devices by JAX's collectives and lax.ppermute only.
A program may use at most 32 MiB of HBM per device.

v0:
```python
import jax
import jax.numpy as jnp
from jax import lax
from jax.experimental import pallas as pl
from jax.experimental.pallas import tpu as pltpu
from jax.sharding import Mesh
from jax.sharding import PartitionSpec as P


epsilon = 1e-06
VMEM = pltpu.VMEM
BF16 = jnp.bfloat16
F32 = jnp.float32


def shift(value, axis, by):
    n = lax.axis_size(axis)
    return lax.ppermute(value, axis, [(i, (i + by) % n) for i in range(n)])


def after(value, *others):
    return lax.optimization_barrier((value, *others))[0]


def local_call(body, outs, scratch=(), n_scalars=0, n_in=0, limit=20):
    return pl.pallas_call(
        body,
        out_shape=outs,
        in_specs=[pl.BlockSpec(memory_space=pltpu.SMEM)] * n_scalars
        + [pl.BlockSpec(memory_space=VMEM)] * n_in,
        out_specs=jax.tree.map(lambda _: pl.BlockSpec(memory_space=VMEM), outs),
        scratch_shapes=list(scratch),
        compiler_params=pltpu.CompilerParams(vmem_limit_bytes=limit << 20),
    )


def first_round(block):
    return shift(block, "x", -1), shift(block, "x", 1)


def halves_body(left, right, low, high):
    half = low.shape[0]
    low[...] = left[:half]
    high[...] = right[half:]


def second_round(right, left):
    part = jax.ShapeDtypeStruct((left.shape[0] // 2, *left.shape[1:]), BF16)
    low, high = local_call(halves_body, [part, part], n_in=2, limit=4)(left, right)
    return shift(low, "x", 1), shift(high, "x", -1)


def norm_body(tokens, gain, out):
    step = 16

    def lines(i, carry):
        at = pl.ds(pl.multiple_of(i * step, step), step)
        widened = tokens[at, :].astype(F32)
        scale = lax.rsqrt(jnp.mean(widened * widened, axis=-1, keepdims=True) + epsilon)
        out[at, :] = (widened * scale * gain[...]).astype(BF16)
        return carry

    lax.fori_loop(0, tokens.shape[0] // step, lines, 0)


def interleave(x, own, right, left, low, high, whole):
    slots = [lax.rem(x + k, 4) for k in range(4)]
    half = low.shape[0]
    for z in range(own.shape[0]):
        whole[z, slots[0]] = own[z]
        whole[z, slots[1]] = right[z]
        whole[z, slots[3]] = left[z]
        whole[z, slots[2]] = low[z] if z < half else high[z - half]


def hidden_body(x_ref, normed, own, right, left, low, high, hidden, whole):
    interleave(x_ref[0], own, right, left, low, high, whole)
    planes, across, rows, columns = whole.shape
    weight = whole[...].reshape(planes * across * rows, columns)
    width = columns // 2
    both = jnp.dot(normed[...], weight, preferred_element_type=F32)
    gate, up = both[:, :width], both[:, width:]
    hidden[...] = (gate * jax.nn.sigmoid(gate) * up).astype(BF16)


def half_product(hidden, which, weight):
    half = hidden.shape[0] // 2
    lines = hidden[pl.ds(pl.multiple_of(which * half, 32), half), :]
    planes, across, rows, width = weight.shape
    return lax.dot_general(
        lines,
        weight[...].reshape(planes * across * rows, width),
        (((1,), (1,)), ((), ())),
        preferred_element_type=F32,
    ).astype(BF16)


def send_body(x_ref, c_ref, hidden, own, right, left, low, high, send, whole):
    interleave(x_ref[0], own, right, left, low, high, whole)
    send[...] = half_product(hidden, 1 - c_ref[0], whole)


def keep_body(c_ref, hidden, whole, keep):
    keep[...] = half_product(hidden, c_ref[0], whole)


def pair_sum_body(mine, theirs, out, total, folded):
    total[...] = mine[...].astype(F32) + theirs[...].astype(F32)
    count, rows, width = out.shape
    rows = rows // 2
    for j in range(count):
        for part in range(2):
            folded[j, part * rows : (part + 1) * rows, :] = total[
                j * rows : (j + 1) * rows, part * width : (part + 1) * width
            ]
        out[j] = folded[j].astype(BF16)


def finish_body(pieces, tokens, gain, out, branch, full):
    total = pieces[0].astype(F32)
    for j in range(1, pieces.shape[0]):
        total = total + pieces[j].astype(F32)
    branch[...] = total
    rows, width = tokens.shape[0], total.shape[1]
    parts = [branch[part * rows : (part + 1) * rows, :] for part in range(2)]
    squares = sum(jnp.sum(p * p, axis=-1, keepdims=True) for p in parts)
    scale = lax.rsqrt(squares / (2 * width) + epsilon)
    for part, value in enumerate(parts):
        columns = slice(part * width, (part + 1) * width)
        full[part * rows : (part + 1) * rows, :] = (
            tokens[:, columns].astype(F32) + value * scale * gain[:, columns]
        )
    rounded = full[...].astype(BF16)
    for j in range(out.shape[0]):
        out[j] = rounded


def join_body(c_ref, mine, theirs, out, folded, lines):
    count, rows, width = mine.shape
    rows = rows // 2
    half = count * rows
    for at, (source, which) in enumerate(((mine, c_ref[0]), (theirs, 1 - c_ref[0]))):
        for j in range(count):
            folded[at, j] = source[j].astype(F32)
            for part in range(2):
                lines[at, j * rows : (j + 1) * rows, part * width : (part + 1) * width] = (
                    folded[at, j, part * rows : (part + 1) * rows, :]
                )
        out[pl.ds(pl.multiple_of(which * half, 32), half), :] = lines[at].astype(BF16)


def per_device(tokens, norm_gain, gate_weight, up_weight, down_weight, branch_gain):
    x, y, c = (lax.axis_index(a) for a in ("x", "y", "c"))
    x1, c1 = x.astype(jnp.int32)[None], c.astype(jnp.int32)[None]
    n_x, n_y, n_z = (lax.axis_size(a) for a in ("x", "y", "z"))
    count, width = tokens.shape
    half, rows = count // 2, count // 2 // n_y
    units, piece = gate_weight.shape[1], gate_weight.shape[0]
    folded = (n_y, 2 * rows, width // 2)

    own_tokens = lax.dynamic_slice_in_dim(tokens, c * half + y * rows, rows, 0)
    own_both, own_down, own_tokens, gain, branch_gain = lax.optimization_barrier(
        (
            jnp.concatenate([gate_weight, up_weight], axis=1),
            down_weight.T,
            own_tokens,
            norm_gain[None],
            branch_gain[None],
        )
    )
    both_z = lax.all_gather(own_both, "z")
    near = first_round(both_z)
    down_z = lax.all_gather(after(own_down, both_z), "z")
    far = second_round(*near)
    down_near = first_round(after(down_z, *near))
    down_far = second_round(*down_near)
    normed = local_call(
        norm_body, jax.ShapeDtypeStruct((count, width), BF16), n_in=2, limit=8
    )(tokens, gain)
    hidden = local_call(
        hidden_body,
        jax.ShapeDtypeStruct((count, units), BF16),
        [VMEM((n_z, n_x, piece, 2 * units), BF16)],
        1, 6,
    )(x1, normed, both_z, *near, *far)
    send, whole = local_call(
        send_body,
        [
            jax.ShapeDtypeStruct((half, width), BF16),
            jax.ShapeDtypeStruct((n_z, n_x, piece, units), BF16),
        ],
        (), 2, 6,
    )(x1, c1, hidden, down_z, *down_near, *down_far)
    theirs = shift(send, "c", 1)
    keep = local_call(
        keep_body, jax.ShapeDtypeStruct((half, width), BF16), (), 1, 2
    )(c1, hidden, whole)
    pair = local_call(
        pair_sum_body,
        jax.ShapeDtypeStruct(folded, BF16),
        [VMEM((half, width), F32), VMEM(folded, F32)],
        0, 2,
    )(keep, theirs)
    pieces = lax.all_to_all(pair, "y", 0, 0, tiled=True)
    done = local_call(
        finish_body,
        jax.ShapeDtypeStruct(folded, BF16),
        [VMEM(folded[1:], F32)] * 2,
        0, 3,
    )(pieces, own_tokens, branch_gain)
    mine = lax.all_to_all(done, "y", 0, 0, tiled=True)
    return local_call(
        join_body,
        jax.ShapeDtypeStruct((count, width), BF16),
        [VMEM((2, *folded), F32), VMEM((2, half, width), F32)],
        1, 2,
    )(c1, mine, shift(mine, "c", 1))


def solution(mesh):
    n_tp = mesh.shape["tp"]
    split = Mesh(mesh.devices.reshape(12, 4, n_tp // 2, 2), ("z", "x", "y", "c"))
    fs, tp = ("z", "x"), ("y", "c")
    placed = (P(fs, None), P(), P(fs, tp), P(fs, tp), P(tp, fs), P())

    return jax.shard_map(
        per_device, mesh=split, in_specs=placed, out_specs=P(fs, None), check_vma=False
    )
```

profile of v0, /device:TPU:1, one launch (start us, length us, event | category | flops | bytes accessed | tf_op | source)
XLA Modules:
  0.0 187.4 jit_solution(8390235213030637340)
XLA Ops:
  0.0 1.3 broadcast_in_dim.14.gain
  2.8 1.6 constant_dynamic-slice_fusion.tokens
  4.4 33.3 %all-gather = bf16[576,768]{1,0:T(8,128)(2,1)S(1)} all-gather(bf16[48,768]{1,0:T(8,128)(2,1)S(1)} %pad_maximum_fusion), channel_id=2, replica_groups=mesh['z'=12,'x'=4,'y'=8,'c'=2] {'z'}, dimensions={0}, use_global_device_ids=true | all-gather | bytes 958464 | tf_op jit(solution)/shard_map/all_gather | solution.py:171
  37.7 4.4 %collective-permute-start = (bf16[12,48,768]{2,1,0:T(8,128)(2,1)S(1)}, bf16[12,48,768]{2,1,0:T(8,128)(2,1)S(1)}, u32[]{:S(2)}, u32[]{:S(2)}) collective-permute-start(bf16[12,48,768]{2,1,0:T(8,128)(2,1)S(1)} %bitcast.5), channel_id=1, source_target_pairs={{0,48},{16,0},{32,16},{48,32},{1,49},{17,1},{33,17},{49,33},{2,50}... | collective-permute-start | bytes 2654216 | tf_op jit(solution)/shard_map/ppermute | solution.py:18
  42.1 1.9 %collective-permute-start.1 = (bf16[12,48,768]{2,1,0:T(8,128)(2,1)S(1)}, bf16[12,48,768]{2,1,0:T(8,128)(2,1)S(1)}, u32[]{:S(2)}, u32[]{:S(2)}) collective-permute-start(bf16[12,48,768]{2,1,0:T(8,128)(2,1)S(1)} %bitcast.6), channel_id=1, source_target_pairs={{0,16},{16,32},{32,48},{48,0},{1,17},{17,33},{33,49},{49,1},{2,18}... | collective-permute-start | bytes 2654216 | tf_op jit(solution)/shard_map/ppermute | solution.py:18
  44.1 18.5 %all-gather.1 = bf16[576,384]{1,0:T(8,128)(2,1)S(1)} all-gather(bf16[48,384]{1,0:T(8,128)(2,1)} %bitcast.11), channel_id=3, replica_groups=mesh['z'=12,'x'=4,'y'=8,'c'=2] {'z'}, dimensions={0}, use_global_device_ids=true | all-gather | bytes 479232 | tf_op jit(solution)/shard_map/all_gather | solution.py:173
  62.5 4.6 %collective-permute-start.4 = (bf16[12,48,384]{2,1,0:T(8,128)(2,1)S(1)}, bf16[12,48,384]{2,1,0:T(8,128)(2,1)S(1)}, u32[]{:S(2)}, u32[]{:S(2)}) collective-permute-start(bf16[12,48,384]{2,1,0:T(8,128)(2,1)S(1)} %bitcast.8), channel_id=1, source_target_pairs={{0,48},{16,0},{32,16},{48,32},{1,49},{17,1},{33,17},{49,33},{2,50}... | collective-permute-start | bytes 1327112 | tf_op jit(solution)/shard_map/ppermute | solution.py:18
  67.1 1.9 %collective-permute-start.5 = (bf16[12,48,384]{2,1,0:T(8,128)(2,1)S(1)}, bf16[12,48,384]{2,1,0:T(8,128)(2,1)S(1)}, u32[]{:S(2)}, u32[]{:S(2)}) collective-permute-start(bf16[12,48,384]{2,1,0:T(8,128)(2,1)S(1)} %bitcast.9), channel_id=1, source_target_pairs={{0,16},{16,32},{32,48},{48,0},{1,17},{17,33},{33,49},{49,1},{2,18}... | collective-permute-start | bytes 1327112 | tf_op jit(solution)/shard_map/ppermute | solution.py:18
  69.0 1.0 shard_map.65
  70.0 1.9 %collective-permute-start.2 = (bf16[6,48,768]{2,1,0:T(8,128)(2,1)}, bf16[6,48,768]{2,1,0:T(8,128)(2,1)}, u32[]{:S(2)}, u32[]{:S(2)}) collective-permute-start(bf16[6,48,768]{2,1,0:T(8,128)(2,1)} %get-tuple-element.20), channel_id=1, source_target_pairs={{0,16},{16,32},{32,48},{48,0},{1,17},{17,33},{33,49},{49,1},{2,18}... | collective-permute-start | bytes 1327112 | tf_op jit(solution)/shard_map/ppermute | solution.py:18
  71.9 4.6 %collective-permute-start.3 = (bf16[6,48,768]{2,1,0:T(8,128)(2,1)}, bf16[6,48,768]{2,1,0:T(8,128)(2,1)}, u32[]{:S(2)}, u32[]{:S(2)}) collective-permute-start(bf16[6,48,768]{2,1,0:T(8,128)(2,1)} %get-tuple-element.21), channel_id=1, source_target_pairs={{0,48},{16,0},{32,16},{48,32},{1,49},{17,1},{33,17},{49,33},{2,50}... | collective-permute-start | bytes 1327112 | tf_op jit(solution)/shard_map/ppermute | solution.py:18
  78.2 1.9 %collective-permute-start.6 = (bf16[6,48,384]{2,1,0:T(8,128)(2,1)}, bf16[6,48,384]{2,1,0:T(8,128)(2,1)}, u32[]{:S(2)}, u32[]{:S(2)}) collective-permute-start(bf16[6,48,384]{2,1,0:T(8,128)(2,1)} %get-tuple-element.25), channel_id=1, source_target_pairs={{0,16},{16,32},{32,48},{48,0},{1,17},{17,33},{33,49},{49,1},{2,18}... | collective-permute-start | bytes 663560 | tf_op jit(solution)/shard_map/ppermute | solution.py:18
  80.1 4.6 %collective-permute-start.7 = (bf16[6,48,384]{2,1,0:T(8,128)(2,1)}, bf16[6,48,384]{2,1,0:T(8,128)(2,1)}, u32[]{:S(2)}, u32[]{:S(2)}) collective-permute-start(bf16[6,48,384]{2,1,0:T(8,128)(2,1)} %get-tuple-element.26), channel_id=1, source_target_pairs={{0,48},{16,0},{32,16},{48,32},{1,49},{17,1},{33,17},{49,33},{2,50}... | collective-permute-start | bytes 663560 | tf_op jit(solution)/shard_map/ppermute | solution.py:18
  84.7 1.6 copy-done
  86.9 3.4 %shard_map.64.normed = bf16[448,2304]{1,0:T(8,128)(2,1)S(1)} custom-call(bf16[448,2304]{1,0:T(8,128)(2,1)S(1)} %copy-done, f32[1,2304]{1,0:T(1,128)S(1)} %copy-done.4), custom_call_target="tpu_custom_call" | custom-call | tf_op jit(solution)/shard_map/pallas_call | solution.py:177
  90.3 3.1 %shard_map.66.hidden = bf16[448,384]{1,0:T(8,128)(2,1)S(1)} custom-call(s32[1]{0:T(128)} %bitcast.1.x_ref, bf16[448,2304]{1,0:T(8,128)(2,1)S(1)} %shard_map.64.normed, bf16[12,48,768]{2,1,0:T(8,128)(2,1)S(1)} %bitcast.7, bf16[12,48,768]{2,1,0:T(8,128)(2,1)S(1)} %collective-permute-done.right, bf16[12,48,768]{2,1,0:T(8,128)(2,1)S(1)} %collective-permute-done.1.left, ...), custom_call_target="tpu_custom_call" | custom-call | tf_op jit(solution)/shard_map/pallas_call | solution.py:180
  93.5 2.1 %shard_map.68 = (bf16[224,2304]{1,0:T(8,128)(2,1)S(1)}, bf16[12,4,48,384]{3,2,1,0:T(8,128)(2,1)S(1)}) custom-call(s32[1]{0:T(128)} %bitcast.1.x_ref, s32[1]{0:T(128)} %bitcast.c_ref, bf16[448,384]{1,0:T(8,128)(2,1)S(1)} %shard_map.66.hidden, bf16[12,48,384]{2,1,0:T(8,128)(2,1)S(1)} %bitcast.10, bf16[12,48,384]{2,1,0:T(8,128)(2,1)S(1)} %collective-permute-done.4.right, ...), custom_call_target="tpu_custom_call" | custom-call | tf_op jit(solution)/shard_map/pallas_call | solution.py:186
  95.5 16.8 %collective-permute-start.8 = (bf16[224,2304]{1,0:T(8,128)(2,1)S(1)}, bf16[224,2304]{1,0:T(8,128)(2,1)S(1)}, u32[]{:S(2)}, u32[]{:S(2)}) collective-permute-start(bf16[224,2304]{1,0:T(8,128)(2,1)S(1)} %get-tuple-element.28), channel_id=1, source_target_pairs={{0,1},{1,0},{2,3},{3,2},{4,5},{5,4},{6,7},{7,6},{8,9},{9,8},{10,11... | collective-permute-start | bytes 3096584 | tf_op jit(solution)/shard_map/ppermute | solution.py:18
  113.1 1.4 collective-permute-done.8.theirs
  115.1 34.2 %all_to_all.10.pieces = bf16[8,56,1152]{2,1,0:T(8,128)(2,1)S(1)} all-to-all(bf16[8,56,1152]{2,1,0:T(8,128)(2,1)S(1)} %shard_map.70), channel_id=1, replica_groups=mesh['z'=12,'x'=4,'y'=8,'c'=2] {'y'}, dimensions={0} | all-to-all | bytes 2064384 | tf_op jit(solution)/shard_map/all_to_all | solution.py:204
  149.7 28.2 %all_to_all.11.mine = bf16[8,56,1152]{2,1,0:T(8,128)(2,1)S(1)} all-to-all(bf16[8,56,1152]{2,1,0:T(8,128)(2,1)S(1)} %shard_map.71), channel_id=1, replica_groups=mesh['z'=12,'x'=4,'y'=8,'c'=2] {'y'}, dimensions={0} | all-to-all | bytes 2064384 | tf_op jit(solution)/shard_map/all_to_all | solution.py:211
  177.9 5.4 %collective-permute-start.9 = (bf16[8,56,1152]{2,1,0:T(8,128)(2,1)S(1)}, bf16[8,56,1152]{2,1,0:T(8,128)(2,1)S(1)}, u32[]{:S(2)}, u32[]{:S(2)}) collective-permute-start(bf16[8,56,1152]{2,1,0:T(8,128)(2,1)S(1)} %all_to_all.11.mine), channel_id=1, source_target_pairs={{0,1},{1,0},{2,3},{3,2},{4,5},{5,4},{6,7},{7,6},{8,9},{9,8},{10,11... | collective-permute-start | bytes 3096584 | tf_op jit(solution)/shard_map/ppermute | solution.py:18
  183.3 2.2 %collective-permute-done.9.theirs = bf16[8,56,1152]{2,1,0:T(8,128)(2,1)S(1)} collective-permute-done((bf16[8,56,1152]{2,1,0:T(8,128)(2,1)S(1)}, bf16[8,56,1152]{2,1,0:T(8,128)(2,1)S(1)}, u32[]{:S(2)}, u32[]{:S(2)}) %collective-permute-start.9) | collective-permute-done | bytes 1032224 | tf_op jit(solution)/shard_map/ppermute | solution.py:18
  185.6 1.9 %shard_map.72 = bf16[448,2304]{1,0:T(8,128)(2,1)} custom-call(s32[1]{0:T(128)} %bitcast.c_ref, bf16[8,56,1152]{2,1,0:T(8,128)(2,1)S(1)} %all_to_all.11.mine, bf16[8,56,1152]{2,1,0:T(8,128)(2,1)S(1)} %collective-permute-done.9.theirs), custom_call_target="tpu_custom_call" | custom-call | tf_op jit(solution)/shard_map/pallas_call | solution.py:212
  (23 shorter events, 5.6 us)
Async XLA Ops:
  37.7 24.8 %collective-permute-start = (bf16[12,48,768]{2,1,0:T(8,128)(2,1)S(1)}, bf16[12,48,768]{2,1,0:T(8,128)(2,1)S(1)}, u32[]{:S(2)}, u32[]{:S(2)}) collective-permute-start(bf16[12,48,768]{2,1,0:T(8,128)(2,1)S(1)} %bitcast.5), channel_id=1, source_target_pairs={{0,48},{16,0},{32,16},{48,32},{1,49},{17,1},{33,17},{49,33},{2,50}... | collective-permute-start | bytes 2654216 | tf_op jit(solution)/shard_map/ppermute | solution.py:18
  42.1 20.4 %collective-permute-start.1 = (bf16[12,48,768]{2,1,0:T(8,128)(2,1)S(1)}, bf16[12,48,768]{2,1,0:T(8,128)(2,1)S(1)}, u32[]{:S(2)}, u32[]{:S(2)}) collective-permute-start(bf16[12,48,768]{2,1,0:T(8,128)(2,1)S(1)} %bitcast.6), channel_id=1, source_target_pairs={{0,16},{16,32},{32,48},{48,0},{1,17},{17,33},{33,49},{49,1},{2,18}... | collective-permute-start | bytes 2654216 | tf_op jit(solution)/shard_map/ppermute | solution.py:18
  62.5 14.9 %copy-start.1 = (bf16[576,384]{1,0:T(8,128)(2,1)}, bf16[576,384]{1,0:T(8,128)(2,1)S(1)}, u32[]{:S(2)}) copy-start(bf16[576,384]{1,0:T(8,128)(2,1)S(1)} %all-gather.1) | copy-start | bytes 1327108
  62.5 14.0 %collective-permute-start.4 = (bf16[12,48,384]{2,1,0:T(8,128)(2,1)S(1)}, bf16[12,48,384]{2,1,0:T(8,128)(2,1)S(1)}, u32[]{:S(2)}, u32[]{:S(2)}) collective-permute-start(bf16[12,48,384]{2,1,0:T(8,128)(2,1)S(1)} %bitcast.8), channel_id=1, source_target_pairs={{0,48},{16,0},{32,16},{48,32},{1,49},{17,1},{33,17},{49,33},{2,50}... | collective-permute-start | bytes 1327112 | tf_op jit(solution)/shard_map/ppermute | solution.py:18
  67.1 10.3 %collective-permute-start.5 = (bf16[12,48,384]{2,1,0:T(8,128)(2,1)S(1)}, bf16[12,48,384]{2,1,0:T(8,128)(2,1)S(1)}, u32[]{:S(2)}, u32[]{:S(2)}) collective-permute-start(bf16[12,48,384]{2,1,0:T(8,128)(2,1)S(1)} %bitcast.9), channel_id=1, source_target_pairs={{0,16},{16,32},{32,48},{48,0},{1,17},{17,33},{33,49},{49,1},{2,18}... | collective-permute-start | bytes 1327112 | tf_op jit(solution)/shard_map/ppermute | solution.py:18
  70.0 20.3 %collective-permute-start.2 = (bf16[6,48,768]{2,1,0:T(8,128)(2,1)}, bf16[6,48,768]{2,1,0:T(8,128)(2,1)}, u32[]{:S(2)}, u32[]{:S(2)}) collective-permute-start(bf16[6,48,768]{2,1,0:T(8,128)(2,1)} %get-tuple-element.20), channel_id=1, source_target_pairs={{0,16},{16,32},{32,48},{48,0},{1,17},{17,33},{33,49},{49,1},{2,18}... | collective-permute-start | bytes 1327112 | tf_op jit(solution)/shard_map/ppermute | solution.py:18
  71.9 18.4 %collective-permute-start.3 = (bf16[6,48,768]{2,1,0:T(8,128)(2,1)}, bf16[6,48,768]{2,1,0:T(8,128)(2,1)}, u32[]{:S(2)}, u32[]{:S(2)}) collective-permute-start(bf16[6,48,768]{2,1,0:T(8,128)(2,1)} %get-tuple-element.21), channel_id=1, source_target_pairs={{0,48},{16,0},{32,16},{48,32},{1,49},{17,1},{33,17},{49,33},{2,50}... | collective-permute-start | bytes 1327112 | tf_op jit(solution)/shard_map/ppermute | solution.py:18
  78.2 15.3 %collective-permute-start.6 = (bf16[6,48,384]{2,1,0:T(8,128)(2,1)}, bf16[6,48,384]{2,1,0:T(8,128)(2,1)}, u32[]{:S(2)}, u32[]{:S(2)}) collective-permute-start(bf16[6,48,384]{2,1,0:T(8,128)(2,1)} %get-tuple-element.25), channel_id=1, source_target_pairs={{0,16},{16,32},{32,48},{48,0},{1,17},{17,33},{33,49},{49,1},{2,18}... | collective-permute-start | bytes 663560 | tf_op jit(solution)/shard_map/ppermute | solution.py:18
  80.1 13.4 %collective-permute-start.7 = (bf16[6,48,384]{2,1,0:T(8,128)(2,1)}, bf16[6,48,384]{2,1,0:T(8,128)(2,1)}, u32[]{:S(2)}, u32[]{:S(2)}) collective-permute-start(bf16[6,48,384]{2,1,0:T(8,128)(2,1)} %get-tuple-element.26), channel_id=1, source_target_pairs={{0,48},{16,0},{32,16},{48,32},{1,49},{17,1},{33,17},{49,33},{2,50}... | collective-permute-start | bytes 663560 | tf_op jit(solution)/shard_map/ppermute | solution.py:18
  84.7 1.6 copy-start
  86.2 0.7 copy-start.4
  90.3 3.1 %copy-start.2 = (bf16[576,384]{1,0:T(8,128)(2,1)S(1)}, bf16[576,384]{1,0:T(8,128)(2,1)}, u32[]{:S(2)}) copy-start(bf16[576,384]{1,0:T(8,128)(2,1)} %copy-done.1) | copy-start | bytes 1327108
  95.5 19.0 %collective-permute-start.8 = (bf16[224,2304]{1,0:T(8,128)(2,1)S(1)}, bf16[224,2304]{1,0:T(8,128)(2,1)S(1)}, u32[]{:S(2)}, u32[]{:S(2)}) collective-permute-start(bf16[224,2304]{1,0:T(8,128)(2,1)S(1)} %get-tuple-element.28), channel_id=1, source_target_pairs={{0,1},{1,0},{2,3},{3,2},{4,5},{5,4},{6,7},{7,6},{8,9},{9,8},{10,11... | collective-permute-start | bytes 3096584 | tf_op jit(solution)/shard_map/ppermute | solution.py:18
  113.1 36.1 %copy-start.3 = (bf16[28,2304]{1,0:T(8,128)(2,1)S(1)}, bf16[28,2304]{1,0:T(8,128)(2,1)}, u32[]{:S(2)}) copy-start(bf16[28,2304]{1,0:T(8,128)(2,1)} %constant_dynamic-slice_fusion.tokens) | copy-start | bytes 387076
  177.9 7.6 %collective-permute-start.9 = (bf16[8,56,1152]{2,1,0:T(8,128)(2,1)S(1)}, bf16[8,56,1152]{2,1,0:T(8,128)(2,1)S(1)}, u32[]{:S(2)}, u32[]{:S(2)}) collective-permute-start(bf16[8,56,1152]{2,1,0:T(8,128)(2,1)S(1)} %all_to_all.11.mine), channel_id=1, source_target_pairs={{0,1},{1,0},{2,3},{3,2},{4,5},{5,4},{6,7},{7,6},{8,9},{9,8},{10,11... | collective-permute-start | bytes 3096584 | tf_op jit(solution)/shard_map/ppermute | solution.py:18
where the time goes:
time: 188 us; the launch traced here: 187 us
  blocking collectives  114 us (61%)
  starting transfers between devices  47.9 us (25%)
  Pallas kernels  13.8 us (7%)
  local copies, waits for them, and re-layouts  5.92 us (3%)
  waiting for transfers between devices  4.55 us (2%)
    ppermute x10, starting transfers between devices, shift(): return lax.ppermute(value, axis, [(i, (i + by) % n) for i in range(n)])  47.9 us
    all_to_all x1, blocking collectives, per_device(): pieces = lax.all_to_all(pair, 'y', 0, 0, tiled=True)  34.2 us
    all_gather x1, blocking collectives, per_device(): both_z = lax.all_gather(own_both, 'z')  33.3 us
    all_to_all x1, blocking collectives, per_device(): mine = lax.all_to_all(done, 'y', 0, 0, tiled=True)  28.2 us
    all_gather x1, blocking collectives, per_device(): down_z = lax.all_gather(after(own_down, both_z), 'z')  18.5 us
    ppermute x10, waiting for transfers between devices, shift(): return lax.ppermute(value, axis, [(i, (i + by) % n) for i in range(n)])  4.55 us
  transfers between devices with their start and end apart: 10, of which 3 were waited for; matrix products, arithmetic and copies ran while one was open for 0% of the time, Pallas kernels for 5%

commit v1 on v0

--- a/solution.py
+++ b/solution.py
@@ -60,7 +60,7 @@
         out[at, :] = (widened * scale * gain[...]).astype(BF16)
         return carry
 
-    lax.fori_loop(0, tokens.shape[0] // step, lines, 0)
+    lax.fori_loop(0, tokens.shape[0] // step, lines, 0, unroll=4)
 
 
 def interleave(x, own, right, left, low, high, whole):
@@ -130,9 +130,7 @@
         full[part * rows : (part + 1) * rows, :] = (
             tokens[:, columns].astype(F32) + value * scale * gain[:, columns]
         )
-    rounded = full[...].astype(BF16)
-    for j in range(out.shape[0]):
-        out[j] = rounded
+    out[...] = full[...].astype(BF16)
 
 
 def join_body(c_ref, mine, theirs, out, folded, lines):
@@ -158,31 +156,24 @@
     units, piece = gate_weight.shape[1], gate_weight.shape[0]
     folded = (n_y, 2 * rows, width // 2)
 
-    own_tokens = lax.dynamic_slice_in_dim(tokens, c * half + y * rows, rows, 0)
-    own_both, own_down, own_tokens, gain, branch_gain = lax.optimization_barrier(
-        (
-            jnp.concatenate([gate_weight, up_weight], axis=1),
-            down_weight.T,
-            own_tokens,
-            norm_gain[None],
-            branch_gain[None],
-        )
-    )
-    both_z = lax.all_gather(own_both, "z")
+    both_z = lax.all_gather(jnp.concatenate([gate_weight, up_weight], axis=1), "z")
     near = first_round(both_z)
-    down_z = lax.all_gather(after(own_down, both_z), "z")
+    copies = jnp.broadcast_to(after(down_weight.T, both_z)[None], (n_z, piece, units))
+    down_z = lax.all_to_all(copies, "z", 0, 0, tiled=True)
+    normed = local_call(
+        norm_body, jax.ShapeDtypeStruct((count, width), BF16), n_in=2, limit=8
+    )(tokens, norm_gain[None])
+    *near, normed = lax.optimization_barrier((*near, normed))
     far = second_round(*near)
     down_near = first_round(after(down_z, *near))
-    down_far = second_round(*down_near)
-    normed = local_call(
-        norm_body, jax.ShapeDtypeStruct((count, width), BF16), n_in=2, limit=8
-    )(tokens, gain)
     hidden = local_call(
         hidden_body,
         jax.ShapeDtypeStruct((count, units), BF16),
         [VMEM((n_z, n_x, piece, 2 * units), BF16)],
         1, 6,
     )(x1, normed, both_z, *near, *far)
+    *down_near, hidden = lax.optimization_barrier((*down_near, hidden))
+    down_far = second_round(*down_near)
     send, whole = local_call(
         send_body,
         [
@@ -202,13 +193,14 @@
         0, 2,
     )(keep, theirs)
     pieces = lax.all_to_all(pair, "y", 0, 0, tiled=True)
+    own_tokens = lax.dynamic_slice_in_dim(tokens, c * half + y * rows, rows, 0)
     done = local_call(
         finish_body,
-        jax.ShapeDtypeStruct(folded, BF16),
+        jax.ShapeDtypeStruct(folded[1:], BF16),
         [VMEM(folded[1:], F32)] * 2,
         0, 3,
-    )(pieces, own_tokens, branch_gain)
-    mine = lax.all_to_all(done, "y", 0, 0, tiled=True)
+    )(pieces, own_tokens, branch_gain[None])
+    mine = lax.all_gather(done, "y")
     return local_call(
         join_body,
         jax.ShapeDtypeStruct((count, width), BF16),

time: 188 us -> 185 us (0.984)
  blocking collectives: 114 us -> 56.1 us
  waiting for transfers between devices: 4.55 us -> 53.6 us
  starting transfers between devices: 47.9 us -> 51.8 us
  local copies, waits for them, and re-layouts: 5.92 us -> 8 us
    all_to_all x2 -> x0, blocking collectives: 62.4 us -> none  [the longest x1 34.2 us: per_device(): pieces = lax.all_to_all(pair, 'y', 0, 0, tiled=True)]
    all_to_all x0 -> x2, waiting for transfers between devices: none -> 27.8 us  [the longest x1 27.8 us: per_device(): pieces = lax.all_to_all(pair, 'y', 0, 0, tiled=True)]
    ppermute x10, waiting for transfers between devices: 4.55 us -> 25.8 us  [shift(): return lax.ppermute(value, axis, [(i, (i + by) % n) for i in range(n)])]
    all_to_all x0 -> x2, starting transfers between devices: none -> 11.1 us  [the longest x1 6.82 us: per_device(): pieces = lax.all_to_all(pair, 'y', 0, 0, tiled=True)]
    ppermute x10, starting transfers between devices: 47.9 us -> 40.7 us  [shift(): return lax.ppermute(value, axis, [(i, (i + by) % n) for i in range(n)])]
    all_gather x2, blocking collectives: 51.8 us -> 56.1 us  [the longest x1 35 us: per_device(): lax.all_gather(jnp.concatenate([gate_weight, up_weight], axis=1), 'z')]
    unnamed x10 -> x14, local copies, waits for them, and re-layouts: 2.29 us -> 5.44 us
    pallas_call x1, Pallas kernels: 3.35 us -> 1.19 us  [per_device(): local_call(norm_body, jax.ShapeDtypeStruct((count, width), BF16), n_in=2,...]
  transfers between devices with their start and end apart: 10 -> 12, of which waited for: 3 -> 9; matrix products, arithmetic and copies ran while one was open for 0% -> 1% of each run, Pallas kernels for 5% -> 3%
where the time goes in v1:
time: 185 us; the launch traced here: 184 us
  blocking collectives  56.1 us (30%)
  waiting for transfers between devices  53.6 us (29%)
  starting transfers between devices  51.8 us (28%)
  Pallas kernels  13.3 us (7%)
  local copies, waits for them, and re-layouts  8 us (4%)
    ppermute x10, starting transfers between devices, shift(): return lax.ppermute(value, axis, [(i, (i + by) % n) for i in range(n)])  40.7 us
    all_gather x1, blocking collectives, per_device(): lax.all_gather(jnp.concatenate([gate_weight, up_weight], axis=1), 'z')  35 us
    all_to_all x1, waiting for transfers between devices, per_device(): pieces = lax.all_to_all(pair, 'y', 0, 0, tiled=True)  27.8 us
    ppermute x10, waiting for transfers between devices, shift(): return lax.ppermute(value, axis, [(i, (i + by) % n) for i in range(n)])  25.8 us
    all_gather x1, blocking collectives, per_device(): mine = lax.all_gather(done, 'y')  21.1 us
    all_to_all x1, starting transfers between devices, per_device(): pieces = lax.all_to_all(pair, 'y', 0, 0, tiled=True)  6.82 us
    unnamed x14, local copies, waits for them, and re-layouts  5.44 us
    all_to_all x1, starting transfers between devices, per_device(): down_z = lax.all_to_all(copies, 'z', 0, 0, tiled=True)  4.23 us
  transfers between devices with their start and end apart: 12, of which 9 were waited for; matrix products, arithmetic and copies ran while one was open for 1% of the time, Pallas kernels for 3%

profile of v1, /device:TPU:1, one launch (start us, length us, event | category | flops | bytes accessed | tf_op | source)
XLA Modules:
  0.0 183.8 jit_solution(1730176107423770505)
XLA Ops:
  0.8 35.0 %all-gather = bf16[576,768]{1,0:T(8,128)(2,1)} all-gather(bf16[48,768]{1,0:T(8,128)(2,1)S(1)} %pad_maximum_fusion), channel_id=2, replica_groups=mesh['z'=12,'x'=4,'y'=8,'c'=2] {'z'}, dimensions={0}, use_global_device_ids=true | all-gather | bytes 958464 | tf_op jit(solution)/shard_map/all_gather | solution.py:159
  35.8 1.6 broadcast_in_dim.19
  37.4 4.2 %all-to-all-start = ((bf16[12,48,384]{2,1,0:T(8,128)(2,1)}), bf16[12,48,384]{2,1,0:T(8,128)(2,1)}, u32[]{:S(2)}, u32[]{:S(2)}) async-start(bf16[12,48,384]{2,1,0:T(8,128)(2,1)} %broadcast_in_dim.19), calls=%async_computation | async-start | bytes 884736 | tf_op jit(solution)/shard_map/all_to_all | solution.py:162
  41.6 4.4 %collective-permute-start = (bf16[12,48,768]{2,1,0:T(8,128)(2,1)}, bf16[12,48,768]{2,1,0:T(8,128)(2,1)S(1)}, u32[]{:S(2)}, u32[]{:S(2)}) collective-permute-start(bf16[12,48,768]{2,1,0:T(8,128)(2,1)} %bitcast.2.own), channel_id=1, source_target_pairs={{0,48},{16,0},{32,16},{48,32},{1,49},{17,1},{33,17},{49,33},{2,50}... | collective-permute-start | bytes 2654216 | tf_op jit(solution)/shard_map/ppermute | solution.py:18
  46.0 1.9 %collective-permute-start.1 = (bf16[12,48,768]{2,1,0:T(8,128)(2,1)}, bf16[12,48,768]{2,1,0:T(8,128)(2,1)S(1)}, u32[]{:S(2)}, u32[]{:S(2)}) collective-permute-start(bf16[12,48,768]{2,1,0:T(8,128)(2,1)} %bitcast.2.own), channel_id=1, source_target_pairs={{0,16},{16,32},{32,48},{48,0},{1,17},{17,33},{33,49},{49,1},{2,18}... | collective-permute-start | bytes 2654216 | tf_op jit(solution)/shard_map/ppermute | solution.py:18
  48.0 1.6 copy-done.2
  50.7 8.7 %collective-permute-done.right = bf16[12,48,768]{2,1,0:T(8,128)(2,1)S(1)} collective-permute-done((bf16[12,48,768]{2,1,0:T(8,128)(2,1)}, bf16[12,48,768]{2,1,0:T(8,128)(2,1)S(1)}, u32[]{:S(2)}, u32[]{:S(2)}) %collective-permute-start) | collective-permute-done | bytes 884768 | tf_op jit(solution)/shard_map/ppermute | solution.py:18
  59.4 5.0 %collective-permute-done.1.left = bf16[12,48,768]{2,1,0:T(8,128)(2,1)S(1)} collective-permute-done((bf16[12,48,768]{2,1,0:T(8,128)(2,1)}, bf16[12,48,768]{2,1,0:T(8,128)(2,1)S(1)}, u32[]{:S(2)}, u32[]{:S(2)}) %collective-permute-start.1) | collective-permute-done | bytes 884768 | tf_op jit(solution)/shard_map/ppermute | solution.py:18
  66.4 1.9 %collective-permute-start.4 = (bf16[6,48,768]{2,1,0:T(8,128)(2,1)}, bf16[6,48,768]{2,1,0:T(8,128)(2,1)S(1)}, u32[]{:S(2)}, u32[]{:S(2)}) collective-permute-start(bf16[6,48,768]{2,1,0:T(8,128)(2,1)} %get-tuple-element.24), channel_id=1, source_target_pairs={{0,16},{16,32},{32,48},{48,0},{1,17},{17,33},{33,49},{49,1},{2,18}... | collective-permute-start | bytes 1327112 | tf_op jit(solution)/shard_map/ppermute | solution.py:18
  68.3 4.6 %collective-permute-start.5 = (bf16[6,48,768]{2,1,0:T(8,128)(2,1)}, bf16[6,48,768]{2,1,0:T(8,128)(2,1)}, u32[]{:S(2)}, u32[]{:S(2)}) collective-permute-start(bf16[6,48,768]{2,1,0:T(8,128)(2,1)} %get-tuple-element.25), channel_id=1, source_target_pairs={{0,48},{16,0},{32,16},{48,32},{1,49},{17,1},{33,17},{49,33},{2,50}... | collective-permute-start | bytes 1327112 | tf_op jit(solution)/shard_map/ppermute | solution.py:18
  72.9 1.9 %collective-permute-start.2 = (bf16[12,48,384]{2,1,0:T(8,128)(2,1)}, bf16[12,48,384]{2,1,0:T(8,128)(2,1)}, u32[]{:S(2)}, u32[]{:S(2)}) collective-permute-start(bf16[12,48,384]{2,1,0:T(8,128)(2,1)} %all-to-all-done.own), channel_id=1, source_target_pairs={{0,48},{16,0},{32,16},{48,32},{1,49},{17,1},{33,17},{49,33},{2,50}... | collective-permute-start | bytes 1327112 | tf_op jit(solution)/shard_map/ppermute | solution.py:18
  74.8 3.4 %collective-permute-start.3 = (bf16[12,48,384]{2,1,0:T(8,128)(2,1)}, bf16[12,48,384]{2,1,0:T(8,128)(2,1)}, u32[]{:S(2)}, u32[]{:S(2)}) collective-permute-start(bf16[12,48,384]{2,1,0:T(8,128)(2,1)} %all-to-all-done.own), channel_id=1, source_target_pairs={{0,16},{16,32},{32,48},{48,0},{1,17},{17,33},{33,49},{49,1},{2,18}... | collective-permute-start | bytes 1327112 | tf_op jit(solution)/shard_map/ppermute | solution.py:18
  81.2 3.2 %shard_map.66.hidden = bf16[448,384]{1,0:T(8,128)(2,1)S(1)} custom-call(s32[1]{0:T(128)} %bitcast.3.x_ref, bf16[448,2304]{1,0:T(8,128)(2,1)S(1)} %shard_map.64.normed, bf16[12,48,768]{2,1,0:T(8,128)(2,1)} %bitcast.2.own, bf16[12,48,768]{2,1,0:T(8,128)(2,1)S(1)} %collective-permute-done.right, bf16[12,48,768]{2,1,0:T(8,128)(2,1)S(1)} %copy-done.1, ...), custom_call_target="tpu_custom_call" | custom-call | tf_op jit(solution)/shard_map/pallas_call | solution.py:169
  85.0 4.8 %collective-permute-done.3.left = bf16[12,48,384]{2,1,0:T(8,128)(2,1)} collective-permute-done((bf16[12,48,384]{2,1,0:T(8,128)(2,1)}, bf16[12,48,384]{2,1,0:T(8,128)(2,1)}, u32[]{:S(2)}, u32[]{:S(2)}) %collective-permute-start.3) | collective-permute-done | bytes 442400 | tf_op jit(solution)/shard_map/ppermute | solution.py:18
  91.0 1.9 %collective-permute-start.6 = (bf16[6,48,384]{2,1,0:T(8,128)(2,1)S(1)}, bf16[6,48,384]{2,1,0:T(8,128)(2,1)S(1)}, u32[]{:S(2)}, u32[]{:S(2)}) collective-permute-start(bf16[6,48,384]{2,1,0:T(8,128)(2,1)S(1)} %get-tuple-element.29), channel_id=1, source_target_pairs={{0,16},{16,32},{32,48},{48,0},{1,17},{17,33},{33,49},{49,1},{2,18}... | collective-permute-start | bytes 663560 | tf_op jit(solution)/shard_map/ppermute | solution.py:18
  92.9 4.6 %collective-permute-start.7 = (bf16[6,48,384]{2,1,0:T(8,128)(2,1)S(1)}, bf16[6,48,384]{2,1,0:T(8,128)(2,1)S(1)}, u32[]{:S(2)}, u32[]{:S(2)}) collective-permute-start(bf16[6,48,384]{2,1,0:T(8,128)(2,1)S(1)} %get-tuple-element.30), channel_id=1, source_target_pairs={{0,48},{16,0},{32,16},{48,32},{1,49},{17,1},{33,17},{49,33},{2,50}... | collective-permute-start | bytes 663560 | tf_op jit(solution)/shard_map/ppermute | solution.py:18
  100.4 2.3 %shard_map.68 = (bf16[224,2304]{1,0:T(8,128)(2,1)S(1)}, bf16[12,4,48,384]{3,2,1,0:T(8,128)(2,1)S(1)}) custom-call(s32[1]{0:T(128)} %bitcast.3.x_ref, s32[1]{0:T(128)} %bitcast.c_ref, bf16[448,384]{1,0:T(8,128)(2,1)S(1)} %shard_map.66.hidden, bf16[12,48,384]{2,1,0:T(8,128)(2,1)} %all-to-all-done.own, bf16[12,48,384]{2,1,0:T(8,128)(2,1)} %collective-permute-done.2.right, ...), custom_call_target="tpu_custom_call" | custom-call | tf_op jit(solution)/shard_map/pallas_call | solution.py:177
  102.7 7.9 %collective-permute-start.8 = (bf16[224,2304]{1,0:T(8,128)(2,1)S(1)}, bf16[224,2304]{1,0:T(8,128)(2,1)S(1)}, u32[]{:S(2)}, u32[]{:S(2)}) collective-permute-start(bf16[224,2304]{1,0:T(8,128)(2,1)S(1)} %get-tuple-element.32), channel_id=1, source_target_pairs={{0,1},{1,0},{2,3},{3,2},{4,5},{5,4},{6,7},{7,6},{8,9},{9,8},{10,11... | collective-permute-start | bytes 3096584 | tf_op jit(solution)/shard_map/ppermute | solution.py:18
  114.3 6.8 %all-to-all-start.1 = ((bf16[8,56,1152]{2,1,0:T(8,128)(2,1)}), bf16[8,56,1152]{2,1,0:T(8,128)(2,1)S(1)}, u32[]{:S(2)}, u32[]{:S(2)}) async-start(bf16[8,56,1152]{2,1,0:T(8,128)(2,1)} %shard_map.70), calls=%async_computation.1 | async-start | bytes 2064384 | tf_op jit(solution)/shard_map/all_to_all | solution.py:195
  122.1 27.8 %all-to-all-done.1.pieces = bf16[8,56,1152]{2,1,0:T(8,128)(2,1)S(1)} async-done(((bf16[8,56,1152]{2,1,0:T(8,128)(2,1)}), bf16[8,56,1152]{2,1,0:T(8,128)(2,1)S(1)}, u32[]{:S(2)}, u32[]{:S(2)}) %all-to-all-start.1) | async-done | bytes 1032224 | tf_op jit(solution)/shard_map/all_to_all | solution.py:195
  150.3 21.1 %all-gather.1 = bf16[448,1152]{1,0:T(8,128)(2,1)S(1)} all-gather(bf16[56,1152]{1,0:T(8,128)(2,1)S(1)} %shard_map.71), channel_id=3, replica_groups=mesh['z'=12,'x'=4,'y'=8,'c'=2] {'y'}, dimensions={0}, use_global_device_ids=true | all-gather | bytes 1161216 | tf_op jit(solution)/shard_map/all_gather | solution.py:203
  171.4 8.2 %collective-permute-start.9 = (bf16[8,56,1152]{2,1,0:T(8,128)(2,1)S(1)}, bf16[8,56,1152]{2,1,0:T(8,128)(2,1)S(1)}, u32[]{:S(2)}, u32[]{:S(2)}) collective-permute-start(bf16[8,56,1152]{2,1,0:T(8,128)(2,1)S(1)} %bitcast.5), channel_id=1, source_target_pairs={{0,1},{1,0},{2,3},{3,2},{4,5},{5,4},{6,7},{7,6},{8,9},{9,8},{10,11... | collective-permute-start | bytes 3096584 | tf_op jit(solution)/shard_map/ppermute | solution.py:18
  179.6 2.2 %collective-permute-done.9.theirs = bf16[8,56,1152]{2,1,0:T(8,128)(2,1)S(1)} collective-permute-done((bf16[8,56,1152]{2,1,0:T(8,128)(2,1)S(1)}, bf16[8,56,1152]{2,1,0:T(8,128)(2,1)S(1)}, u32[]{:S(2)}, u32[]{:S(2)}) %collective-permute-start.9) | collective-permute-done | bytes 1032224 | tf_op jit(solution)/shard_map/ppermute | solution.py:18
  181.9 1.9 %shard_map.72 = bf16[448,2304]{1,0:T(8,128)(2,1)} custom-call(s32[1]{0:T(128)} %bitcast.c_ref, bf16[8,56,1152]{2,1,0:T(8,128)(2,1)S(1)} %bitcast.6, bf16[8,56,1152]{2,1,0:T(8,128)(2,1)S(1)} %collective-permute-done.9.theirs), custom_call_target="tpu_custom_call" | custom-call | tf_op jit(solution)/shard_map/pallas_call | solution.py:204
  (30 shorter events, 16.6 us)
Async XLA Ops:
  0.0 47.9 %copy-start.5 = (f32[2304]{0:T(1024)S(1)}, f32[2304]{0:T(1024)}, u32[]{:S(2)}) copy-start(f32[2304]{0:T(1024)} %param.7) | copy-start | bytes 27652
  37.4 35.5 %all-to-all-start = ((bf16[12,48,384]{2,1,0:T(8,128)(2,1)}), bf16[12,48,384]{2,1,0:T(8,128)(2,1)}, u32[]{:S(2)}, u32[]{:S(2)}) async-start(bf16[12,48,384]{2,1,0:T(8,128)(2,1)} %broadcast_in_dim.19), calls=%async_computation | async-start | bytes 884736 | tf_op jit(solution)/shard_map/all_to_all | solution.py:162
  41.6 17.8 %collective-permute-start = (bf16[12,48,768]{2,1,0:T(8,128)(2,1)}, bf16[12,48,768]{2,1,0:T(8,128)(2,1)S(1)}, u32[]{:S(2)}, u32[]{:S(2)}) collective-permute-start(bf16[12,48,768]{2,1,0:T(8,128)(2,1)} %bitcast.2.own), channel_id=1, source_target_pairs={{0,48},{16,0},{32,16},{48,32},{1,49},{17,1},{33,17},{49,33},{2,50}... | collective-permute-start | bytes 2654216 | tf_op jit(solution)/shard_map/ppermute | solution.py:18
  46.0 18.5 %collective-permute-start.1 = (bf16[12,48,768]{2,1,0:T(8,128)(2,1)}, bf16[12,48,768]{2,1,0:T(8,128)(2,1)S(1)}, u32[]{:S(2)}, u32[]{:S(2)}) collective-permute-start(bf16[12,48,768]{2,1,0:T(8,128)(2,1)} %bitcast.2.own), channel_id=1, source_target_pairs={{0,16},{16,32},{32,48},{48,0},{1,17},{17,33},{33,49},{49,1},{2,18}... | collective-permute-start | bytes 2654216 | tf_op jit(solution)/shard_map/ppermute | solution.py:18
  48.0 1.6 copy-start.2
  65.5 0.9 copy-start
  66.4 11.8 %collective-permute-start.4 = (bf16[6,48,768]{2,1,0:T(8,128)(2,1)}, bf16[6,48,768]{2,1,0:T(8,128)(2,1)S(1)}, u32[]{:S(2)}, u32[]{:S(2)}) collective-permute-start(bf16[6,48,768]{2,1,0:T(8,128)(2,1)} %get-tuple-element.24), channel_id=1, source_target_pairs={{0,16},{16,32},{32,48},{48,0},{1,17},{17,33},{33,49},{49,1},{2,18}... | collective-permute-start | bytes 1327112 | tf_op jit(solution)/shard_map/ppermute | solution.py:18
  68.3 10.7 %collective-permute-start.5 = (bf16[6,48,768]{2,1,0:T(8,128)(2,1)}, bf16[6,48,768]{2,1,0:T(8,128)(2,1)}, u32[]{:S(2)}, u32[]{:S(2)}) collective-permute-start(bf16[6,48,768]{2,1,0:T(8,128)(2,1)} %get-tuple-element.25), channel_id=1, source_target_pairs={{0,48},{16,0},{32,16},{48,32},{1,49},{17,1},{33,17},{49,33},{2,50}... | collective-permute-start | bytes 1327112 | tf_op jit(solution)/shard_map/ppermute | solution.py:18
  72.9 12.1 %collective-permute-start.2 = (bf16[12,48,384]{2,1,0:T(8,128)(2,1)}, bf16[12,48,384]{2,1,0:T(8,128)(2,1)}, u32[]{:S(2)}, u32[]{:S(2)}) collective-permute-start(bf16[12,48,384]{2,1,0:T(8,128)(2,1)} %all-to-all-done.own), channel_id=1, source_target_pairs={{0,48},{16,0},{32,16},{48,32},{1,49},{17,1},{33,17},{49,33},{2,50}... | collective-permute-start | bytes 1327112 | tf_op jit(solution)/shard_map/ppermute | solution.py:18
  74.8 15.0 %collective-permute-start.3 = (bf16[12,48,384]{2,1,0:T(8,128)(2,1)}, bf16[12,48,384]{2,1,0:T(8,128)(2,1)}, u32[]{:S(2)}, u32[]{:S(2)}) collective-permute-start(bf16[12,48,384]{2,1,0:T(8,128)(2,1)} %all-to-all-done.own), channel_id=1, source_target_pairs={{0,16},{16,32},{32,48},{48,0},{1,17},{17,33},{33,49},{49,1},{2,18}... | collective-permute-start | bytes 1327112 | tf_op jit(solution)/shard_map/ppermute | solution.py:18
  78.2 0.8 copy-start.3
  79.0 1.2 copy-start.1
  80.1 1.0 copy-start.4
  91.0 7.9 %collective-permute-start.6 = (bf16[6,48,384]{2,1,0:T(8,128)(2,1)S(1)}, bf16[6,48,384]{2,1,0:T(8,128)(2,1)S(1)}, u32[]{:S(2)}, u32[]{:S(2)}) collective-permute-start(bf16[6,48,384]{2,1,0:T(8,128)(2,1)S(1)} %get-tuple-element.29), channel_id=1, source_target_pairs={{0,16},{16,32},{32,48},{48,0},{1,17},{17,33},{33,49},{49,1},{2,18}... | collective-permute-start | bytes 663560 | tf_op jit(solution)/shard_map/ppermute | solution.py:18
  92.9 7.4 %collective-permute-start.7 = (bf16[6,48,384]{2,1,0:T(8,128)(2,1)S(1)}, bf16[6,48,384]{2,1,0:T(8,128)(2,1)S(1)}, u32[]{:S(2)}, u32[]{:S(2)}) collective-permute-start(bf16[6,48,384]{2,1,0:T(8,128)(2,1)S(1)} %get-tuple-element.30), channel_id=1, source_target_pairs={{0,48},{16,0},{32,16},{48,32},{1,49},{17,1},{33,17},{49,33},{2,50}... | collective-permute-start | bytes 663560 | tf_op jit(solution)/shard_map/ppermute | solution.py:18
  102.7 10.2 %collective-permute-start.8 = (bf16[224,2304]{1,0:T(8,128)(2,1)S(1)}, bf16[224,2304]{1,0:T(8,128)(2,1)S(1)}, u32[]{:S(2)}, u32[]{:S(2)}) collective-permute-start(bf16[224,2304]{1,0:T(8,128)(2,1)S(1)} %get-tuple-element.32), channel_id=1, source_target_pairs={{0,1},{1,0},{2,3},{3,2},{4,5},{5,4},{6,7},{7,6},{8,9},{9,8},{10,11... | collective-permute-start | bytes 3096584 | tf_op jit(solution)/shard_map/ppermute | solution.py:18
  111.4 9.7 %copy-start.6 = (f32[2304]{0:T(1024)S(1)}, f32[2304]{0:T(1024)}, u32[]{:S(2)}) copy-start(f32[2304]{0:T(1024)} %param.11) | copy-start | bytes 27652
  114.3 35.7 %all-to-all-start.1 = ((bf16[8,56,1152]{2,1,0:T(8,128)(2,1)}), bf16[8,56,1152]{2,1,0:T(8,128)(2,1)S(1)}, u32[]{:S(2)}, u32[]{:S(2)}) async-start(bf16[8,56,1152]{2,1,0:T(8,128)(2,1)} %shard_map.70), calls=%async_computation.1 | async-start | bytes 2064384 | tf_op jit(solution)/shard_map/all_to_all | solution.py:195
  171.4 10.5 %collective-permute-start.9 = (bf16[8,56,1152]{2,1,0:T(8,128)(2,1)S(1)}, bf16[8,56,1152]{2,1,0:T(8,128)(2,1)S(1)}, u32[]{:S(2)}, u32[]{:S(2)}) collective-permute-start(bf16[8,56,1152]{2,1,0:T(8,128)(2,1)S(1)} %bitcast.5), channel_id=1, source_target_pairs={{0,1},{1,0},{2,3},{3,2},{4,5},{5,4},{6,7},{7,6},{8,9},{9,8},{10,11... | collective-permute-start | bytes 3096584 | tf_op jit(solution)/shard_map/ppermute | solution.py:18

commit v2 on v1

v2 whole, which is shorter than its diff:
```python
import jax
import jax.numpy as jnp
from jax import lax
from jax.experimental import pallas as pl
from jax.experimental.pallas import tpu as pltpu
from jax.sharding import Mesh
from jax.sharding import PartitionSpec as P


epsilon = 1e-06
VMEM = pltpu.VMEM
BF16 = jnp.bfloat16
F32 = jnp.float32


def shift(value, axis, by):
    n = lax.axis_size(axis)
    return lax.ppermute(value, axis, [(i, (i + by) % n) for i in range(n)])


def after(value, *others):
    return lax.optimization_barrier((value, *others))[0]


def local_call(body, outs, scratch=(), n_scalars=0, n_in=0, limit=20):
    return pl.pallas_call(
        body,
        out_shape=outs,
        in_specs=[pl.BlockSpec(memory_space=pltpu.SMEM)] * n_scalars
        + [pl.BlockSpec(memory_space=VMEM)] * n_in,
        out_specs=jax.tree.map(lambda _: pl.BlockSpec(memory_space=VMEM), outs),
        scratch_shapes=list(scratch),
        compiler_params=pltpu.CompilerParams(vmem_limit_bytes=limit << 20),
    )


def first_round(block):
    return shift(block, "x", -1), shift(block, "x", 1)


def halves_body(left, right, low, high):
    half = low.shape[0]
    low[...] = left[:half]
    high[...] = right[half:]


def second_round(right, left):
    part = jax.ShapeDtypeStruct((left.shape[0] // 2, *left.shape[1:]), BF16)
    low, high = local_call(halves_body, [part, part], n_in=2, limit=4)(left, right)
    return shift(low, "x", 1), shift(high, "x", -1)


def norm_body(c_ref, y_ref, tokens, gain, out, own, window):
    step = 16

    def lines(i, carry):
        at = pl.ds(pl.multiple_of(i * step, step), step)
        widened = tokens[at, :].astype(F32)
        scale = lax.rsqrt(jnp.mean(widened * widened, axis=-1, keepdims=True) + epsilon)
        out[at, :] = (widened * scale * gain[...][None]).astype(BF16)
        return carry

    lax.fori_loop(0, tokens.shape[0] // step, lines, 0, unroll=4)
    count, rows, reach = tokens.shape[0], own.shape[0], window.shape[0]
    first = c_ref[0] * (count // 2) + y_ref[0] * rows
    base = jnp.minimum(first - lax.rem(first, step), count - reach)
    window[...] = tokens[pl.ds(pl.multiple_of(base, step), reach), :].astype(F32)
    for skip in range(0, reach - rows + 1, 4):

        @pl.when(first - base == skip)
        def _():
            own[...] = window[skip : skip + rows, :]


def interleave(x, own, right, left, low, high, whole):
    slots = [lax.rem(x + k, 4) for k in range(4)]
    half = low.shape[0]
    for z in range(own.shape[0]):
        whole[z, slots[0]] = own[z]
        whole[z, slots[1]] = right[z]
        whole[z, slots[3]] = left[z]
        whole[z, slots[2]] = low[z] if z < half else high[z - half]


def hidden_body(x_ref, normed, own, right, left, low, high, hidden, whole):
    interleave(x_ref[0], own, right, left, low, high, whole)
    planes, across, rows, columns = whole.shape
    weight = whole[...].reshape(planes * across * rows, columns)
    width = columns // 2
    both = jnp.dot(normed[...], weight, preferred_element_type=F32)
    gate, up = both[:, :width], both[:, width:]
    hidden[...] = (gate * jax.nn.sigmoid(gate) * up).astype(BF16)


def prepare_body(gate, up, down, both, copies):
    units = gate.shape[1]
    both[:, :units] = gate[...]
    both[:, units:] = up[...]
    for z in range(copies.shape[0]):
        copies[z] = down[...]


def partial_body(x_ref, c_ref, hidden, own, right, left, low, high, send, whole):
    interleave(x_ref[0], own, right, left, low, high, whole)
    send[...] = half_product(hidden, 1 - c_ref[0], whole)


def keep_body(c_ref, hidden, whole, keep):
    keep[...] = half_product(hidden, c_ref[0], whole)


def half_product(hidden, which, whole):
    half = hidden.shape[0] // 2
    lines = hidden[pl.ds(pl.multiple_of(which * half, 32), half), :]
    planes, across, rows, width = whole.shape
    return lax.dot_general(
        lines,
        whole[...].reshape(planes * across * rows, width),
        (((1,), (1,)), ((), ())),
        preferred_element_type=F32,
    ).astype(BF16)


def pair_sum_body(mine, theirs, out, total, folded):
    total[...] = mine[...].astype(F32) + theirs[...].astype(F32)
    count, lines, lanes = out.shape
    parts = total.shape[1] // lanes
    rows = lines // parts
    for j in range(count):
        for t in range(parts):
            folded[j, t * rows : (t + 1) * rows, :] = total[
                j * rows : (j + 1) * rows, t * lanes : (t + 1) * lanes
            ]
        out[j] = folded[j].astype(BF16)


def finish_body(pieces, tokens, gain, out, branch, full):
    count, _, lanes = pieces.shape
    total = pieces[0].astype(F32)
    for j in range(1, count):
        total = total + pieces[j].astype(F32)
    branch[...] = total
    rows, width = tokens.shape
    parts = [branch[t * rows : (t + 1) * rows, :] for t in range(width // lanes)]
    squares = parts[0] * parts[0]
    for value in parts[1:]:
        squares = squares + value * value
    scale = lax.rsqrt(jnp.sum(squares, axis=-1, keepdims=True) / width + epsilon)
    for t, value in enumerate(parts):
        columns = slice(t * lanes, (t + 1) * lanes)
        full[t * rows : (t + 1) * rows, :] = (
            tokens[:, columns] + value * scale * gain[columns][None]
        )
    out[...] = full[...].astype(BF16)


def join_body(c_ref, mine, theirs, out, folded, lines):
    count, _, lanes = mine.shape
    half, width = lines.shape[1:]
    rows = half // count
    for at, (source, which) in enumerate(((mine, c_ref[0]), (theirs, 1 - c_ref[0]))):
        for j in range(count):
            folded[at, j] = source[j].astype(F32)
            for t in range(width // lanes):
                lines[at, j * rows : (j + 1) * rows, t * lanes : (t + 1) * lanes] = (
                    folded[at, j, t * rows : (t + 1) * rows, :]
                )
        out[pl.ds(pl.multiple_of(which * half, 32), half), :] = lines[at].astype(BF16)


def per_device(tokens, norm_gain, gate_weight, up_weight, down_weight, branch_gain):
    places = [lax.axis_index(a).astype(jnp.int32)[None] for a in ("x", "y", "c")]
    gate_weight, x1, y1, c1 = lax.optimization_barrier((gate_weight, *places))
    n_x, n_y, n_z = (lax.axis_size(a) for a in ("x", "y", "z"))
    count, width = tokens.shape
    half, rows = count // 2, count // 2 // n_y
    units, piece = gate_weight.shape[1], gate_weight.shape[0]
    lanes = 128
    flat = (rows * width // lanes, lanes)

    own_both, copies = local_call(
        prepare_body,
        [
            jax.ShapeDtypeStruct((piece, 2 * units), BF16),
            jax.ShapeDtypeStruct((n_z, piece, units), BF16),
        ],
        n_in=3, limit=4,
    )(gate_weight, up_weight, down_weight.T)
    down_z = lax.all_to_all(copies, "z", 0, 0, tiled=True)
    both_z = lax.all_gather(own_both, "z")
    near = first_round(both_z)
    down_near = first_round(after(down_z, both_z))
    normed, own_tokens = local_call(
        norm_body,
        [jax.ShapeDtypeStruct((count, width), BF16), jax.ShapeDtypeStruct((rows, width), F32)],
        [VMEM((48, width), F32)],
        2, 2, 8,
    )(c1, y1, tokens, norm_gain)
    *near, normed = lax.optimization_barrier((*near, normed))
    far = second_round(*near)
    down_far = second_round(*down_near)
    hidden = local_call(
        hidden_body,
        jax.ShapeDtypeStruct((count, units), BF16),
        [VMEM((n_z, n_x, piece, 2 * units), BF16)],
        1, 6,
    )(x1, normed, both_z, *near, *far)

    send, whole = local_call(
        partial_body,
        [
            jax.ShapeDtypeStruct((half, width), BF16),
            jax.ShapeDtypeStruct((n_z, n_x, piece, units), BF16),
        ],
        (), 2, 6,
    )(x1, c1, hidden, down_z, *down_near, *down_far)
    theirs = shift(send, "c", 1)
    keep = local_call(
        keep_body, jax.ShapeDtypeStruct((half, width), BF16), (), 1, 2
    )(c1, hidden, whole)
    folded = (n_y, *flat)
    pair = local_call(
        pair_sum_body,
        jax.ShapeDtypeStruct(folded, BF16),
        [VMEM((half, width), F32), VMEM(folded, F32)],
        0, 2,
    )(keep, theirs)
    pieces = lax.all_to_all(pair, "y", 0, 0, tiled=True)
    done = local_call(
        finish_body,
        jax.ShapeDtypeStruct(flat, BF16),
        [VMEM(flat, F32)] * 2,
        0, 3,
    )(pieces, own_tokens, branch_gain)
    mine = lax.all_gather(done, "y")
    return local_call(
        join_body,
        jax.ShapeDtypeStruct((count, width), BF16),
        [VMEM((2, n_y, *flat), F32), VMEM((2, half, width), F32)],
        1, 2,
    )(c1, mine, shift(mine, "c", 1))


def solution(mesh):
    n_tp = mesh.shape["tp"]
    split = Mesh(mesh.devices.reshape(12, 4, n_tp // 2, 2), ("z", "x", "y", "c"))
    fs, tp = ("z", "x"), ("y", "c")
    placed = (P(fs, None), P(), P(fs, tp), P(fs, tp), P(tp, fs), P())

    return jax.shard_map(
        per_device, mesh=split, in_specs=placed, out_specs=P(fs, None), check_vma=False
    )
```

time: 185 us -> 185 us (level)
  blocking collectives: 56.1 us -> 92.1 us
  waiting for transfers between devices: 53.6 us -> 19.9 us
  starting transfers between devices: 51.8 us -> 58.8 us
  Pallas kernels: 13.3 us -> 8.72 us
  local copies, waits for them, and re-layouts: 8 us -> 4.59 us
    all_to_all x0 -> x1, blocking collectives: none -> 34.2 us  [per_device(): pieces = lax.all_to_all(pair, 'y', 0, 0, tiled=True)]
    all_to_all x1 -> x0, waiting for transfers between devices: 27.8 us -> none  [per_device(): pieces = lax.all_to_all(pair, 'y', 0, 0, tiled=True)]
    all_to_all x1, starting transfers between devices: 4.23 us -> 15.7 us  [per_device(): down_z = lax.all_to_all(copies, 'z', 0, 0, tiled=True)]
    all_to_all x1 -> x0, starting transfers between devices: 6.82 us -> none  [per_device(): pieces = lax.all_to_all(pair, 'y', 0, 0, tiled=True)]
    ppermute x10, waiting for transfers between devices: 25.8 us -> 19.9 us  [shift(): return lax.ppermute(value, axis, [(i, (i + by) % n) for i in range(n)])]
    ppermute x10, starting transfers between devices: 40.7 us -> 43.1 us  [shift(): return lax.ppermute(value, axis, [(i, (i + by) % n) for i in range(n)])]
    pallas_call x2, Pallas kernels: 2.16 us -> 0.1 us  [second_round(): local_call(halves_body, [part, part], n_in=2, limit=4)(left, right)]
    unnamed x14 -> x12, local copies, waits for them, and re-layouts: 5.44 us -> 4.59 us
  transfers between devices with their start and end apart: 12 -> 11, of which waited for: 9 -> 7; matrix products, arithmetic and copies ran while one was open for 1% -> 0% of each run, Pallas kernels for 3% -> 2%
where the time goes in v2:
time: 185 us; the launch traced here: 184 us
  blocking collectives  92.1 us (50%)
  starting transfers between devices  58.8 us (32%)
  waiting for transfers between devices  19.9 us (11%)
  Pallas kernels  8.72 us (5%)
  local copies, waits for them, and re-layouts  4.59 us (2%)
    ppermute x10, starting transfers between devices, shift(): return lax.ppermute(value, axis, [(i, (i + by) % n) for i in range(n)])  43.1 us
    all_gather x1, blocking collectives, per_device(): both_z = lax.all_gather(own_both, 'z')  36 us
    all_to_all x1, blocking collectives, per_device(): pieces = lax.all_to_all(pair, 'y', 0, 0, tiled=True)  34.2 us
    all_gather x1, blocking collectives, per_device(): mine = lax.all_gather(done, 'y')  21.9 us
    ppermute x10, waiting for transfers between devices, shift(): return lax.ppermute(value, axis, [(i, (i + by) % n) for i in range(n)])  19.9 us
    all_to_all x1, starting transfers between devices, per_device(): down_z = lax.all_to_all(copies, 'z', 0, 0, tiled=True)  15.7 us
    unnamed x12, local copies, waits for them, and re-layouts  4.59 us
  transfers between devices with their start and end apart: 11, of which 7 were waited for; matrix products, arithmetic and copies ran while one was open for 0% of the time, Pallas kernels for 2%

profile of v2, /device:TPU:1, one launch (start us, length us, event | category | flops | bytes accessed | tf_op | source)
XLA Modules:
  0.0 184.3 jit_solution(3459090591124278073)
XLA Ops:
  3.1 15.7 %all-to-all-start = ((bf16[12,48,384]{2,1,0:T(8,128)(2,1)}), bf16[12,48,384]{2,1,0:T(8,128)(2,1)S(1)}, u32[]{:S(2)}, u32[]{:S(2)}) async-start(bf16[12,48,384]{2,1,0:T(8,128)(2,1)} %get-tuple-element.34), calls=%async_computation | async-start | bytes 884736 | tf_op jit(solution)/shard_map/all_to_all | solution.py:189
  18.8 36.0 %all-gather = bf16[576,768]{1,0:T(8,128)(2,1)S(1)} all-gather(bf16[48,768]{1,0:T(8,128)(2,1)S(1)} %get-tuple-element.26), channel_id=2, replica_groups=mesh['z'=12,'x'=4,'y'=8,'c'=2] {'z'}, dimensions={0}, use_global_device_ids=true | all-gather | bytes 958464 | tf_op jit(solution)/shard_map/all_gather | solution.py:190
  54.9 4.4 %collective-permute-start = (bf16[12,48,768]{2,1,0:T(8,128)(2,1)S(1)}, bf16[12,48,768]{2,1,0:T(8,128)(2,1)S(1)}, u32[]{:S(2)}, u32[]{:S(2)}) collective-permute-start(bf16[12,48,768]{2,1,0:T(8,128)(2,1)S(1)} %bitcast.8), channel_id=1, source_target_pairs={{0,48},{16,0},{32,16},{48,32},{1,49},{17,1},{33,17},{49,33},{2,50}... | collective-permute-start | bytes 2654216 | tf_op jit(solution)/shard_map/ppermute | solution.py:18
  59.2 1.9 %collective-permute-start.1 = (bf16[12,48,768]{2,1,0:T(8,128)(2,1)S(1)}, bf16[12,48,768]{2,1,0:T(8,128)(2,1)S(1)}, u32[]{:S(2)}, u32[]{:S(2)}) collective-permute-start(bf16[12,48,768]{2,1,0:T(8,128)(2,1)S(1)} %bitcast.9), channel_id=1, source_target_pairs={{0,16},{16,32},{32,48},{48,0},{1,17},{17,33},{33,49},{49,1},{2,18}... | collective-permute-start | bytes 2654216 | tf_op jit(solution)/shard_map/ppermute | solution.py:18
  61.2 4.6 %collective-permute-start.4 = (bf16[12,48,384]{2,1,0:T(8,128)(2,1)S(1)}, bf16[12,48,384]{2,1,0:T(8,128)(2,1)S(1)}, u32[]{:S(2)}, u32[]{:S(2)}) collective-permute-start(bf16[12,48,384]{2,1,0:T(8,128)(2,1)S(1)} %all-to-all-done.own), channel_id=1, source_target_pairs={{0,48},{16,0},{32,16},{48,32},{1,49},{17,1},{33,17},{49,33},{2,50}... | collective-permute-start | bytes 1327112 | tf_op jit(solution)/shard_map/ppermute | solution.py:18
  65.8 1.9 %collective-permute-start.5 = (bf16[12,48,384]{2,1,0:T(8,128)(2,1)S(1)}, bf16[12,48,384]{2,1,0:T(8,128)(2,1)S(1)}, u32[]{:S(2)}, u32[]{:S(2)}) collective-permute-start(bf16[12,48,384]{2,1,0:T(8,128)(2,1)S(1)} %all-to-all-done.own), channel_id=1, source_target_pairs={{0,16},{16,32},{32,48},{48,0},{1,17},{17,33},{33,49},{49,1},{2,18}... | collective-permute-start | bytes 1327112 | tf_op jit(solution)/shard_map/ppermute | solution.py:18
  67.7 1.6 copy-done
  71.2 2.5 %collective-permute-done.right = bf16[12,48,768]{2,1,0:T(8,128)(2,1)S(1)} collective-permute-done((bf16[12,48,768]{2,1,0:T(8,128)(2,1)S(1)}, bf16[12,48,768]{2,1,0:T(8,128)(2,1)S(1)}, u32[]{:S(2)}, u32[]{:S(2)}) %collective-permute-start) | collective-permute-done | bytes 884768 | tf_op jit(solution)/shard_map/ppermute | solution.py:18
  73.7 5.0 %collective-permute-done.1.left = bf16[12,48,768]{2,1,0:T(8,128)(2,1)S(1)} collective-permute-done((bf16[12,48,768]{2,1,0:T(8,128)(2,1)S(1)}, bf16[12,48,768]{2,1,0:T(8,128)(2,1)S(1)}, u32[]{:S(2)}, u32[]{:S(2)}) %collective-permute-start.1) | collective-permute-done | bytes 884768 | tf_op jit(solution)/shard_map/ppermute | solution.py:18
  78.8 1.9 %collective-permute-start.2 = (bf16[6,48,768]{2,1,0:T(8,128)(2,1)S(1)}, bf16[6,48,768]{2,1,0:T(8,128)(2,1)S(1)}, u32[]{:S(2)}, u32[]{:S(2)}) collective-permute-start(bf16[6,48,768]{2,1,0:T(8,128)(2,1)S(1)} %get-tuple-element.32), channel_id=1, source_target_pairs={{0,16},{16,32},{32,48},{48,0},{1,17},{17,33},{33,49},{49,1},{2,18}... | collective-permute-start | bytes 1327112 | tf_op jit(solution)/shard_map/ppermute | solution.py:18
  80.8 4.6 %collective-permute-start.3 = (bf16[6,48,768]{2,1,0:T(8,128)(2,1)S(1)}, bf16[6,48,768]{2,1,0:T(8,128)(2,1)S(1)}, u32[]{:S(2)}, u32[]{:S(2)}) collective-permute-start(bf16[6,48,768]{2,1,0:T(8,128)(2,1)S(1)} %get-tuple-element.33), channel_id=1, source_target_pairs={{0,48},{16,0},{32,16},{48,32},{1,49},{17,1},{33,17},{49,33},{2,50}... | collective-permute-start | bytes 1327112 | tf_op jit(solution)/shard_map/ppermute | solution.py:18
  85.3 2.9 %collective-permute-done.5.left = bf16[12,48,384]{2,1,0:T(8,128)(2,1)S(1)} collective-permute-done((bf16[12,48,384]{2,1,0:T(8,128)(2,1)S(1)}, bf16[12,48,384]{2,1,0:T(8,128)(2,1)S(1)}, u32[]{:S(2)}, u32[]{:S(2)}) %collective-permute-start.5) | collective-permute-done | bytes 442400 | tf_op jit(solution)/shard_map/ppermute | solution.py:18
  88.3 1.9 %collective-permute-start.6 = (bf16[6,48,384]{2,1,0:T(8,128)(2,1)S(1)}, bf16[6,48,384]{2,1,0:T(8,128)(2,1)S(1)}, u32[]{:S(2)}, u32[]{:S(2)}) collective-permute-start(bf16[6,48,384]{2,1,0:T(8,128)(2,1)S(1)} %get-tuple-element.36), channel_id=1, source_target_pairs={{0,16},{16,32},{32,48},{48,0},{1,17},{17,33},{33,49},{49,1},{2,18}... | collective-permute-start | bytes 663560 | tf_op jit(solution)/shard_map/ppermute | solution.py:18
  90.2 4.6 %collective-permute-start.7 = (bf16[6,48,384]{2,1,0:T(8,128)(2,1)S(1)}, bf16[6,48,384]{2,1,0:T(8,128)(2,1)S(1)}, u32[]{:S(2)}, u32[]{:S(2)}) collective-permute-start(bf16[6,48,384]{2,1,0:T(8,128)(2,1)S(1)} %get-tuple-element.37), channel_id=1, source_target_pairs={{0,48},{16,0},{32,16},{48,32},{1,49},{17,1},{33,17},{49,33},{2,50}... | collective-permute-start | bytes 663560 | tf_op jit(solution)/shard_map/ppermute | solution.py:18
  94.8 2.9 %collective-permute-done.2.low = bf16[6,48,768]{2,1,0:T(8,128)(2,1)S(1)} collective-permute-done((bf16[6,48,768]{2,1,0:T(8,128)(2,1)S(1)}, bf16[6,48,768]{2,1,0:T(8,128)(2,1)S(1)}, u32[]{:S(2)}, u32[]{:S(2)}) %collective-permute-start.2) | collective-permute-done | bytes 442400 | tf_op jit(solution)/shard_map/ppermute | solution.py:18
  97.7 1.9 %shard_map.67.hidden = bf16[448,384]{1,0:T(8,128)(2,1)S(1)} custom-call(s32[1]{0:T(128)} %bitcast.x_ref, bf16[448,2304]{1,0:T(8,128)(2,1)S(1)} %get-tuple-element.29.normed, bf16[12,48,768]{2,1,0:T(8,128)(2,1)S(1)} %bitcast.10, bf16[12,48,768]{2,1,0:T(8,128)(2,1)S(1)} %collective-permute-done.right, bf16[12,48,768]{2,1,0:T(8,128)(2,1)S(1)} %collective-permute-done.1.left, ...), custom_call_target="tpu_custom_call" | custom-call | tf_op jit(solution)/shard_map/pallas_call | solution.py:202
  99.6 2.8 %collective-permute-done.6.low = bf16[6,48,384]{2,1,0:T(8,128)(2,1)S(1)} collective-permute-done((bf16[6,48,384]{2,1,0:T(8,128)(2,1)S(1)}, bf16[6,48,384]{2,1,0:T(8,128)(2,1)S(1)}, u32[]{:S(2)}, u32[]{:S(2)}) %collective-permute-start.6) | collective-permute-done | bytes 221216 | tf_op jit(solution)/shard_map/ppermute | solution.py:18
  103.5 9.1 %collective-permute-start.8 = (bf16[224,2304]{1,0:T(8,128)(2,1)S(1)}, bf16[224,2304]{1,0:T(8,128)(2,1)S(1)}, u32[]{:S(2)}, u32[]{:S(2)}) collective-permute-start(bf16[224,2304]{1,0:T(8,128)(2,1)S(1)} %get-tuple-element.39), channel_id=1, source_target_pairs={{0,1},{1,0},{2,3},{3,2},{4,5},{5,4},{6,7},{7,6},{8,9},{9,8},{10,11... | collective-permute-start | bytes 3096584 | tf_op jit(solution)/shard_map/ppermute | solution.py:18
  113.5 1.4 collective-permute-done.8.theirs
  115.4 34.2 %all_to_all.10.pieces = bf16[8,504,128]{2,1,0:T(8,128)(2,1)S(1)} all-to-all(bf16[8,504,128]{2,1,0:T(8,128)(2,1)S(1)} %shard_map.71), channel_id=1, replica_groups=mesh['z'=12,'x'=4,'y'=8,'c'=2] {'y'}, dimensions={0} | all-to-all | bytes 2064384 | tf_op jit(solution)/shard_map/all_to_all | solution.py:228
  149.9 21.9 %all-gather.1 = bf16[4032,128]{1,0:T(8,128)(2,1)S(1)} all-gather(bf16[504,128]{1,0:T(8,128)(2,1)S(1)} %shard_map.72), channel_id=3, replica_groups=mesh['z'=12,'x'=4,'y'=8,'c'=2] {'y'}, dimensions={0}, use_global_device_ids=true | all-gather | bytes 1161216 | tf_op jit(solution)/shard_map/all_gather | solution.py:235
  171.8 8.2 %collective-permute-start.9 = (bf16[8,504,128]{2,1,0:T(8,128)(2,1)S(1)}, bf16[8,504,128]{2,1,0:T(8,128)(2,1)S(1)}, u32[]{:S(2)}, u32[]{:S(2)}) collective-permute-start(bf16[8,504,128]{2,1,0:T(8,128)(2,1)S(1)} %bitcast.6), channel_id=1, source_target_pairs={{0,1},{1,0},{2,3},{3,2},{4,5},{5,4},{6,7},{7,6},{8,9},{9,8},{10,11... | collective-permute-start | bytes 3096584 | tf_op jit(solution)/shard_map/ppermute | solution.py:18
  180.0 2.2 %collective-permute-done.9.theirs = bf16[8,504,128]{2,1,0:T(8,128)(2,1)S(1)} collective-permute-done((bf16[8,504,128]{2,1,0:T(8,128)(2,1)S(1)}, bf16[8,504,128]{2,1,0:T(8,128)(2,1)S(1)}, u32[]{:S(2)}, u32[]{:S(2)}) %collective-permute-start.9) | collective-permute-done | bytes 1032224 | tf_op jit(solution)/shard_map/ppermute | solution.py:18
  182.2 2.0 %shard_map.73 = bf16[448,2304]{1,0:T(8,128)(2,1)} custom-call(s32[1]{0:T(128)} %bitcast.2.c_ref, bf16[8,504,128]{2,1,0:T(8,128)(2,1)S(1)} %bitcast.7, bf16[8,504,128]{2,1,0:T(8,128)(2,1)S(1)} %collective-permute-done.9.theirs), custom_call_target="tpu_custom_call" | custom-call | tf_op jit(solution)/shard_map/pallas_call | solution.py:236
  (23 shorter events, 7.8 us)
Async XLA Ops:
  0.0 0.8 copy-start.1
  0.8 0.8 copy-start.2
  1.5 0.8 copy-start.3
  3.1 58.1 %all-to-all-start = ((bf16[12,48,384]{2,1,0:T(8,128)(2,1)}), bf16[12,48,384]{2,1,0:T(8,128)(2,1)S(1)}, u32[]{:S(2)}, u32[]{:S(2)}) async-start(bf16[12,48,384]{2,1,0:T(8,128)(2,1)} %get-tuple-element.34), calls=%async_computation | async-start | bytes 884736 | tf_op jit(solution)/shard_map/all_to_all | solution.py:189
  54.9 18.9 %collective-permute-start = (bf16[12,48,768]{2,1,0:T(8,128)(2,1)S(1)}, bf16[12,48,768]{2,1,0:T(8,128)(2,1)S(1)}, u32[]{:S(2)}, u32[]{:S(2)}) collective-permute-start(bf16[12,48,768]{2,1,0:T(8,128)(2,1)S(1)} %bitcast.8), channel_id=1, source_target_pairs={{0,48},{16,0},{32,16},{48,32},{1,49},{17,1},{33,17},{49,33},{2,50}... | collective-permute-start | bytes 2654216 | tf_op jit(solution)/shard_map/ppermute | solution.py:18
  59.2 19.5 %collective-permute-start.1 = (bf16[12,48,768]{2,1,0:T(8,128)(2,1)S(1)}, bf16[12,48,768]{2,1,0:T(8,128)(2,1)S(1)}, u32[]{:S(2)}, u32[]{:S(2)}) collective-permute-start(bf16[12,48,768]{2,1,0:T(8,128)(2,1)S(1)} %bitcast.9), channel_id=1, source_target_pairs={{0,16},{16,32},{32,48},{48,0},{1,17},{17,33},{33,49},{49,1},{2,18}... | collective-permute-start | bytes 2654216 | tf_op jit(solution)/shard_map/ppermute | solution.py:18
  61.2 24.2 %collective-permute-start.4 = (bf16[12,48,384]{2,1,0:T(8,128)(2,1)S(1)}, bf16[12,48,384]{2,1,0:T(8,128)(2,1)S(1)}, u32[]{:S(2)}, u32[]{:S(2)}) collective-permute-start(bf16[12,48,384]{2,1,0:T(8,128)(2,1)S(1)} %all-to-all-done.own), channel_id=1, source_target_pairs={{0,48},{16,0},{32,16},{48,32},{1,49},{17,1},{33,17},{49,33},{2,50}... | collective-permute-start | bytes 1327112 | tf_op jit(solution)/shard_map/ppermute | solution.py:18
  65.8 22.5 %collective-permute-start.5 = (bf16[12,48,384]{2,1,0:T(8,128)(2,1)S(1)}, bf16[12,48,384]{2,1,0:T(8,128)(2,1)S(1)}, u32[]{:S(2)}, u32[]{:S(2)}) collective-permute-start(bf16[12,48,384]{2,1,0:T(8,128)(2,1)S(1)} %all-to-all-done.own), channel_id=1, source_target_pairs={{0,16},{16,32},{32,48},{48,0},{1,17},{17,33},{33,49},{49,1},{2,18}... | collective-permute-start | bytes 1327112 | tf_op jit(solution)/shard_map/ppermute | solution.py:18
  67.7 1.6 copy-start
  69.3 0.7 copy-start.4
  78.8 18.9 %collective-permute-start.2 = (bf16[6,48,768]{2,1,0:T(8,128)(2,1)S(1)}, bf16[6,48,768]{2,1,0:T(8,128)(2,1)S(1)}, u32[]{:S(2)}, u32[]{:S(2)}) collective-permute-start(bf16[6,48,768]{2,1,0:T(8,128)(2,1)S(1)} %get-tuple-element.32), channel_id=1, source_target_pairs={{0,16},{16,32},{32,48},{48,0},{1,17},{17,33},{33,49},{49,1},{2,18}... | collective-permute-start | bytes 1327112 | tf_op jit(solution)/shard_map/ppermute | solution.py:18
  80.8 17.0 %collective-permute-start.3 = (bf16[6,48,768]{2,1,0:T(8,128)(2,1)S(1)}, bf16[6,48,768]{2,1,0:T(8,128)(2,1)S(1)}, u32[]{:S(2)}, u32[]{:S(2)}) collective-permute-start(bf16[6,48,768]{2,1,0:T(8,128)(2,1)S(1)} %get-tuple-element.33), channel_id=1, source_target_pairs={{0,48},{16,0},{32,16},{48,32},{1,49},{17,1},{33,17},{49,33},{2,50}... | collective-permute-start | bytes 1327112 | tf_op jit(solution)/shard_map/ppermute | solution.py:18
  88.3 14.2 %collective-permute-start.6 = (bf16[6,48,384]{2,1,0:T(8,128)(2,1)S(1)}, bf16[6,48,384]{2,1,0:T(8,128)(2,1)S(1)}, u32[]{:S(2)}, u32[]{:S(2)}) collective-permute-start(bf16[6,48,384]{2,1,0:T(8,128)(2,1)S(1)} %get-tuple-element.36), channel_id=1, source_target_pairs={{0,16},{16,32},{32,48},{48,0},{1,17},{17,33},{33,49},{49,1},{2,18}... | collective-permute-start | bytes 663560 | tf_op jit(solution)/shard_map/ppermute | solution.py:18
  90.2 12.3 %collective-permute-start.7 = (bf16[6,48,384]{2,1,0:T(8,128)(2,1)S(1)}, bf16[6,48,384]{2,1,0:T(8,128)(2,1)S(1)}, u32[]{:S(2)}, u32[]{:S(2)}) collective-permute-start(bf16[6,48,384]{2,1,0:T(8,128)(2,1)S(1)} %get-tuple-element.37), channel_id=1, source_target_pairs={{0,48},{16,0},{32,16},{48,32},{1,49},{17,1},{33,17},{49,33},{2,50}... | collective-permute-start | bytes 663560 | tf_op jit(solution)/shard_map/ppermute | solution.py:18
  103.5 11.4 %collective-permute-start.8 = (bf16[224,2304]{1,0:T(8,128)(2,1)S(1)}, bf16[224,2304]{1,0:T(8,128)(2,1)S(1)}, u32[]{:S(2)}, u32[]{:S(2)}) collective-permute-start(bf16[224,2304]{1,0:T(8,128)(2,1)S(1)} %get-tuple-element.39), channel_id=1, source_target_pairs={{0,1},{1,0},{2,3},{3,2},{4,5},{5,4},{6,7},{7,6},{8,9},{9,8},{10,11... | collective-permute-start | bytes 3096584 | tf_op jit(solution)/shard_map/ppermute | solution.py:18
  113.4 36.1 %copy-start.5 = (f32[2304]{0:T(1024)S(1)}, f32[2304]{0:T(1024)}, u32[]{:S(2)}) copy-start(f32[2304]{0:T(1024)} %gain.3) | copy-start | bytes 27652
  171.8 10.5 %collective-permute-start.9 = (bf16[8,504,128]{2,1,0:T(8,128)(2,1)S(1)}, bf16[8,504,128]{2,1,0:T(8,128)(2,1)S(1)}, u32[]{:S(2)}, u32[]{:S(2)}) collective-permute-start(bf16[8,504,128]{2,1,0:T(8,128)(2,1)S(1)} %bitcast.6), channel_id=1, source_target_pairs={{0,1},{1,0},{2,3},{3,2},{4,5},{5,4},{6,7},{7,6},{8,9},{9,8},{10,11... | collective-permute-start | bytes 3096584 | tf_op jit(solution)/shard_map/ppermute | solution.py:18

commit v3 on v2

--- a/solution.py
+++ b/solution.py
@@ -92,12 +92,9 @@
     hidden[...] = (gate * jax.nn.sigmoid(gate) * up).astype(BF16)
 
 
-def prepare_body(gate, up, down, both, copies):
-    units = gate.shape[1]
-    both[:, :units] = gate[...]
-    both[:, units:] = up[...]
+def copies_body(value, copies):
     for z in range(copies.shape[0]):
-        copies[z] = down[...]
+        copies[z] = value[...]
 
 
 def partial_body(x_ref, c_ref, hidden, own, right, left, low, high, send, whole):
@@ -178,33 +175,29 @@
     lanes = 128
     flat = (rows * width // lanes, lanes)
 
-    own_both, copies = local_call(
-        prepare_body,
-        [
-            jax.ShapeDtypeStruct((piece, 2 * units), BF16),
-            jax.ShapeDtypeStruct((n_z, piece, units), BF16),
-        ],
-        n_in=3, limit=4,
-    )(gate_weight, up_weight, down_weight.T)
-    down_z = lax.all_to_all(copies, "z", 0, 0, tiled=True)
+    own_both = jnp.concatenate([gate_weight, up_weight], axis=1)
     both_z = lax.all_gather(own_both, "z")
     near = first_round(both_z)
-    down_near = first_round(after(down_z, both_z))
+    copies = local_call(
+        copies_body, jax.ShapeDtypeStruct((n_z, piece, units), BF16), n_in=1, limit=2
+    )(after(down_weight.T, both_z))
+    down_z = lax.all_to_all(copies, "z", 0, 0, tiled=True)
+    far = second_round(*near)
+    down_near = first_round(after(down_z, *near))
     normed, own_tokens = local_call(
         norm_body,
         [jax.ShapeDtypeStruct((count, width), BF16), jax.ShapeDtypeStruct((rows, width), F32)],
         [VMEM((48, width), F32)],
         2, 2, 8,
-    )(c1, y1, tokens, norm_gain)
-    *near, normed = lax.optimization_barrier((*near, normed))
-    far = second_round(*near)
-    down_far = second_round(*down_near)
+    )(c1, y1, after(tokens, down_z), norm_gain)
     hidden = local_call(
         hidden_body,
         jax.ShapeDtypeStruct((count, units), BF16),
         [VMEM((n_z, n_x, piece, 2 * units), BF16)],
         1, 6,
     )(x1, normed, both_z, *near, *far)
+    *down_near, hidden = lax.optimization_barrier((*down_near, hidden))
+    down_far = second_round(*down_near)
 
     send, whole = local_call(
         partial_body,

time: 185 us -> 177 us (0.957)
  starting transfers between devices: 58.8 us -> 44.1 us
  waiting for transfers between devices: 19.9 us -> 28.6 us
  blocking collectives: 92.1 us -> 89.4 us
  local copies, waits for them, and re-layouts: 4.59 us -> 2.35 us
  Pallas kernels: 8.72 us -> 10.6 us
    all_to_all x1, starting transfers between devices: 15.7 us -> 3.58 us  [per_device(): down_z = lax.all_to_all(copies, 'z', 0, 0, tiled=True)]
    ppermute x10, waiting for transfers between devices: 19.9 us -> 28.6 us  [shift(): return lax.ppermute(value, axis, [(i, (i + by) % n) for i in range(n)])]
    all_gather x1, blocking collectives: 36 us -> 33.3 us  [per_device(): both_z = lax.all_gather(own_both, 'z')]
    ppermute x10, starting transfers between devices: 43.1 us -> 40.5 us  [shift(): return lax.ppermute(value, axis, [(i, (i + by) % n) for i in range(n)])]
    unnamed x12 -> x8, local copies, waits for them, and re-layouts: 4.59 us -> 2.35 us
  transfers between devices with their start and end apart: 11 -> 11, of which waited for: 7 -> 8; matrix products, arithmetic and copies ran while one was open for 0% -> 0% of each run, Pallas kernels for 2% -> 3%
where the time goes in v3:
time: 177 us; the launch traced here: 176 us
  blocking collectives  89.4 us (51%)
  starting transfers between devices  44.1 us (25%)
  waiting for transfers between devices  28.6 us (16%)
  Pallas kernels  10.6 us (6%)
  local copies, waits for them, and re-layouts  2.35 us (1%)
    ppermute x10, starting transfers between devices, shift(): return lax.ppermute(value, axis, [(i, (i + by) % n) for i in range(n)])  40.5 us
    all_to_all x1, blocking collectives, per_device(): pieces = lax.all_to_all(pair, 'y', 0, 0, tiled=True)  34.2 us
    all_gather x1, blocking collectives, per_device(): both_z = lax.all_gather(own_both, 'z')  33.3 us
    ppermute x10, waiting for transfers between devices, shift(): return lax.ppermute(value, axis, [(i, (i + by) % n) for i in range(n)])  28.6 us
    all_gather x1, blocking collectives, per_device(): mine = lax.all_gather(done, 'y')  21.9 us
    all_to_all x1, starting transfers between devices, per_device(): down_z = lax.all_to_all(copies, 'z', 0, 0, tiled=True)  3.58 us
  transfers between devices with their start and end apart: 11, of which 8 were waited for; matrix products, arithmetic and copies ran while one was open for 0% of the time, Pallas kernels for 3%

profile of v3, /device:TPU:1, one launch (start us, length us, event | category | flops | bytes accessed | tf_op | source)
XLA Modules:
  0.0 176.1 jit_solution(6969311493782753345)
XLA Ops:
  0.8 33.3 %all-gather = bf16[576,768]{1,0:T(8,128)(2,1)S(1)} all-gather(bf16[48,768]{1,0:T(8,128)(2,1)S(1)} %pad_maximum_fusion), channel_id=2, replica_groups=mesh['z'=12,'x'=4,'y'=8,'c'=2] {'z'}, dimensions={0}, use_global_device_ids=true | all-gather | bytes 958464 | tf_op jit(solution)/shard_map/all_gather | solution.py:179
  35.7 3.6 %all-to-all-start = ((bf16[12,48,384]{2,1,0:T(8,128)(2,1)}), bf16[12,48,384]{2,1,0:T(8,128)(2,1)S(1)}, u32[]{:S(2)}, u32[]{:S(2)}) async-start(bf16[12,48,384]{2,1,0:T(8,128)(2,1)} %shard_map.64), calls=%async_computation | async-start | bytes 884736 | tf_op jit(solution)/shard_map/all_to_all | solution.py:184
  39.3 4.4 %collective-permute-start = (bf16[12,48,768]{2,1,0:T(8,128)(2,1)S(1)}, bf16[12,48,768]{2,1,0:T(8,128)(2,1)S(1)}, u32[]{:S(2)}, u32[]{:S(2)}) collective-permute-start(bf16[12,48,768]{2,1,0:T(8,128)(2,1)S(1)} %bitcast.8), channel_id=1, source_target_pairs={{0,48},{16,0},{32,16},{48,32},{1,49},{17,1},{33,17},{49,33},{2,50}... | collective-permute-start | bytes 2654216 | tf_op jit(solution)/shard_map/ppermute | solution.py:18
  43.7 1.9 %collective-permute-start.1 = (bf16[12,48,768]{2,1,0:T(8,128)(2,1)S(1)}, bf16[12,48,768]{2,1,0:T(8,128)(2,1)S(1)}, u32[]{:S(2)}, u32[]{:S(2)}) collective-permute-start(bf16[12,48,768]{2,1,0:T(8,128)(2,1)S(1)} %bitcast.9), channel_id=1, source_target_pairs={{0,16},{16,32},{32,48},{48,0},{1,17},{17,33},{33,49},{49,1},{2,18}... | collective-permute-start | bytes 2654216 | tf_op jit(solution)/shard_map/ppermute | solution.py:18
  45.6 10.9 %collective-permute-done.right = bf16[12,48,768]{2,1,0:T(8,128)(2,1)S(1)} collective-permute-done((bf16[12,48,768]{2,1,0:T(8,128)(2,1)S(1)}, bf16[12,48,768]{2,1,0:T(8,128)(2,1)S(1)}, u32[]{:S(2)}, u32[]{:S(2)}) %collective-permute-start) | collective-permute-done | bytes 884768 | tf_op jit(solution)/shard_map/ppermute | solution.py:18
  56.5 5.0 %collective-permute-done.1.left = bf16[12,48,768]{2,1,0:T(8,128)(2,1)S(1)} collective-permute-done((bf16[12,48,768]{2,1,0:T(8,128)(2,1)S(1)}, bf16[12,48,768]{2,1,0:T(8,128)(2,1)S(1)}, u32[]{:S(2)}, u32[]{:S(2)}) %collective-permute-start.1) | collective-permute-done | bytes 884768 | tf_op jit(solution)/shard_map/ppermute | solution.py:18
  62.5 1.9 %collective-permute-start.4 = (bf16[6,48,768]{2,1,0:T(8,128)(2,1)}, bf16[6,48,768]{2,1,0:T(8,128)(2,1)S(1)}, u32[]{:S(2)}, u32[]{:S(2)}) collective-permute-start(bf16[6,48,768]{2,1,0:T(8,128)(2,1)} %get-tuple-element.31), channel_id=1, source_target_pairs={{0,16},{16,32},{32,48},{48,0},{1,17},{17,33},{33,49},{49,1},{2,18}... | collective-permute-start | bytes 1327112 | tf_op jit(solution)/shard_map/ppermute | solution.py:18
  64.5 4.6 %collective-permute-start.5 = (bf16[6,48,768]{2,1,0:T(8,128)(2,1)}, bf16[6,48,768]{2,1,0:T(8,128)(2,1)}, u32[]{:S(2)}, u32[]{:S(2)}) collective-permute-start(bf16[6,48,768]{2,1,0:T(8,128)(2,1)} %get-tuple-element.32), channel_id=1, source_target_pairs={{0,48},{16,0},{32,16},{48,32},{1,49},{17,1},{33,17},{49,33},{2,50}... | collective-permute-start | bytes 1327112 | tf_op jit(solution)/shard_map/ppermute | solution.py:18
  69.0 1.9 %collective-permute-start.2 = (bf16[12,48,384]{2,1,0:T(8,128)(2,1)S(1)}, bf16[12,48,384]{2,1,0:T(8,128)(2,1)S(1)}, u32[]{:S(2)}, u32[]{:S(2)}) collective-permute-start(bf16[12,48,384]{2,1,0:T(8,128)(2,1)S(1)} %all-to-all-done.own), channel_id=1, source_target_pairs={{0,48},{16,0},{32,16},{48,32},{1,49},{17,1},{33,17},{49,33},{2,50}... | collective-permute-start | bytes 1327112 | tf_op jit(solution)/shard_map/ppermute | solution.py:18
  71.0 3.4 %collective-permute-start.3 = (bf16[12,48,384]{2,1,0:T(8,128)(2,1)S(1)}, bf16[12,48,384]{2,1,0:T(8,128)(2,1)S(1)}, u32[]{:S(2)}, u32[]{:S(2)}) collective-permute-start(bf16[12,48,384]{2,1,0:T(8,128)(2,1)S(1)} %all-to-all-done.own), channel_id=1, source_target_pairs={{0,16},{16,32},{32,48},{48,0},{1,17},{17,33},{33,49},{49,1},{2,18}... | collective-permute-start | bytes 1327112 | tf_op jit(solution)/shard_map/ppermute | solution.py:18
  74.4 1.6 copy-done
  77.2 2.9 %shard_map.67.hidden = bf16[448,384]{1,0:T(8,128)(2,1)S(1)} custom-call(s32[1]{0:T(128)} %bitcast.x_ref, bf16[448,2304]{1,0:T(8,128)(2,1)S(1)} %get-tuple-element.30.normed, bf16[12,48,768]{2,1,0:T(8,128)(2,1)S(1)} %bitcast.10, bf16[12,48,768]{2,1,0:T(8,128)(2,1)S(1)} %collective-permute-done.right, bf16[12,48,768]{2,1,0:T(8,128)(2,1)S(1)} %collective-permute-done.1.left, ...), custom_call_target="tpu_custom_call" | custom-call | tf_op jit(solution)/shard_map/pallas_call | solution.py:193
  80.6 5.6 %collective-permute-done.3.left = bf16[12,48,384]{2,1,0:T(8,128)(2,1)S(1)} collective-permute-done((bf16[12,48,384]{2,1,0:T(8,128)(2,1)S(1)}, bf16[12,48,384]{2,1,0:T(8,128)(2,1)S(1)}, u32[]{:S(2)}, u32[]{:S(2)}) %collective-permute-start.3) | collective-permute-done | bytes 442400 | tf_op jit(solution)/shard_map/ppermute | solution.py:18
  86.3 1.9 %collective-permute-start.6 = (bf16[6,48,384]{2,1,0:T(8,128)(2,1)S(1)}, bf16[6,48,384]{2,1,0:T(8,128)(2,1)S(1)}, u32[]{:S(2)}, u32[]{:S(2)}) collective-permute-start(bf16[6,48,384]{2,1,0:T(8,128)(2,1)S(1)} %get-tuple-element.36), channel_id=1, source_target_pairs={{0,16},{16,32},{32,48},{48,0},{1,17},{17,33},{33,49},{49,1},{2,18}... | collective-permute-start | bytes 663560 | tf_op jit(solution)/shard_map/ppermute | solution.py:18
  88.2 4.6 %collective-permute-start.7 = (bf16[6,48,384]{2,1,0:T(8,128)(2,1)S(1)}, bf16[6,48,384]{2,1,0:T(8,128)(2,1)S(1)}, u32[]{:S(2)}, u32[]{:S(2)}) collective-permute-start(bf16[6,48,384]{2,1,0:T(8,128)(2,1)S(1)} %get-tuple-element.37), channel_id=1, source_target_pairs={{0,48},{16,0},{32,16},{48,32},{1,49},{17,1},{33,17},{49,33},{2,50}... | collective-permute-start | bytes 663560 | tf_op jit(solution)/shard_map/ppermute | solution.py:18
  92.8 1.4 collective-permute-done.6.low
  94.2 1.5 collective-permute-done.7.high
  96.7 7.7 %collective-permute-start.8 = (bf16[224,2304]{1,0:T(8,128)(2,1)S(1)}, bf16[224,2304]{1,0:T(8,128)(2,1)S(1)}, u32[]{:S(2)}, u32[]{:S(2)}) collective-permute-start(bf16[224,2304]{1,0:T(8,128)(2,1)S(1)} %get-tuple-element.39), channel_id=1, source_target_pairs={{0,1},{1,0},{2,3},{3,2},{4,5},{5,4},{6,7},{7,6},{8,9},{9,8},{10,11... | collective-permute-start | bytes 3096584 | tf_op jit(solution)/shard_map/ppermute | solution.py:18
  105.2 1.4 collective-permute-done.8.theirs
  107.2 34.2 %all_to_all.10.pieces = bf16[8,504,128]{2,1,0:T(8,128)(2,1)S(1)} all-to-all(bf16[8,504,128]{2,1,0:T(8,128)(2,1)S(1)} %shard_map.71), channel_id=1, replica_groups=mesh['z'=12,'x'=4,'y'=8,'c'=2] {'y'}, dimensions={0} | all-to-all | bytes 2064384 | tf_op jit(solution)/shard_map/all_to_all | solution.py:221
  141.7 21.9 %all-gather.1 = bf16[4032,128]{1,0:T(8,128)(2,1)S(1)} all-gather(bf16[504,128]{1,0:T(8,128)(2,1)S(1)} %shard_map.72), channel_id=3, replica_groups=mesh['z'=12,'x'=4,'y'=8,'c'=2] {'y'}, dimensions={0}, use_global_device_ids=true | all-gather | bytes 1161216 | tf_op jit(solution)/shard_map/all_gather | solution.py:228
  163.6 8.2 %collective-permute-start.9 = (bf16[8,504,128]{2,1,0:T(8,128)(2,1)S(1)}, bf16[8,504,128]{2,1,0:T(8,128)(2,1)S(1)}, u32[]{:S(2)}, u32[]{:S(2)}) collective-permute-start(bf16[8,504,128]{2,1,0:T(8,128)(2,1)S(1)} %bitcast.6), channel_id=1, source_target_pairs={{0,1},{1,0},{2,3},{3,2},{4,5},{5,4},{6,7},{7,6},{8,9},{9,8},{10,11... | collective-permute-start | bytes 3096584 | tf_op jit(solution)/shard_map/ppermute | solution.py:18
  171.8 2.2 %collective-permute-done.9.theirs = bf16[8,504,128]{2,1,0:T(8,128)(2,1)S(1)} collective-permute-done((bf16[8,504,128]{2,1,0:T(8,128)(2,1)S(1)}, bf16[8,504,128]{2,1,0:T(8,128)(2,1)S(1)}, u32[]{:S(2)}, u32[]{:S(2)}) %collective-permute-start.9) | collective-permute-done | bytes 1032224 | tf_op jit(solution)/shard_map/ppermute | solution.py:18
  174.0 2.0 %shard_map.73 = bf16[448,2304]{1,0:T(8,128)(2,1)} custom-call(s32[1]{0:T(128)} %bitcast.2.c_ref, bf16[8,504,128]{2,1,0:T(8,128)(2,1)S(1)} %bitcast.7, bf16[8,504,128]{2,1,0:T(8,128)(2,1)S(1)} %collective-permute-done.9.theirs), custom_call_target="tpu_custom_call" | custom-call | tf_op jit(solution)/shard_map/pallas_call | solution.py:229
  (20 shorter events, 7.8 us)
Async XLA Ops:
  0.8 73.5 %copy-start.2 = (f32[2304]{0:T(1024)S(1)}, f32[2304]{0:T(1024)}, u32[]{:S(2)}) copy-start(f32[2304]{0:T(1024)} %gain.2) | copy-start | bytes 27652
  34.1 0.8 copy-start.1
  35.7 33.3 %all-to-all-start = ((bf16[12,48,384]{2,1,0:T(8,128)(2,1)}), bf16[12,48,384]{2,1,0:T(8,128)(2,1)S(1)}, u32[]{:S(2)}, u32[]{:S(2)}) async-start(bf16[12,48,384]{2,1,0:T(8,128)(2,1)} %shard_map.64), calls=%async_computation | async-start | bytes 884736 | tf_op jit(solution)/shard_map/all_to_all | solution.py:184
  39.3 17.2 %collective-permute-start = (bf16[12,48,768]{2,1,0:T(8,128)(2,1)S(1)}, bf16[12,48,768]{2,1,0:T(8,128)(2,1)S(1)}, u32[]{:S(2)}, u32[]{:S(2)}) collective-permute-start(bf16[12,48,768]{2,1,0:T(8,128)(2,1)S(1)} %bitcast.8), channel_id=1, source_target_pairs={{0,48},{16,0},{32,16},{48,32},{1,49},{17,1},{33,17},{49,33},{2,50}... | collective-permute-start | bytes 2654216 | tf_op jit(solution)/shard_map/ppermute | solution.py:18
  43.7 17.9 %collective-permute-start.1 = (bf16[12,48,768]{2,1,0:T(8,128)(2,1)S(1)}, bf16[12,48,768]{2,1,0:T(8,128)(2,1)S(1)}, u32[]{:S(2)}, u32[]{:S(2)}) collective-permute-start(bf16[12,48,768]{2,1,0:T(8,128)(2,1)S(1)} %bitcast.9), channel_id=1, source_target_pairs={{0,16},{16,32},{32,48},{48,0},{1,17},{17,33},{33,49},{49,1},{2,18}... | collective-permute-start | bytes 2654216 | tf_op jit(solution)/shard_map/ppermute | solution.py:18
  62.5 14.7 %collective-permute-start.4 = (bf16[6,48,768]{2,1,0:T(8,128)(2,1)}, bf16[6,48,768]{2,1,0:T(8,128)(2,1)S(1)}, u32[]{:S(2)}, u32[]{:S(2)}) collective-permute-start(bf16[6,48,768]{2,1,0:T(8,128)(2,1)} %get-tuple-element.31), channel_id=1, source_target_pairs={{0,16},{16,32},{32,48},{48,0},{1,17},{17,33},{33,49},{49,1},{2,18}... | collective-permute-start | bytes 1327112 | tf_op jit(solution)/shard_map/ppermute | solution.py:18
  64.5 12.8 %collective-permute-start.5 = (bf16[6,48,768]{2,1,0:T(8,128)(2,1)}, bf16[6,48,768]{2,1,0:T(8,128)(2,1)}, u32[]{:S(2)}, u32[]{:S(2)}) collective-permute-start(bf16[6,48,768]{2,1,0:T(8,128)(2,1)} %get-tuple-element.32), channel_id=1, source_target_pairs={{0,48},{16,0},{32,16},{48,32},{1,49},{17,1},{33,17},{49,33},{2,50}... | collective-permute-start | bytes 1327112 | tf_op jit(solution)/shard_map/ppermute | solution.py:18
  69.0 11.6 %collective-permute-start.2 = (bf16[12,48,384]{2,1,0:T(8,128)(2,1)S(1)}, bf16[12,48,384]{2,1,0:T(8,128)(2,1)S(1)}, u32[]{:S(2)}, u32[]{:S(2)}) collective-permute-start(bf16[12,48,384]{2,1,0:T(8,128)(2,1)S(1)} %all-to-all-done.own), channel_id=1, source_target_pairs={{0,48},{16,0},{32,16},{48,32},{1,49},{17,1},{33,17},{49,33},{2,50}... | collective-permute-start | bytes 1327112 | tf_op jit(solution)/shard_map/ppermute | solution.py:18
  71.0 15.3 %collective-permute-start.3 = (bf16[12,48,384]{2,1,0:T(8,128)(2,1)S(1)}, bf16[12,48,384]{2,1,0:T(8,128)(2,1)S(1)}, u32[]{:S(2)}, u32[]{:S(2)}) collective-permute-start(bf16[12,48,384]{2,1,0:T(8,128)(2,1)S(1)} %all-to-all-done.own), channel_id=1, source_target_pairs={{0,16},{16,32},{32,48},{48,0},{1,17},{17,33},{33,49},{49,1},{2,18}... | collective-permute-start | bytes 1327112 | tf_op jit(solution)/shard_map/ppermute | solution.py:18
  74.4 1.6 copy-start
  86.3 7.9 %collective-permute-start.6 = (bf16[6,48,384]{2,1,0:T(8,128)(2,1)S(1)}, bf16[6,48,384]{2,1,0:T(8,128)(2,1)S(1)}, u32[]{:S(2)}, u32[]{:S(2)}) collective-permute-start(bf16[6,48,384]{2,1,0:T(8,128)(2,1)S(1)} %get-tuple-element.36), channel_id=1, source_target_pairs={{0,16},{16,32},{32,48},{48,0},{1,17},{17,33},{33,49},{49,1},{2,18}... | collective-permute-start | bytes 663560 | tf_op jit(solution)/shard_map/ppermute | solution.py:18
  88.2 7.4 %collective-permute-start.7 = (bf16[6,48,384]{2,1,0:T(8,128)(2,1)S(1)}, bf16[6,48,384]{2,1,0:T(8,128)(2,1)S(1)}, u32[]{:S(2)}, u32[]{:S(2)}) collective-permute-start(bf16[6,48,384]{2,1,0:T(8,128)(2,1)S(1)} %get-tuple-element.37), channel_id=1, source_target_pairs={{0,48},{16,0},{32,16},{48,32},{1,49},{17,1},{33,17},{49,33},{2,50}... | collective-permute-start | bytes 663560 | tf_op jit(solution)/shard_map/ppermute | solution.py:18
  96.7 10.0 %collective-permute-start.8 = (bf16[224,2304]{1,0:T(8,128)(2,1)S(1)}, bf16[224,2304]{1,0:T(8,128)(2,1)S(1)}, u32[]{:S(2)}, u32[]{:S(2)}) collective-permute-start(bf16[224,2304]{1,0:T(8,128)(2,1)S(1)} %get-tuple-element.39), channel_id=1, source_target_pairs={{0,1},{1,0},{2,3},{3,2},{4,5},{5,4},{6,7},{7,6},{8,9},{9,8},{10,11... | collective-permute-start | bytes 3096584 | tf_op jit(solution)/shard_map/ppermute | solution.py:18
  105.2 36.1 %copy-start.3 = (f32[2304]{0:T(1024)S(1)}, f32[2304]{0:T(1024)}, u32[]{:S(2)}) copy-start(f32[2304]{0:T(1024)} %gain.3) | copy-start | bytes 27652
  163.6 10.5 %collective-permute-start.9 = (bf16[8,504,128]{2,1,0:T(8,128)(2,1)S(1)}, bf16[8,504,128]{2,1,0:T(8,128)(2,1)S(1)}, u32[]{:S(2)}, u32[]{:S(2)}) collective-permute-start(bf16[8,504,128]{2,1,0:T(8,128)(2,1)S(1)} %bitcast.6), channel_id=1, source_target_pairs={{0,1},{1,0},{2,3},{3,2},{4,5},{5,4},{6,7},{7,6},{8,9},{9,8},{10,11... | collective-permute-start | bytes 3096584 | tf_op jit(solution)/shard_map/ppermute | solution.py:18

commit v4 on v3

--- a/solution.py
+++ b/solution.py
@@ -72,18 +72,17 @@
             own[...] = window[skip : skip + rows, :]
 
 
-def interleave(x, own, right, left, low, high, whole):
-    slots = [lax.rem(x + k, 4) for k in range(4)]
-    half = low.shape[0]
-    for z in range(own.shape[0]):
-        whole[z, slots[0]] = own[z]
-        whole[z, slots[1]] = right[z]
-        whole[z, slots[3]] = left[z]
-        whole[z, slots[2]] = low[z] if z < half else high[z - half]
+def interleave(x, blocks, whole):
+    for offset, block in enumerate(blocks):
+        at = lax.rem(x + offset, len(blocks))
+        for first, piece in block:
+            for z in range(piece.shape[0]):
+                whole[first + z, at] = piece[z]
 
 
 def hidden_body(x_ref, normed, own, right, left, low, high, hidden, whole):
-    interleave(x_ref[0], own, right, left, low, high, whole)
+    far = ((0, low), (low.shape[0], high))
+    interleave(x_ref[0], (((0, own),), ((0, right),), far, ((0, left),)), whole)
     planes, across, rows, columns = whole.shape
     weight = whole[...].reshape(planes * across * rows, columns)
     width = columns // 2
@@ -97,8 +96,8 @@
         copies[z] = value[...]
 
 
-def partial_body(x_ref, c_ref, hidden, own, right, left, low, high, send, whole):
-    interleave(x_ref[0], own, right, left, low, high, whole)
+def partial_body(x_ref, c_ref, hidden, own, right, left, far, send, whole):
+    interleave(x_ref[0], [((0, block),) for block in (own, right, far, left)], whole)
     send[...] = half_product(hidden, 1 - c_ref[0], whole)
 
 
@@ -183,7 +182,8 @@
     )(after(down_weight.T, both_z))
     down_z = lax.all_to_all(copies, "z", 0, 0, tiled=True)
     far = second_round(*near)
-    down_near = first_round(after(down_z, *near))
+    down_z = after(down_z, *near)
+    down = (*first_round(down_z), shift(down_z, "x", 2))
     normed, own_tokens = local_call(
         norm_body,
         [jax.ShapeDtypeStruct((count, width), BF16), jax.ShapeDtypeStruct((rows, width), F32)],
@@ -196,17 +196,14 @@
         [VMEM((n_z, n_x, piece, 2 * units), BF16)],
         1, 6,
     )(x1, normed, both_z, *near, *far)
-    *down_near, hidden = lax.optimization_barrier((*down_near, hidden))
-    down_far = second_round(*down_near)
-
     send, whole = local_call(
         partial_body,
         [
             jax.ShapeDtypeStruct((half, width), BF16),
             jax.ShapeDtypeStruct((n_z, n_x, piece, units), BF16),
         ],
-        (), 2, 6,
-    )(x1, c1, hidden, down_z, *down_near, *down_far)
+        (), 2, 5,
+    )(x1, c1, hidden, down_z, *down)
     theirs = shift(send, "c", 1)
     keep = local_call(
         keep_body, jax.ShapeDtypeStruct((half, width), BF16), (), 1, 2

time: 177 us -> 176 us (level)
  starting transfers between devices: 44.1 us -> 39.8 us
  waiting for transfers between devices: 28.6 us -> 31.8 us
    ppermute x10 -> x9, starting transfers between devices: 40.5 us -> 36.3 us  [shift(): return lax.ppermute(value, axis, [(i, (i + by) % n) for i in range(n)])]
    ppermute x10 -> x9, waiting for transfers between devices: 28.6 us -> 31.8 us  [shift(): return lax.ppermute(value, axis, [(i, (i + by) % n) for i in range(n)])]
  transfers between devices with their start and end apart: 11 -> 10, of which waited for: 8 -> 6; matrix products, arithmetic and copies ran while one was open for 0% -> 0% of each run, Pallas kernels for 3% -> 3%
where the time goes in v4:
time: 176 us; the launch traced here: 175 us
  blocking collectives  89.4 us (51%)
  starting transfers between devices  39.8 us (23%)
  waiting for transfers between devices  31.8 us (18%)
  Pallas kernels  10.6 us (6%)
  local copies, waits for them, and re-layouts  2.35 us (1%)
    ppermute x9, starting transfers between devices, shift(): return lax.ppermute(value, axis, [(i, (i + by) % n) for i in range(n)])  36.3 us
    all_to_all x1, blocking collectives, per_device(): pieces = lax.all_to_all(pair, 'y', 0, 0, tiled=True)  34.2 us
    all_gather x1, blocking collectives, per_device(): both_z = lax.all_gather(own_both, 'z')  33.3 us
    ppermute x9, waiting for transfers between devices, shift(): return lax.ppermute(value, axis, [(i, (i + by) % n) for i in range(n)])  31.8 us
    all_gather x1, blocking collectives, per_device(): mine = lax.all_gather(done, 'y')  21.9 us
    all_to_all x1, starting transfers between devices, per_device(): down_z = lax.all_to_all(copies, 'z', 0, 0, tiled=True)  3.58 us
  transfers between devices with their start and end apart: 10, of which 6 were waited for; matrix products, arithmetic and copies ran while one was open for 0% of the time, Pallas kernels for 3%

profile of v4, /device:TPU:1, one launch (start us, length us, event | category | flops | bytes accessed | tf_op | source)
XLA Modules:
  0.0 175.0 jit_solution(7821162938834824644)
XLA Ops:
  0.8 33.3 %all-gather = bf16[576,768]{1,0:T(8,128)(2,1)S(1)} all-gather(bf16[48,768]{1,0:T(8,128)(2,1)S(1)} %pad_maximum_fusion), channel_id=2, replica_groups=mesh['z'=12,'x'=4,'y'=8,'c'=2] {'z'}, dimensions={0}, use_global_device_ids=true | all-gather | bytes 958464 | tf_op jit(solution)/shard_map/all_gather | solution.py:178
  35.7 3.6 %all-to-all-start = ((bf16[12,48,384]{2,1,0:T(8,128)(2,1)}), bf16[12,48,384]{2,1,0:T(8,128)(2,1)S(1)}, u32[]{:S(2)}, u32[]{:S(2)}) async-start(bf16[12,48,384]{2,1,0:T(8,128)(2,1)} %shard_map.64), calls=%async_computation | async-start | bytes 884736 | tf_op jit(solution)/shard_map/all_to_all | solution.py:183
  39.3 4.4 %collective-permute-start = (bf16[12,48,768]{2,1,0:T(8,128)(2,1)S(1)}, bf16[12,48,768]{2,1,0:T(8,128)(2,1)S(1)}, u32[]{:S(2)}, u32[]{:S(2)}) collective-permute-start(bf16[12,48,768]{2,1,0:T(8,128)(2,1)S(1)} %bitcast.8), channel_id=1, source_target_pairs={{0,48},{16,0},{32,16},{48,32},{1,49},{17,1},{33,17},{49,33},{2,50}... | collective-permute-start | bytes 2654216 | tf_op jit(solution)/shard_map/ppermute | solution.py:18
  43.7 1.9 %collective-permute-start.1 = (bf16[12,48,768]{2,1,0:T(8,128)(2,1)S(1)}, bf16[12,48,768]{2,1,0:T(8,128)(2,1)S(1)}, u32[]{:S(2)}, u32[]{:S(2)}) collective-permute-start(bf16[12,48,768]{2,1,0:T(8,128)(2,1)S(1)} %bitcast.9), channel_id=1, source_target_pairs={{0,16},{16,32},{32,48},{48,0},{1,17},{17,33},{33,49},{49,1},{2,18}... | collective-permute-start | bytes 2654216 | tf_op jit(solution)/shard_map/ppermute | solution.py:18
  45.6 10.9 %collective-permute-done.right = bf16[12,48,768]{2,1,0:T(8,128)(2,1)S(1)} collective-permute-done((bf16[12,48,768]{2,1,0:T(8,128)(2,1)S(1)}, bf16[12,48,768]{2,1,0:T(8,128)(2,1)S(1)}, u32[]{:S(2)}, u32[]{:S(2)}) %collective-permute-start) | collective-permute-done | bytes 884768 | tf_op jit(solution)/shard_map/ppermute | solution.py:18
  56.5 5.0 %collective-permute-done.1.left = bf16[12,48,768]{2,1,0:T(8,128)(2,1)S(1)} collective-permute-done((bf16[12,48,768]{2,1,0:T(8,128)(2,1)S(1)}, bf16[12,48,768]{2,1,0:T(8,128)(2,1)S(1)}, u32[]{:S(2)}, u32[]{:S(2)}) %collective-permute-start.1) | collective-permute-done | bytes 884768 | tf_op jit(solution)/shard_map/ppermute | solution.py:18
  62.5 1.9 %collective-permute-start.2 = (bf16[6,48,768]{2,1,0:T(8,128)(2,1)}, bf16[6,48,768]{2,1,0:T(8,128)(2,1)S(1)}, u32[]{:S(2)}, u32[]{:S(2)}) collective-permute-start(bf16[6,48,768]{2,1,0:T(8,128)(2,1)} %get-tuple-element.26), channel_id=1, source_target_pairs={{0,16},{16,32},{32,48},{48,0},{1,17},{17,33},{33,49},{49,1},{2,18}... | collective-permute-start | bytes 1327112 | tf_op jit(solution)/shard_map/ppermute | solution.py:18
  64.4 4.6 %collective-permute-start.3 = (bf16[6,48,768]{2,1,0:T(8,128)(2,1)}, bf16[6,48,768]{2,1,0:T(8,128)(2,1)}, u32[]{:S(2)}, u32[]{:S(2)}) collective-permute-start(bf16[6,48,768]{2,1,0:T(8,128)(2,1)} %get-tuple-element.27), channel_id=1, source_target_pairs={{0,48},{16,0},{32,16},{48,32},{1,49},{17,1},{33,17},{49,33},{2,50}... | collective-permute-start | bytes 1327112 | tf_op jit(solution)/shard_map/ppermute | solution.py:18
  69.0 1.9 %collective-permute-start.4 = (bf16[12,48,384]{2,1,0:T(8,128)(2,1)S(1)}, bf16[12,48,384]{2,1,0:T(8,128)(2,1)S(1)}, u32[]{:S(2)}, u32[]{:S(2)}) collective-permute-start(bf16[12,48,384]{2,1,0:T(8,128)(2,1)S(1)} %all-to-all-done.own), channel_id=1, source_target_pairs={{0,48},{16,0},{32,16},{48,32},{1,49},{17,1},{33,17},{49,33},{2,50}... | collective-permute-start | bytes 1327112 | tf_op jit(solution)/shard_map/ppermute | solution.py:18
  71.0 3.4 %collective-permute-start.5 = (bf16[12,48,384]{2,1,0:T(8,128)(2,1)S(1)}, bf16[12,48,384]{2,1,0:T(8,128)(2,1)S(1)}, u32[]{:S(2)}, u32[]{:S(2)}) collective-permute-start(bf16[12,48,384]{2,1,0:T(8,128)(2,1)S(1)} %all-to-all-done.own), channel_id=1, source_target_pairs={{0,16},{16,32},{32,48},{48,0},{1,17},{17,33},{33,49},{49,1},{2,18}... | collective-permute-start | bytes 1327112 | tf_op jit(solution)/shard_map/ppermute | solution.py:18
  74.3 1.9 %collective-permute-start.6 = (bf16[12,48,384]{2,1,0:T(8,128)(2,1)S(1)}, bf16[12,48,384]{2,1,0:T(8,128)(2,1)S(1)}, u32[]{:S(2)}, u32[]{:S(2)}) collective-permute-start(bf16[12,48,384]{2,1,0:T(8,128)(2,1)S(1)} %all-to-all-done.own), channel_id=1, source_target_pairs={{0,32},{16,48},{32,0},{48,16},{1,33},{17,49},{33,1},{49,17},{2,34}... | collective-permute-start | bytes 1327112 | tf_op jit(solution)/shard_map/ppermute | solution.py:18
  76.3 1.6 copy-done
  77.9 1.3 shard_map.65
  79.1 2.9 %shard_map.67.hidden = bf16[448,384]{1,0:T(8,128)(2,1)S(1)} custom-call(s32[1]{0:T(128)} %bitcast.x_ref, bf16[448,2304]{1,0:T(8,128)(2,1)S(1)} %get-tuple-element.25.normed, bf16[12,48,768]{2,1,0:T(8,128)(2,1)S(1)} %bitcast.10, bf16[12,48,768]{2,1,0:T(8,128)(2,1)S(1)} %collective-permute-done.right, bf16[12,48,768]{2,1,0:T(8,128)(2,1)S(1)} %collective-permute-done.1.left, ...), custom_call_target="tpu_custom_call" | custom-call | tf_op jit(solution)/shard_map/pallas_call | solution.py:193
  82.1 5.7 %collective-permute-done.5.left = bf16[12,48,384]{2,1,0:T(8,128)(2,1)S(1)} collective-permute-done((bf16[12,48,384]{2,1,0:T(8,128)(2,1)S(1)}, bf16[12,48,384]{2,1,0:T(8,128)(2,1)S(1)}, u32[]{:S(2)}, u32[]{:S(2)}) %collective-permute-start.5) | collective-permute-done | bytes 442400 | tf_op jit(solution)/shard_map/ppermute | solution.py:18
  87.7 6.5 %collective-permute-done.6.far = bf16[12,48,384]{2,1,0:T(8,128)(2,1)S(1)} collective-permute-done((bf16[12,48,384]{2,1,0:T(8,128)(2,1)S(1)}, bf16[12,48,384]{2,1,0:T(8,128)(2,1)S(1)}, u32[]{:S(2)}, u32[]{:S(2)}) %collective-permute-start.6) | collective-permute-done | bytes 442400 | tf_op jit(solution)/shard_map/ppermute | solution.py:18
  94.3 1.0 shard_map.68
  95.3 8.1 %collective-permute-start.7 = (bf16[224,2304]{1,0:T(8,128)(2,1)S(1)}, bf16[224,2304]{1,0:T(8,128)(2,1)S(1)}, u32[]{:S(2)}, u32[]{:S(2)}) collective-permute-start(bf16[224,2304]{1,0:T(8,128)(2,1)S(1)} %get-tuple-element.29), channel_id=1, source_target_pairs={{0,1},{1,0},{2,3},{3,2},{4,5},{5,4},{6,7},{7,6},{8,9},{9,8},{10,11... | collective-permute-start | bytes 3096584 | tf_op jit(solution)/shard_map/ppermute | solution.py:18
  104.2 1.4 collective-permute-done.7.theirs
  106.1 34.2 %all_to_all.10.pieces = bf16[8,504,128]{2,1,0:T(8,128)(2,1)S(1)} all-to-all(bf16[8,504,128]{2,1,0:T(8,128)(2,1)S(1)} %shard_map.70), channel_id=1, replica_groups=mesh['z'=12,'x'=4,'y'=8,'c'=2] {'y'}, dimensions={0} | all-to-all | bytes 2064384 | tf_op jit(solution)/shard_map/all_to_all | solution.py:218
  140.6 21.9 %all-gather.1 = bf16[4032,128]{1,0:T(8,128)(2,1)S(1)} all-gather(bf16[504,128]{1,0:T(8,128)(2,1)S(1)} %shard_map.71), channel_id=3, replica_groups=mesh['z'=12,'x'=4,'y'=8,'c'=2] {'y'}, dimensions={0}, use_global_device_ids=true | all-gather | bytes 1161216 | tf_op jit(solution)/shard_map/all_gather | solution.py:225
  162.5 8.2 %collective-permute-start.8 = (bf16[8,504,128]{2,1,0:T(8,128)(2,1)S(1)}, bf16[8,504,128]{2,1,0:T(8,128)(2,1)S(1)}, u32[]{:S(2)}, u32[]{:S(2)}) collective-permute-start(bf16[8,504,128]{2,1,0:T(8,128)(2,1)S(1)} %bitcast.6), channel_id=1, source_target_pairs={{0,1},{1,0},{2,3},{3,2},{4,5},{5,4},{6,7},{7,6},{8,9},{9,8},{10,11... | collective-permute-start | bytes 3096584 | tf_op jit(solution)/shard_map/ppermute | solution.py:18
  170.7 2.2 %collective-permute-done.8.theirs = bf16[8,504,128]{2,1,0:T(8,128)(2,1)S(1)} collective-permute-done((bf16[8,504,128]{2,1,0:T(8,128)(2,1)S(1)}, bf16[8,504,128]{2,1,0:T(8,128)(2,1)S(1)}, u32[]{:S(2)}, u32[]{:S(2)}) %collective-permute-start.8) | collective-permute-done | bytes 1032224 | tf_op jit(solution)/shard_map/ppermute | solution.py:18
  172.9 2.0 %shard_map.72 = bf16[448,2304]{1,0:T(8,128)(2,1)} custom-call(s32[1]{0:T(128)} %bitcast.2.c_ref, bf16[8,504,128]{2,1,0:T(8,128)(2,1)S(1)} %bitcast.7, bf16[8,504,128]{2,1,0:T(8,128)(2,1)S(1)} %collective-permute-done.8.theirs), custom_call_target="tpu_custom_call" | custom-call | tf_op jit(solution)/shard_map/pallas_call | solution.py:226
  (17 shorter events, 4.9 us)
Async XLA Ops:
  0.8 75.5 %copy-start.2 = (f32[2304]{0:T(1024)S(1)}, f32[2304]{0:T(1024)}, u32[]{:S(2)}) copy-start(f32[2304]{0:T(1024)} %gain.2) | copy-start | bytes 27652
  34.1 0.8 copy-start.1
  35.7 33.3 %all-to-all-start = ((bf16[12,48,384]{2,1,0:T(8,128)(2,1)}), bf16[12,48,384]{2,1,0:T(8,128)(2,1)S(1)}, u32[]{:S(2)}, u32[]{:S(2)}) async-start(bf16[12,48,384]{2,1,0:T(8,128)(2,1)} %shard_map.64), calls=%async_computation | async-start | bytes 884736 | tf_op jit(solution)/shard_map/all_to_all | solution.py:183
  39.3 17.2 %collective-permute-start = (bf16[12,48,768]{2,1,0:T(8,128)(2,1)S(1)}, bf16[12,48,768]{2,1,0:T(8,128)(2,1)S(1)}, u32[]{:S(2)}, u32[]{:S(2)}) collective-permute-start(bf16[12,48,768]{2,1,0:T(8,128)(2,1)S(1)} %bitcast.8), channel_id=1, source_target_pairs={{0,48},{16,0},{32,16},{48,32},{1,49},{17,1},{33,17},{49,33},{2,50}... | collective-permute-start | bytes 2654216 | tf_op jit(solution)/shard_map/ppermute | solution.py:18
  43.7 17.9 %collective-permute-start.1 = (bf16[12,48,768]{2,1,0:T(8,128)(2,1)S(1)}, bf16[12,48,768]{2,1,0:T(8,128)(2,1)S(1)}, u32[]{:S(2)}, u32[]{:S(2)}) collective-permute-start(bf16[12,48,768]{2,1,0:T(8,128)(2,1)S(1)} %bitcast.9), channel_id=1, source_target_pairs={{0,16},{16,32},{32,48},{48,0},{1,17},{17,33},{33,49},{49,1},{2,18}... | collective-permute-start | bytes 2654216 | tf_op jit(solution)/shard_map/ppermute | solution.py:18
  62.5 16.6 %collective-permute-start.2 = (bf16[6,48,768]{2,1,0:T(8,128)(2,1)}, bf16[6,48,768]{2,1,0:T(8,128)(2,1)S(1)}, u32[]{:S(2)}, u32[]{:S(2)}) collective-permute-start(bf16[6,48,768]{2,1,0:T(8,128)(2,1)} %get-tuple-element.26), channel_id=1, source_target_pairs={{0,16},{16,32},{32,48},{48,0},{1,17},{17,33},{33,49},{49,1},{2,18}... | collective-permute-start | bytes 1327112 | tf_op jit(solution)/shard_map/ppermute | solution.py:18
  64.4 14.7 %collective-permute-start.3 = (bf16[6,48,768]{2,1,0:T(8,128)(2,1)}, bf16[6,48,768]{2,1,0:T(8,128)(2,1)}, u32[]{:S(2)}, u32[]{:S(2)}) collective-permute-start(bf16[6,48,768]{2,1,0:T(8,128)(2,1)} %get-tuple-element.27), channel_id=1, source_target_pairs={{0,48},{16,0},{32,16},{48,32},{1,49},{17,1},{33,17},{49,33},{2,50}... | collective-permute-start | bytes 1327112 | tf_op jit(solution)/shard_map/ppermute | solution.py:18
  69.0 13.0 %collective-permute-start.4 = (bf16[12,48,384]{2,1,0:T(8,128)(2,1)S(1)}, bf16[12,48,384]{2,1,0:T(8,128)(2,1)S(1)}, u32[]{:S(2)}, u32[]{:S(2)}) collective-permute-start(bf16[12,48,384]{2,1,0:T(8,128)(2,1)S(1)} %all-to-all-done.own), channel_id=1, source_target_pairs={{0,48},{16,0},{32,16},{48,32},{1,49},{17,1},{33,17},{49,33},{2,50}... | collective-permute-start | bytes 1327112 | tf_op jit(solution)/shard_map/ppermute | solution.py:18
  71.0 16.8 %collective-permute-start.5 = (bf16[12,48,384]{2,1,0:T(8,128)(2,1)S(1)}, bf16[12,48,384]{2,1,0:T(8,128)(2,1)S(1)}, u32[]{:S(2)}, u32[]{:S(2)}) collective-permute-start(bf16[12,48,384]{2,1,0:T(8,128)(2,1)S(1)} %all-to-all-done.own), channel_id=1, source_target_pairs={{0,16},{16,32},{32,48},{48,0},{1,17},{17,33},{33,49},{49,1},{2,18}... | collective-permute-start | bytes 1327112 | tf_op jit(solution)/shard_map/ppermute | solution.py:18
  74.3 19.9 %collective-permute-start.6 = (bf16[12,48,384]{2,1,0:T(8,128)(2,1)S(1)}, bf16[12,48,384]{2,1,0:T(8,128)(2,1)S(1)}, u32[]{:S(2)}, u32[]{:S(2)}) collective-permute-start(bf16[12,48,384]{2,1,0:T(8,128)(2,1)S(1)} %all-to-all-done.own), channel_id=1, source_target_pairs={{0,32},{16,48},{32,0},{48,16},{1,33},{17,49},{33,1},{49,17},{2,34}... | collective-permute-start | bytes 1327112 | tf_op jit(solution)/shard_map/ppermute | solution.py:18
  76.3 1.6 copy-start
  95.3 10.3 %collective-permute-start.7 = (bf16[224,2304]{1,0:T(8,128)(2,1)S(1)}, bf16[224,2304]{1,0:T(8,128)(2,1)S(1)}, u32[]{:S(2)}, u32[]{:S(2)}) collective-permute-start(bf16[224,2304]{1,0:T(8,128)(2,1)S(1)} %get-tuple-element.29), channel_id=1, source_target_pairs={{0,1},{1,0},{2,3},{3,2},{4,5},{5,4},{6,7},{7,6},{8,9},{9,8},{10,11... | collective-permute-start | bytes 3096584 | tf_op jit(solution)/shard_map/ppermute | solution.py:18
  104.1 36.1 %copy-start.3 = (f32[2304]{0:T(1024)S(1)}, f32[2304]{0:T(1024)}, u32[]{:S(2)}) copy-start(f32[2304]{0:T(1024)} %gain.3) | copy-start | bytes 27652
  162.5 10.5 %collective-permute-start.8 = (bf16[8,504,128]{2,1,0:T(8,128)(2,1)S(1)}, bf16[8,504,128]{2,1,0:T(8,128)(2,1)S(1)}, u32[]{:S(2)}, u32[]{:S(2)}) collective-permute-start(bf16[8,504,128]{2,1,0:T(8,128)(2,1)S(1)} %bitcast.6), channel_id=1, source_target_pairs={{0,1},{1,0},{2,3},{3,2},{4,5},{5,4},{6,7},{7,6},{8,9},{9,8},{10,11... | collective-permute-start | bytes 3096584 | tf_op jit(solution)/shard_map/ppermute | solution.py:18

commit v5 on v4

--- a/solution.py
+++ b/solution.py
@@ -16,6 +16,10 @@
 def shift(value, axis, by):
     n = lax.axis_size(axis)
     return lax.ppermute(value, axis, [(i, (i + by) % n) for i in range(n)])
+
+
+def alternating(n):
+    return [[2 * y + (h + y) % 2 for y in range(n)] for h in range(2)]
 
 
 def after(value, *others):
@@ -50,7 +54,7 @@
     return shift(low, "x", 1), shift(high, "x", -1)
 
 
-def norm_body(c_ref, y_ref, tokens, gain, out, own, window):
+def norm_body(half_ref, y_ref, tokens, gain, out, own, window):
     step = 16
 
     def lines(i, carry):
@@ -62,7 +66,7 @@
 
     lax.fori_loop(0, tokens.shape[0] // step, lines, 0, unroll=4)
     count, rows, reach = tokens.shape[0], own.shape[0], window.shape[0]
-    first = c_ref[0] * (count // 2) + y_ref[0] * rows
+    first = half_ref[0] * (count // 2) + y_ref[0] * rows
     base = jnp.minimum(first - lax.rem(first, step), count - reach)
     window[...] = tokens[pl.ds(pl.multiple_of(base, step), reach), :].astype(F32)
     for skip in range(0, reach - rows + 1, 4):
@@ -96,13 +100,13 @@
         copies[z] = value[...]
 
 
-def partial_body(x_ref, c_ref, hidden, own, right, left, far, send, whole):
+def partial_body(x_ref, half_ref, hidden, own, right, left, far, send, whole):
     interleave(x_ref[0], [((0, block),) for block in (own, right, far, left)], whole)
-    send[...] = half_product(hidden, 1 - c_ref[0], whole)
-
-
-def keep_body(c_ref, hidden, whole, keep):
-    keep[...] = half_product(hidden, c_ref[0], whole)
+    send[...] = half_product(hidden, 1 - half_ref[0], whole)
+
+
+def keep_body(half_ref, hidden, whole, keep):
+    keep[...] = half_product(hidden, half_ref[0], whole)
 
 
 def half_product(hidden, which, whole):
@@ -150,23 +154,44 @@
     out[...] = full[...].astype(BF16)
 
 
-def join_body(c_ref, mine, theirs, out, folded, lines):
-    count, _, lanes = mine.shape
-    half, width = lines.shape[1:]
+def join_body(which_ref, pieces, *refs):
+    out, folded, lines = refs[-3:]
+    count, _, lanes = pieces.shape
+    half, width = lines.shape
     rows = half // count
-    for at, (source, which) in enumerate(((mine, c_ref[0]), (theirs, 1 - c_ref[0]))):
-        for j in range(count):
-            folded[at, j] = source[j].astype(F32)
-            for t in range(width // lanes):
-                lines[at, j * rows : (j + 1) * rows, t * lanes : (t + 1) * lanes] = (
-                    folded[at, j, t * rows : (t + 1) * rows, :]
-                )
-        out[pl.ds(pl.multiple_of(which * half, 32), half), :] = lines[at].astype(BF16)
+    for j in range(count):
+        folded[j] = pieces[j].astype(F32)
+        for t in range(width // lanes):
+            lines[j * rows : (j + 1) * rows, t * lanes : (t + 1) * lanes] = folded[
+                j, t * rows : (t + 1) * rows, :
+            ]
+    out[...] = lines[...].astype(BF16)
+
+
+def join(which, pieces, half, width, *before):
+    grid = pltpu.PrefetchScalarGridSpec(
+        num_scalar_prefetch=1,
+        grid=(1,),
+        in_specs=[pl.BlockSpec(memory_space=VMEM)]
+        + [pl.BlockSpec(memory_space=pltpu.HBM)] * len(before),
+        out_specs=pl.BlockSpec((half, width), lambda i, which: (which[0], 0)),
+        scratch_shapes=[VMEM(pieces.shape, F32), VMEM((half, width), F32)],
+    )
+    return pl.pallas_call(
+        join_body,
+        out_shape=jax.ShapeDtypeStruct((2 * half, width), BF16),
+        grid_spec=grid,
+        input_output_aliases={2: 0} if before else {},
+        compiler_params=pltpu.CompilerParams(vmem_limit_bytes=12 << 20),
+    )(which, pieces, *before)
 
 
 def per_device(tokens, norm_gain, gate_weight, up_weight, down_weight, branch_gain):
-    places = [lax.axis_index(a).astype(jnp.int32)[None] for a in ("x", "y", "c")]
-    gate_weight, x1, y1, c1 = lax.optimization_barrier((gate_weight, *places))
+    x1, y1, c1 = (lax.axis_index(a).astype(jnp.int32)[None] for a in ("x", "y", "c"))
+    own_half = lax.rem(c1 + y1, 2)
+    gate_weight, x1, y1, own_half, other_half = lax.optimization_barrier(
+        (gate_weight, x1, y1, own_half, 1 - own_half)
+    )
     n_x, n_y, n_z = (lax.axis_size(a) for a in ("x", "y", "z"))
     count, width = tokens.shape
     half, rows = count // 2, count // 2 // n_y
@@ -189,7 +214,7 @@
         [jax.ShapeDtypeStruct((count, width), BF16), jax.ShapeDtypeStruct((rows, width), F32)],
         [VMEM((48, width), F32)],
         2, 2, 8,
-    )(c1, y1, after(tokens, down_z), norm_gain)
+    )(own_half, y1, after(tokens, down_z), norm_gain)
     hidden = local_call(
         hidden_body,
         jax.ShapeDtypeStruct((count, units), BF16),
@@ -203,11 +228,11 @@
             jax.ShapeDtypeStruct((n_z, n_x, piece, units), BF16),
         ],
         (), 2, 5,
-    )(x1, c1, hidden, down_z, *down)
+    )(x1, own_half, hidden, down_z, *down)
     theirs = shift(send, "c", 1)
     keep = local_call(
         keep_body, jax.ShapeDtypeStruct((half, width), BF16), (), 1, 2
-    )(c1, hidden, whole)
+    )(own_half, hidden, whole)
     folded = (n_y, *flat)
     pair = local_call(
         pair_sum_body,
@@ -215,20 +240,18 @@
         [VMEM((half, width), F32), VMEM(folded, F32)],
         0, 2,
     )(keep, theirs)
-    pieces = lax.all_to_all(pair, "y", 0, 0, tiled=True)
+    pieces = lax.all_to_all(
+        pair, ("y", "c"), 0, 0, axis_index_groups=alternating(n_y), tiled=True
+    )
     done = local_call(
         finish_body,
         jax.ShapeDtypeStruct(flat, BF16),
         [VMEM(flat, F32)] * 2,
         0, 3,
     )(pieces, own_tokens, branch_gain)
-    mine = lax.all_gather(done, "y")
-    return local_call(
-        join_body,
-        jax.ShapeDtypeStruct((count, width), BF16),
-        [VMEM((2, n_y, *flat), F32), VMEM((2, half, width), F32)],
-        1, 2,
-    )(c1, mine, shift(mine, "c", 1))
+    mine = lax.all_gather(done, ("y", "c"), axis_index_groups=alternating(n_y))
+    theirs = shift(mine, "c", 1)
+    return join(other_half, theirs, half, width, join(own_half, mine, half, width))
 
 
 def solution(mesh):

time: 176 us -> 172 us (0.977)
  starting transfers between devices: 39.8 us -> 34.6 us
  blocking collectives: 89.4 us -> 91.3 us
    ppermute x9, starting transfers between devices: 36.3 us -> 31 us  [shift(): return lax.ppermute(value, axis, [(i, (i + by) % n) for i in range(n)])]
  transfers between devices with their start and end apart: 10 -> 10, of which waited for: 6 -> 6; matrix products, arithmetic and copies ran while one was open for 0% -> 0% of each run, Pallas kernels for 3% -> 4%
where the time goes in v5:
time: 172 us; the launch traced here: 171 us
  blocking collectives  91.3 us (53%)
  starting transfers between devices  34.6 us (20%)
  waiting for transfers between devices  30.5 us (18%)
  Pallas kernels  11.2 us (7%)
  local copies, waits for them, and re-layouts  2.35 us (1%)
    all_to_all x1, blocking collectives, per_device(): lax.all_to_all(pair, ('y', 'c'), 0, 0, axis_index_groups=alternating(n_y)...  34.4 us
    all_gather x1, blocking collectives, per_device(): both_z = lax.all_gather(own_both, 'z')  33.3 us
    ppermute x9, starting transfers between devices, shift(): return lax.ppermute(value, axis, [(i, (i + by) % n) for i in range(n)])  31 us
    ppermute x9, waiting for transfers between devices, shift(): return lax.ppermute(value, axis, [(i, (i + by) % n) for i in range(n)])  30.5 us
    all_gather x1, blocking collectives, per_device(): mine = lax.all_gather(done, ('y', 'c'), axis_index_groups=alternating(n_y))  23.6 us
    all_to_all x1, starting transfers between devices, per_device(): down_z = lax.all_to_all(copies, 'z', 0, 0, tiled=True)  3.58 us
  transfers between devices with their start and end apart: 10, of which 6 were waited for; matrix products, arithmetic and copies ran while one was open for 0% of the time, Pallas kernels for 4%

profile of v5, /device:TPU:1, one launch (start us, length us, event | category | flops | bytes accessed | tf_op | source)
XLA Modules:
  0.0 170.8 jit_solution(7710709042916010703)
XLA Ops:
  0.8 33.3 %all-gather = bf16[576,768]{1,0:T(8,128)(2,1)S(1)} all-gather(bf16[48,768]{1,0:T(8,128)(2,1)S(1)} %pad_maximum_fusion), channel_id=2, replica_groups=mesh['z'=12,'x'=4,'y'=8,'c'=2] {'z'}, dimensions={0}, use_global_device_ids=true | all-gather | bytes 958464 | tf_op jit(solution)/shard_map/all_gather | solution.py:203
  35.7 3.6 %all-to-all-start = ((bf16[12,48,384]{2,1,0:T(8,128)(2,1)}), bf16[12,48,384]{2,1,0:T(8,128)(2,1)S(1)}, u32[]{:S(2)}, u32[]{:S(2)}) async-start(bf16[12,48,384]{2,1,0:T(8,128)(2,1)} %shard_map.64), calls=%async_computation | async-start | bytes 884736 | tf_op jit(solution)/shard_map/all_to_all | solution.py:208
  39.3 4.4 %collective-permute-start = (bf16[12,48,768]{2,1,0:T(8,128)(2,1)S(1)}, bf16[12,48,768]{2,1,0:T(8,128)(2,1)S(1)}, u32[]{:S(2)}, u32[]{:S(2)}) collective-permute-start(bf16[12,48,768]{2,1,0:T(8,128)(2,1)S(1)} %bitcast.8), channel_id=1, source_target_pairs={{0,48},{16,0},{32,16},{48,32},{1,49},{17,1},{33,17},{49,33},{2,50}... | collective-permute-start | bytes 2654216 | tf_op jit(solution)/shard_map/ppermute | solution.py:18
  43.7 1.9 %collective-permute-start.1 = (bf16[12,48,768]{2,1,0:T(8,128)(2,1)S(1)}, bf16[12,48,768]{2,1,0:T(8,128)(2,1)S(1)}, u32[]{:S(2)}, u32[]{:S(2)}) collective-permute-start(bf16[12,48,768]{2,1,0:T(8,128)(2,1)S(1)} %bitcast.9), channel_id=1, source_target_pairs={{0,16},{16,32},{32,48},{48,0},{1,17},{17,33},{33,49},{49,1},{2,18}... | collective-permute-start | bytes 2654216 | tf_op jit(solution)/shard_map/ppermute | solution.py:18
  45.6 10.9 %collective-permute-done.right = bf16[12,48,768]{2,1,0:T(8,128)(2,1)S(1)} collective-permute-done((bf16[12,48,768]{2,1,0:T(8,128)(2,1)S(1)}, bf16[12,48,768]{2,1,0:T(8,128)(2,1)S(1)}, u32[]{:S(2)}, u32[]{:S(2)}) %collective-permute-start) | collective-permute-done | bytes 884768 | tf_op jit(solution)/shard_map/ppermute | solution.py:18
  56.5 5.0 %collective-permute-done.1.left = bf16[12,48,768]{2,1,0:T(8,128)(2,1)S(1)} collective-permute-done((bf16[12,48,768]{2,1,0:T(8,128)(2,1)S(1)}, bf16[12,48,768]{2,1,0:T(8,128)(2,1)S(1)}, u32[]{:S(2)}, u32[]{:S(2)}) %collective-permute-start.1) | collective-permute-done | bytes 884768 | tf_op jit(solution)/shard_map/ppermute | solution.py:18
  62.5 1.9 %collective-permute-start.2 = (bf16[6,48,768]{2,1,0:T(8,128)(2,1)}, bf16[6,48,768]{2,1,0:T(8,128)(2,1)S(1)}, u32[]{:S(2)}, u32[]{:S(2)}) collective-permute-start(bf16[6,48,768]{2,1,0:T(8,128)(2,1)} %get-tuple-element.28), channel_id=1, source_target_pairs={{0,16},{16,32},{32,48},{48,0},{1,17},{17,33},{33,49},{49,1},{2,18}... | collective-permute-start | bytes 1327112 | tf_op jit(solution)/shard_map/ppermute | solution.py:18
  64.4 4.6 %collective-permute-start.3 = (bf16[6,48,768]{2,1,0:T(8,128)(2,1)}, bf16[6,48,768]{2,1,0:T(8,128)(2,1)}, u32[]{:S(2)}, u32[]{:S(2)}) collective-permute-start(bf16[6,48,768]{2,1,0:T(8,128)(2,1)} %get-tuple-element.29), channel_id=1, source_target_pairs={{0,48},{16,0},{32,16},{48,32},{1,49},{17,1},{33,17},{49,33},{2,50}... | collective-permute-start | bytes 1327112 | tf_op jit(solution)/shard_map/ppermute | solution.py:18
  69.0 1.9 %collective-permute-start.4 = (bf16[12,48,384]{2,1,0:T(8,128)(2,1)S(1)}, bf16[12,48,384]{2,1,0:T(8,128)(2,1)S(1)}, u32[]{:S(2)}, u32[]{:S(2)}) collective-permute-start(bf16[12,48,384]{2,1,0:T(8,128)(2,1)S(1)} %all-to-all-done.own), channel_id=1, source_target_pairs={{0,48},{16,0},{32,16},{48,32},{1,49},{17,1},{33,17},{49,33},{2,50}... | collective-permute-start | bytes 1327112 | tf_op jit(solution)/shard_map/ppermute | solution.py:18
  71.0 3.4 %collective-permute-start.5 = (bf16[12,48,384]{2,1,0:T(8,128)(2,1)S(1)}, bf16[12,48,384]{2,1,0:T(8,128)(2,1)S(1)}, u32[]{:S(2)}, u32[]{:S(2)}) collective-permute-start(bf16[12,48,384]{2,1,0:T(8,128)(2,1)S(1)} %all-to-all-done.own), channel_id=1, source_target_pairs={{0,16},{16,32},{32,48},{48,0},{1,17},{17,33},{33,49},{49,1},{2,18}... | collective-permute-start | bytes 1327112 | tf_op jit(solution)/shard_map/ppermute | solution.py:18
  74.3 1.9 %collective-permute-start.6 = (bf16[12,48,384]{2,1,0:T(8,128)(2,1)S(1)}, bf16[12,48,384]{2,1,0:T(8,128)(2,1)S(1)}, u32[]{:S(2)}, u32[]{:S(2)}) collective-permute-start(bf16[12,48,384]{2,1,0:T(8,128)(2,1)S(1)} %all-to-all-done.own), channel_id=1, source_target_pairs={{0,32},{16,48},{32,0},{48,16},{1,33},{17,49},{33,1},{49,17},{2,34}... | collective-permute-start | bytes 1327112 | tf_op jit(solution)/shard_map/ppermute | solution.py:18
  76.3 1.6 copy-done
  77.9 1.3 shard_map.65
  79.1 2.9 %shard_map.67.hidden = bf16[448,384]{1,0:T(8,128)(2,1)S(1)} custom-call(s32[1]{0:T(128)} %bitcast.x_ref, bf16[448,2304]{1,0:T(8,128)(2,1)S(1)} %get-tuple-element.27.normed, bf16[12,48,768]{2,1,0:T(8,128)(2,1)S(1)} %bitcast.10, bf16[12,48,768]{2,1,0:T(8,128)(2,1)S(1)} %collective-permute-done.right, bf16[12,48,768]{2,1,0:T(8,128)(2,1)S(1)} %collective-permute-done.1.left, ...), custom_call_target="tpu_custom_call" | custom-call | tf_op jit(solution)/shard_map/pallas_call | solution.py:218
  82.1 5.7 %collective-permute-done.5.left = bf16[12,48,384]{2,1,0:T(8,128)(2,1)S(1)} collective-permute-done((bf16[12,48,384]{2,1,0:T(8,128)(2,1)S(1)}, bf16[12,48,384]{2,1,0:T(8,128)(2,1)S(1)}, u32[]{:S(2)}, u32[]{:S(2)}) %collective-permute-start.5) | collective-permute-done | bytes 442400 | tf_op jit(solution)/shard_map/ppermute | solution.py:18
  87.7 6.5 %collective-permute-done.6.far = bf16[12,48,384]{2,1,0:T(8,128)(2,1)S(1)} collective-permute-done((bf16[12,48,384]{2,1,0:T(8,128)(2,1)S(1)}, bf16[12,48,384]{2,1,0:T(8,128)(2,1)S(1)}, u32[]{:S(2)}, u32[]{:S(2)}) %collective-permute-start.6) | collective-permute-done | bytes 442400 | tf_op jit(solution)/shard_map/ppermute | solution.py:18
  94.3 1.0 shard_map.68
  95.3 8.1 %collective-permute-start.7 = (bf16[224,2304]{1,0:T(8,128)(2,1)S(1)}, bf16[224,2304]{1,0:T(8,128)(2,1)S(1)}, u32[]{:S(2)}, u32[]{:S(2)}) collective-permute-start(bf16[224,2304]{1,0:T(8,128)(2,1)S(1)} %get-tuple-element.31), channel_id=1, source_target_pairs={{0,1},{1,0},{2,3},{3,2},{4,5},{5,4},{6,7},{7,6},{8,9},{9,8},{10,11... | collective-permute-start | bytes 3096584 | tf_op jit(solution)/shard_map/ppermute | solution.py:18
  104.2 1.4 collective-permute-done.7.theirs
  106.1 34.4 %all_to_all.10.pieces = bf16[8,504,128]{2,1,0:T(8,128)(2,1)S(1)} all-to-all(bf16[8,504,128]{2,1,0:T(8,128)(2,1)S(1)} %shard_map.70), channel_id=1, replica_groups={{0,3,4,7,8,11,12,15},{1,2,5,6,9,10,13,14},{16,19,20,23,24,27,28,31},{17..., dimensions={0} | all-to-all | bytes 2064384 | tf_op jit(solution)/shard_map/all_to_all | solution.py:243
  140.7 23.6 %all-gather.1 = bf16[4032,128]{1,0:T(8,128)(2,1)S(1)} all-gather(bf16[504,128]{1,0:T(8,128)(2,1)S(1)} %shard_map.71), channel_id=3, replica_groups={{0,3,4,7,8,11,12,15},{1,2,5,6,9,10,13,14},{16,19,20,23,24,27,28,31},{17..., dimensions={0}, use_global_device_ids=true | all-gather | bytes 1161216 | tf_op jit(solution)/shard_map/all_gather | solution.py:252
  164.3 2.9 %collective-permute-start.8 = (bf16[8,504,128]{2,1,0:T(8,128)(2,1)S(1)}, bf16[8,504,128]{2,1,0:T(8,128)(2,1)S(1)}, u32[]{:S(2)}, u32[]{:S(2)}) collective-permute-start(bf16[8,504,128]{2,1,0:T(8,128)(2,1)S(1)} %bitcast.6), channel_id=1, source_target_pairs={{0,1},{1,0},{2,3},{3,2},{4,5},{5,4},{6,7},{7,6},{8,9},{9,8},{10,11... | collective-permute-start | bytes 3096584 | tf_op jit(solution)/shard_map/ppermute | solution.py:18
  167.2 1.3 shard_map.72.refs_0_
  169.5 1.3 shard_map.73
  (18 shorter events, 5.8 us)
Async XLA Ops:
  0.8 75.5 %copy-start.2 = (f32[2304]{0:T(1024)S(1)}, f32[2304]{0:T(1024)}, u32[]{:S(2)}) copy-start(f32[2304]{0:T(1024)} %gain.2) | copy-start | bytes 27652
  34.1 0.8 copy-start.1
  35.7 33.3 %all-to-all-start = ((bf16[12,48,384]{2,1,0:T(8,128)(2,1)}), bf16[12,48,384]{2,1,0:T(8,128)(2,1)S(1)}, u32[]{:S(2)}, u32[]{:S(2)}) async-start(bf16[12,48,384]{2,1,0:T(8,128)(2,1)} %shard_map.64), calls=%async_computation | async-start | bytes 884736 | tf_op jit(solution)/shard_map/all_to_all | solution.py:208
  39.3 17.2 %collective-permute-start = (bf16[12,48,768]{2,1,0:T(8,128)(2,1)S(1)}, bf16[12,48,768]{2,1,0:T(8,128)(2,1)S(1)}, u32[]{:S(2)}, u32[]{:S(2)}) collective-permute-start(bf16[12,48,768]{2,1,0:T(8,128)(2,1)S(1)} %bitcast.8), channel_id=1, source_target_pairs={{0,48},{16,0},{32,16},{48,32},{1,49},{17,1},{33,17},{49,33},{2,50}... | collective-permute-start | bytes 2654216 | tf_op jit(solution)/shard_map/ppermute | solution.py:18
  43.7 17.9 %collective-permute-start.1 = (bf16[12,48,768]{2,1,0:T(8,128)(2,1)S(1)}, bf16[12,48,768]{2,1,0:T(8,128)(2,1)S(1)}, u32[]{:S(2)}, u32[]{:S(2)}) collective-permute-start(bf16[12,48,768]{2,1,0:T(8,128)(2,1)S(1)} %bitcast.9), channel_id=1, source_target_pairs={{0,16},{16,32},{32,48},{48,0},{1,17},{17,33},{33,49},{49,1},{2,18}... | collective-permute-start | bytes 2654216 | tf_op jit(solution)/shard_map/ppermute | solution.py:18
  62.5 16.6 %collective-permute-start.2 = (bf16[6,48,768]{2,1,0:T(8,128)(2,1)}, bf16[6,48,768]{2,1,0:T(8,128)(2,1)S(1)}, u32[]{:S(2)}, u32[]{:S(2)}) collective-permute-start(bf16[6,48,768]{2,1,0:T(8,128)(2,1)} %get-tuple-element.28), channel_id=1, source_target_pairs={{0,16},{16,32},{32,48},{48,0},{1,17},{17,33},{33,49},{49,1},{2,18}... | collective-permute-start | bytes 1327112 | tf_op jit(solution)/shard_map/ppermute | solution.py:18
  64.4 14.7 %collective-permute-start.3 = (bf16[6,48,768]{2,1,0:T(8,128)(2,1)}, bf16[6,48,768]{2,1,0:T(8,128)(2,1)}, u32[]{:S(2)}, u32[]{:S(2)}) collective-permute-start(bf16[6,48,768]{2,1,0:T(8,128)(2,1)} %get-tuple-element.29), channel_id=1, source_target_pairs={{0,48},{16,0},{32,16},{48,32},{1,49},{17,1},{33,17},{49,33},{2,50}... | collective-permute-start | bytes 1327112 | tf_op jit(solution)/shard_map/ppermute | solution.py:18
  69.0 13.0 %collective-permute-start.4 = (bf16[12,48,384]{2,1,0:T(8,128)(2,1)S(1)}, bf16[12,48,384]{2,1,0:T(8,128)(2,1)S(1)}, u32[]{:S(2)}, u32[]{:S(2)}) collective-permute-start(bf16[12,48,384]{2,1,0:T(8,128)(2,1)S(1)} %all-to-all-done.own), channel_id=1, source_target_pairs={{0,48},{16,0},{32,16},{48,32},{1,49},{17,1},{33,17},{49,33},{2,50}... | collective-permute-start | bytes 1327112 | tf_op jit(solution)/shard_map/ppermute | solution.py:18
  71.0 16.8 %collective-permute-start.5 = (bf16[12,48,384]{2,1,0:T(8,128)(2,1)S(1)}, bf16[12,48,384]{2,1,0:T(8,128)(2,1)S(1)}, u32[]{:S(2)}, u32[]{:S(2)}) collective-permute-start(bf16[12,48,384]{2,1,0:T(8,128)(2,1)S(1)} %all-to-all-done.own), channel_id=1, source_target_pairs={{0,16},{16,32},{32,48},{48,0},{1,17},{17,33},{33,49},{49,1},{2,18}... | collective-permute-start | bytes 1327112 | tf_op jit(solution)/shard_map/ppermute | solution.py:18
  74.3 19.9 %collective-permute-start.6 = (bf16[12,48,384]{2,1,0:T(8,128)(2,1)S(1)}, bf16[12,48,384]{2,1,0:T(8,128)(2,1)S(1)}, u32[]{:S(2)}, u32[]{:S(2)}) collective-permute-start(bf16[12,48,384]{2,1,0:T(8,128)(2,1)S(1)} %all-to-all-done.own), channel_id=1, source_target_pairs={{0,32},{16,48},{32,0},{48,16},{1,33},{17,49},{33,1},{49,17},{2,34}... | collective-permute-start | bytes 1327112 | tf_op jit(solution)/shard_map/ppermute | solution.py:18
  76.3 1.6 copy-start
  95.3 10.3 %collective-permute-start.7 = (bf16[224,2304]{1,0:T(8,128)(2,1)S(1)}, bf16[224,2304]{1,0:T(8,128)(2,1)S(1)}, u32[]{:S(2)}, u32[]{:S(2)}) collective-permute-start(bf16[224,2304]{1,0:T(8,128)(2,1)S(1)} %get-tuple-element.31), channel_id=1, source_target_pairs={{0,1},{1,0},{2,3},{3,2},{4,5},{5,4},{6,7},{7,6},{8,9},{9,8},{10,11... | collective-permute-start | bytes 3096584 | tf_op jit(solution)/shard_map/ppermute | solution.py:18
  104.1 36.3 %copy-start.3 = (f32[2304]{0:T(1024)S(1)}, f32[2304]{0:T(1024)}, u32[]{:S(2)}) copy-start(f32[2304]{0:T(1024)} %gain.3) | copy-start | bytes 27652
  164.3 5.2 %collective-permute-start.8 = (bf16[8,504,128]{2,1,0:T(8,128)(2,1)S(1)}, bf16[8,504,128]{2,1,0:T(8,128)(2,1)S(1)}, u32[]{:S(2)}, u32[]{:S(2)}) collective-permute-start(bf16[8,504,128]{2,1,0:T(8,128)(2,1)S(1)} %bitcast.6), channel_id=1, source_target_pairs={{0,1},{1,0},{2,3},{3,2},{4,5},{5,4},{6,7},{7,6},{8,9},{9,8},{10,11... | collective-permute-start | bytes 3096584 | tf_op jit(solution)/shard_map/ppermute | solution.py:18

commit v6 on v5

--- a/solution.py
+++ b/solution.py
@@ -121,37 +121,18 @@
     ).astype(BF16)
 
 
-def pair_sum_body(mine, theirs, out, total, folded):
-    total[...] = mine[...].astype(F32) + theirs[...].astype(F32)
-    count, lines, lanes = out.shape
-    parts = total.shape[1] // lanes
-    rows = lines // parts
-    for j in range(count):
-        for t in range(parts):
-            folded[j, t * rows : (t + 1) * rows, :] = total[
-                j * rows : (j + 1) * rows, t * lanes : (t + 1) * lanes
-            ]
-        out[j] = folded[j].astype(BF16)
-
-
-def finish_body(pieces, tokens, gain, out, branch, full):
-    count, _, lanes = pieces.shape
-    total = pieces[0].astype(F32)
-    for j in range(1, count):
-        total = total + pieces[j].astype(F32)
-    branch[...] = total
-    rows, width = tokens.shape
-    parts = [branch[t * rows : (t + 1) * rows, :] for t in range(width // lanes)]
-    squares = parts[0] * parts[0]
-    for value in parts[1:]:
-        squares = squares + value * value
-    scale = lax.rsqrt(jnp.sum(squares, axis=-1, keepdims=True) / width + epsilon)
-    for t, value in enumerate(parts):
-        columns = slice(t * lanes, (t + 1) * lanes)
-        full[t * rows : (t + 1) * rows, :] = (
-            tokens[:, columns] + value * scale * gain[columns][None]
-        )
-    out[...] = full[...].astype(BF16)
+def pair_sum_body(mine, theirs, out):
+    out[...] = (mine[...].astype(F32) + theirs[...].astype(F32)).astype(BF16)
+
+
+def finish_body(summed, tokens, gain, out, folded):
+    branch = summed[...].astype(F32)
+    scale = lax.rsqrt(jnp.mean(branch * branch, axis=-1, keepdims=True) + epsilon)
+    full = tokens[...] + branch * scale * gain[...][None]
+    rows, lanes = summed.shape[0], out.shape[1]
+    for t in range(summed.shape[1] // lanes):
+        folded[t * rows : (t + 1) * rows, :] = full[:, t * lanes : (t + 1) * lanes]
+    out[...] = folded[...].astype(BF16)
 
 
 def join_body(which_ref, pieces, *refs):
@@ -233,22 +214,19 @@
     keep = local_call(
         keep_body, jax.ShapeDtypeStruct((half, width), BF16), (), 1, 2
     )(own_half, hidden, whole)
-    folded = (n_y, *flat)
     pair = local_call(
-        pair_sum_body,
-        jax.ShapeDtypeStruct(folded, BF16),
-        [VMEM((half, width), F32), VMEM(folded, F32)],
-        0, 2,
+        pair_sum_body, jax.ShapeDtypeStruct((half, width), BF16), n_in=2, limit=8
     )(keep, theirs)
-    pieces = lax.all_to_all(
-        pair, ("y", "c"), 0, 0, axis_index_groups=alternating(n_y), tiled=True
+    summed = lax.psum_scatter(
+        pair,
+        ("y", "c"),
+        scatter_dimension=0,
+        axis_index_groups=alternating(n_y),
+        tiled=True,
     )
     done = local_call(
-        finish_body,
-        jax.ShapeDtypeStruct(flat, BF16),
-        [VMEM(flat, F32)] * 2,
-        0, 3,
-    )(pieces, own_tokens, branch_gain)
+        finish_body, jax.ShapeDtypeStruct(flat, BF16), [VMEM(flat, F32)], n_in=3, limit=8
+    )(summed, own_tokens, branch_gain)
     mine = lax.all_gather(done, ("y", "c"), axis_index_groups=alternating(n_y))
     theirs = shift(mine, "c", 1)
     return join(other_half, theirs, half, width, join(own_half, mine, half, width))

time: 172 us -> 170 us (0.988)
  blocking collectives: 91.3 us -> 84.3 us
  local copies, waits for them, and re-layouts: 2.35 us -> 4.11 us
    all_to_all x1 -> x0, blocking collectives: 34.4 us -> none  [per_device(): lax.all_to_all(pair, ('y', 'c'), 0, 0, axis_index_groups=alternating(n_y)...]
    unnamed x0 -> x1, blocking collectives: none -> 23.8 us
    all_gather x1, blocking collectives: 23.6 us -> 27.1 us  [per_device(): mine = lax.all_gather(done, ('y', 'c'), axis_index_groups=alternating(n_y))]
    unnamed x0 -> x1, starting transfers between devices: none -> 2.47 us
    unnamed x8 -> x16, local copies, waits for them, and re-layouts: 2.35 us -> 4.11 us
  transfers between devices with their start and end apart: 10 -> 11, of which waited for: 6 -> 7; matrix products, arithmetic and copies ran while one was open for 0% -> 1% of each run, Pallas kernels for 4% -> 4%
where the time goes in v6:
time: 170 us; the launch traced here: 169 us
  blocking collectives  84.3 us (50%)
  starting transfers between devices  36.1 us (21%)
  waiting for transfers between devices  32 us (19%)
  Pallas kernels  10.9 us (6%)
  local copies, waits for them, and re-layouts  4.11 us (2%)
    all_gather x1, blocking collectives, per_device(): both_z = lax.all_gather(own_both, 'z')  33.3 us
    ppermute x9, waiting for transfers between devices, shift(): return lax.ppermute(value, axis, [(i, (i + by) % n) for i in range(n)])  30.6 us
    ppermute x9, starting transfers between devices, shift(): return lax.ppermute(value, axis, [(i, (i + by) % n) for i in range(n)])  30.1 us
    all_gather x1, blocking collectives, per_device(): mine = lax.all_gather(done, ('y', 'c'), axis_index_groups=alternating(n_y))  27.1 us
    unnamed x1, blocking collectives  23.8 us
    unnamed x16, local copies, waits for them, and re-layouts  4.11 us
    all_to_all x1, starting transfers between devices, per_device(): down_z = lax.all_to_all(copies, 'z', 0, 0, tiled=True)  3.58 us
  transfers between devices with their start and end apart: 11, of which 7 were waited for; matrix products, arithmetic and copies ran while one was open for 1% of the time, Pallas kernels for 4%

profile of v6, /device:TPU:1, one launch (start us, length us, event | category | flops | bytes accessed | tf_op | source)
XLA Modules:
  0.0 169.1 jit_solution(12019026199339976159)
XLA Ops:
  0.8 33.3 %all-gather = bf16[576,768]{1,0:T(8,128)(2,1)S(1)} all-gather(bf16[48,768]{1,0:T(8,128)(2,1)S(1)} %pad_maximum_fusion), channel_id=2, replica_groups=mesh['z'=12,'x'=4,'y'=8,'c'=2] {'z'}, dimensions={0}, use_global_device_ids=true | all-gather | bytes 958464 | tf_op jit(solution)/shard_map/all_gather | solution.py:184
  35.7 3.6 %all-to-all-start = ((bf16[12,48,384]{2,1,0:T(8,128)(2,1)}), bf16[12,48,384]{2,1,0:T(8,128)(2,1)S(1)}, u32[]{:S(2)}, u32[]{:S(2)}) async-start(bf16[12,48,384]{2,1,0:T(8,128)(2,1)} %shard_map.64), calls=%async_computation | async-start | bytes 884736 | tf_op jit(solution)/shard_map/all_to_all | solution.py:189
  39.3 4.4 %collective-permute-start = (bf16[12,48,768]{2,1,0:T(8,128)(2,1)S(1)}, bf16[12,48,768]{2,1,0:T(8,128)(2,1)S(1)}, u32[]{:S(2)}, u32[]{:S(2)}) collective-permute-start(bf16[12,48,768]{2,1,0:T(8,128)(2,1)S(1)} %bitcast.11), channel_id=1, source_target_pairs={{0,48},{16,0},{32,16},{48,32},{1,49},{17,1},{33,17},{49,33},{2,50}... | collective-permute-start | bytes 2654216 | tf_op jit(solution)/shard_map/ppermute | solution.py:18
  43.7 1.9 %collective-permute-start.1 = (bf16[12,48,768]{2,1,0:T(8,128)(2,1)S(1)}, bf16[12,48,768]{2,1,0:T(8,128)(2,1)S(1)}, u32[]{:S(2)}, u32[]{:S(2)}) collective-permute-start(bf16[12,48,768]{2,1,0:T(8,128)(2,1)S(1)} %bitcast.12), channel_id=1, source_target_pairs={{0,16},{16,32},{32,48},{48,0},{1,17},{17,33},{33,49},{49,1},{2,18}... | collective-permute-start | bytes 2654216 | tf_op jit(solution)/shard_map/ppermute | solution.py:18
  45.6 10.9 %collective-permute-done.right = bf16[12,48,768]{2,1,0:T(8,128)(2,1)S(1)} collective-permute-done((bf16[12,48,768]{2,1,0:T(8,128)(2,1)S(1)}, bf16[12,48,768]{2,1,0:T(8,128)(2,1)S(1)}, u32[]{:S(2)}, u32[]{:S(2)}) %collective-permute-start) | collective-permute-done | bytes 884768 | tf_op jit(solution)/shard_map/ppermute | solution.py:18
  56.5 5.0 %collective-permute-done.1.left = bf16[12,48,768]{2,1,0:T(8,128)(2,1)S(1)} collective-permute-done((bf16[12,48,768]{2,1,0:T(8,128)(2,1)S(1)}, bf16[12,48,768]{2,1,0:T(8,128)(2,1)S(1)}, u32[]{:S(2)}, u32[]{:S(2)}) %collective-permute-start.1) | collective-permute-done | bytes 884768 | tf_op jit(solution)/shard_map/ppermute | solution.py:18
  62.5 1.9 %collective-permute-start.2 = (bf16[6,48,768]{2,1,0:T(8,128)(2,1)}, bf16[6,48,768]{2,1,0:T(8,128)(2,1)S(1)}, u32[]{:S(2)}, u32[]{:S(2)}) collective-permute-start(bf16[6,48,768]{2,1,0:T(8,128)(2,1)} %get-tuple-element.28), channel_id=1, source_target_pairs={{0,16},{16,32},{32,48},{48,0},{1,17},{17,33},{33,49},{49,1},{2,18}... | collective-permute-start | bytes 1327112 | tf_op jit(solution)/shard_map/ppermute | solution.py:18
  64.5 4.6 %collective-permute-start.3 = (bf16[6,48,768]{2,1,0:T(8,128)(2,1)}, bf16[6,48,768]{2,1,0:T(8,128)(2,1)}, u32[]{:S(2)}, u32[]{:S(2)}) collective-permute-start(bf16[6,48,768]{2,1,0:T(8,128)(2,1)} %get-tuple-element.29), channel_id=1, source_target_pairs={{0,48},{16,0},{32,16},{48,32},{1,49},{17,1},{33,17},{49,33},{2,50}... | collective-permute-start | bytes 1327112 | tf_op jit(solution)/shard_map/ppermute | solution.py:18
  69.0 1.9 %collective-permute-start.4 = (bf16[12,48,384]{2,1,0:T(8,128)(2,1)S(1)}, bf16[12,48,384]{2,1,0:T(8,128)(2,1)S(1)}, u32[]{:S(2)}, u32[]{:S(2)}) collective-permute-start(bf16[12,48,384]{2,1,0:T(8,128)(2,1)S(1)} %all-to-all-done.own), channel_id=1, source_target_pairs={{0,48},{16,0},{32,16},{48,32},{1,49},{17,1},{33,17},{49,33},{2,50}... | collective-permute-start | bytes 1327112 | tf_op jit(solution)/shard_map/ppermute | solution.py:18
  71.0 3.4 %collective-permute-start.5 = (bf16[12,48,384]{2,1,0:T(8,128)(2,1)S(1)}, bf16[12,48,384]{2,1,0:T(8,128)(2,1)S(1)}, u32[]{:S(2)}, u32[]{:S(2)}) collective-permute-start(bf16[12,48,384]{2,1,0:T(8,128)(2,1)S(1)} %all-to-all-done.own), channel_id=1, source_target_pairs={{0,16},{16,32},{32,48},{48,0},{1,17},{17,33},{33,49},{49,1},{2,18}... | collective-permute-start | bytes 1327112 | tf_op jit(solution)/shard_map/ppermute | solution.py:18
  74.3 1.9 %collective-permute-start.6 = (bf16[12,48,384]{2,1,0:T(8,128)(2,1)S(1)}, bf16[12,48,384]{2,1,0:T(8,128)(2,1)S(1)}, u32[]{:S(2)}, u32[]{:S(2)}) collective-permute-start(bf16[12,48,384]{2,1,0:T(8,128)(2,1)S(1)} %all-to-all-done.own), channel_id=1, source_target_pairs={{0,32},{16,48},{32,0},{48,16},{1,33},{17,49},{33,1},{49,17},{2,34}... | collective-permute-start | bytes 1327112 | tf_op jit(solution)/shard_map/ppermute | solution.py:18
  76.3 1.6 copy-done
  79.2 3.0 %shard_map.67.hidden = bf16[448,384]{1,0:T(8,128)(2,1)S(1)} custom-call(s32[1]{0:T(128)} %bitcast.x_ref, bf16[448,2304]{1,0:T(8,128)(2,1)S(1)} %get-tuple-element.27.normed, bf16[12,48,768]{2,1,0:T(8,128)(2,1)S(1)} %bitcast.13, bf16[12,48,768]{2,1,0:T(8,128)(2,1)S(1)} %collective-permute-done.right, bf16[12,48,768]{2,1,0:T(8,128)(2,1)S(1)} %collective-permute-done.1.left, ...), custom_call_target="tpu_custom_call" | custom-call | tf_op jit(solution)/shard_map/pallas_call | solution.py:199
  82.2 5.5 %collective-permute-done.5.left = bf16[12,48,384]{2,1,0:T(8,128)(2,1)S(1)} collective-permute-done((bf16[12,48,384]{2,1,0:T(8,128)(2,1)S(1)}, bf16[12,48,384]{2,1,0:T(8,128)(2,1)S(1)}, u32[]{:S(2)}, u32[]{:S(2)}) %collective-permute-start.5) | collective-permute-done | bytes 442400 | tf_op jit(solution)/shard_map/ppermute | solution.py:18
  87.7 6.5 %collective-permute-done.6.far = bf16[12,48,384]{2,1,0:T(8,128)(2,1)S(1)} collective-permute-done((bf16[12,48,384]{2,1,0:T(8,128)(2,1)S(1)}, bf16[12,48,384]{2,1,0:T(8,128)(2,1)S(1)}, u32[]{:S(2)}, u32[]{:S(2)}) %collective-permute-start.6) | collective-permute-done | bytes 442400 | tf_op jit(solution)/shard_map/ppermute | solution.py:18
  95.3 8.1 %collective-permute-start.7 = (bf16[224,2304]{1,0:T(8,128)(2,1)S(1)}, bf16[224,2304]{1,0:T(8,128)(2,1)S(1)}, u32[]{:S(2)}, u32[]{:S(2)}) collective-permute-start(bf16[224,2304]{1,0:T(8,128)(2,1)S(1)} %get-tuple-element.31), channel_id=1, source_target_pairs={{0,1},{1,0},{2,3},{3,2},{4,5},{5,4},{6,7},{7,6},{8,9},{9,8},{10,11... | collective-permute-start | bytes 3096584 | tf_op jit(solution)/shard_map/ppermute | solution.py:18
  104.2 1.4 collective-permute-done.7.theirs
  105.8 23.8 %fusion = bf16[32,2304]{1,0:T(8,128)(2,1)S(1)} fusion(bf16[224,2304]{1,0:T(8,128)(2,1)S(1)} %shard_map.70), kind=kCustom, calls=%all-reduce-scatter | all-reduce-scatter fusion | flops 589825 | bytes 1183744
  129.7 2.5 %collective-permute-start.9 = (bf16[28,2304]{1,0:T(8,128)(2,1)S(1)}, bf16[28,2304]{1,0:T(8,128)(2,1)S(1)}, u32[]{:S(2)}, u32[]{:S(2)}) collective-permute-start(bf16[28,2304]{1,0:T(8,128)(2,1)S(1)} %slice), channel_id=1, source_target_pairs={{0,3},{3,4},{4,7},{7,8},{8,11},{11,12},{12,15},{1,2},{2,5},{5,6},{... | collective-permute-start | bytes 387080
  134.1 1.4 collective-permute-done.9
  136.2 27.1 %all-gather.1 = bf16[4032,128]{1,0:T(8,128)(2,1)S(1)} all-gather(bf16[504,128]{1,0:T(8,128)(2,1)S(1)} %shard_map.71), channel_id=3, replica_groups={{0,3,4,7,8,11,12,15},{1,2,5,6,9,10,13,14},{16,19,20,23,24,27,28,31},{17..., dimensions={0}, use_global_device_ids=true | all-gather | bytes 1161216 | tf_op jit(solution)/shard_map/all_gather | solution.py:230
  163.3 2.0 %collective-permute-start.8 = (bf16[8,504,128]{2,1,0:T(8,128)(2,1)S(1)}, bf16[8,504,128]{2,1,0:T(8,128)(2,1)S(1)}, u32[]{:S(2)}, u32[]{:S(2)}) collective-permute-start(bf16[8,504,128]{2,1,0:T(8,128)(2,1)S(1)} %bitcast.9), channel_id=1, source_target_pairs={{0,1},{1,0},{2,3},{3,2},{4,5},{5,4},{6,7},{7,6},{8,9},{9,8},{10,11... | collective-permute-start | bytes 3096584 | tf_op jit(solution)/shard_map/ppermute | solution.py:18
  165.3 1.3 shard_map.72.refs_0_
  167.8 1.3 shard_map.73
  (28 shorter events, 9.7 us)
Async XLA Ops:
  0.8 75.5 %copy-start.4 = (f32[2304]{0:T(1024)S(1)}, f32[2304]{0:T(1024)}, u32[]{:S(2)}) copy-start(f32[2304]{0:T(1024)} %gain.2) | copy-start | bytes 27652
  34.1 0.8 copy-start.3
  35.7 33.3 %all-to-all-start = ((bf16[12,48,384]{2,1,0:T(8,128)(2,1)}), bf16[12,48,384]{2,1,0:T(8,128)(2,1)S(1)}, u32[]{:S(2)}, u32[]{:S(2)}) async-start(bf16[12,48,384]{2,1,0:T(8,128)(2,1)} %shard_map.64), calls=%async_computation | async-start | bytes 884736 | tf_op jit(solution)/shard_map/all_to_all | solution.py:189
  39.3 17.2 %collective-permute-start = (bf16[12,48,768]{2,1,0:T(8,128)(2,1)S(1)}, bf16[12,48,768]{2,1,0:T(8,128)(2,1)S(1)}, u32[]{:S(2)}, u32[]{:S(2)}) collective-permute-start(bf16[12,48,768]{2,1,0:T(8,128)(2,1)S(1)} %bitcast.11), channel_id=1, source_target_pairs={{0,48},{16,0},{32,16},{48,32},{1,49},{17,1},{33,17},{49,33},{2,50}... | collective-permute-start | bytes 2654216 | tf_op jit(solution)/shard_map/ppermute | solution.py:18
  43.7 17.9 %collective-permute-start.1 = (bf16[12,48,768]{2,1,0:T(8,128)(2,1)S(1)}, bf16[12,48,768]{2,1,0:T(8,128)(2,1)S(1)}, u32[]{:S(2)}, u32[]{:S(2)}) collective-permute-start(bf16[12,48,768]{2,1,0:T(8,128)(2,1)S(1)} %bitcast.12), channel_id=1, source_target_pairs={{0,16},{16,32},{32,48},{48,0},{1,17},{17,33},{33,49},{49,1},{2,18}... | collective-permute-start | bytes 2654216 | tf_op jit(solution)/shard_map/ppermute | solution.py:18
  62.5 16.6 %collective-permute-start.2 = (bf16[6,48,768]{2,1,0:T(8,128)(2,1)}, bf16[6,48,768]{2,1,0:T(8,128)(2,1)S(1)}, u32[]{:S(2)}, u32[]{:S(2)}) collective-permute-start(bf16[6,48,768]{2,1,0:T(8,128)(2,1)} %get-tuple-element.28), channel_id=1, source_target_pairs={{0,16},{16,32},{32,48},{48,0},{1,17},{17,33},{33,49},{49,1},{2,18}... | collective-permute-start | bytes 1327112 | tf_op jit(solution)/shard_map/ppermute | solution.py:18
  64.5 14.7 %collective-permute-start.3 = (bf16[6,48,768]{2,1,0:T(8,128)(2,1)}, bf16[6,48,768]{2,1,0:T(8,128)(2,1)}, u32[]{:S(2)}, u32[]{:S(2)}) collective-permute-start(bf16[6,48,768]{2,1,0:T(8,128)(2,1)} %get-tuple-element.29), channel_id=1, source_target_pairs={{0,48},{16,0},{32,16},{48,32},{1,49},{17,1},{33,17},{49,33},{2,50}... | collective-permute-start | bytes 1327112 | tf_op jit(solution)/shard_map/ppermute | solution.py:18
  69.0 13.1 %collective-permute-start.4 = (bf16[12,48,384]{2,1,0:T(8,128)(2,1)S(1)}, bf16[12,48,384]{2,1,0:T(8,128)(2,1)S(1)}, u32[]{:S(2)}, u32[]{:S(2)}) collective-permute-start(bf16[12,48,384]{2,1,0:T(8,128)(2,1)S(1)} %all-to-all-done.own), channel_id=1, source_target_pairs={{0,48},{16,0},{32,16},{48,32},{1,49},{17,1},{33,17},{49,33},{2,50}... | collective-permute-start | bytes 1327112 | tf_op jit(solution)/shard_map/ppermute | solution.py:18
  71.0 16.8 %collective-permute-start.5 = (bf16[12,48,384]{2,1,0:T(8,128)(2,1)S(1)}, bf16[12,48,384]{2,1,0:T(8,128)(2,1)S(1)}, u32[]{:S(2)}, u32[]{:S(2)}) collective-permute-start(bf16[12,48,384]{2,1,0:T(8,128)(2,1)S(1)} %all-to-all-done.own), channel_id=1, source_target_pairs={{0,16},{16,32},{32,48},{48,0},{1,17},{17,33},{33,49},{49,1},{2,18}... | collective-permute-start | bytes 1327112 | tf_op jit(solution)/shard_map/ppermute | solution.py:18
  74.3 19.9 %collective-permute-start.6 = (bf16[12,48,384]{2,1,0:T(8,128)(2,1)S(1)}, bf16[12,48,384]{2,1,0:T(8,128)(2,1)S(1)}, u32[]{:S(2)}, u32[]{:S(2)}) collective-permute-start(bf16[12,48,384]{2,1,0:T(8,128)(2,1)S(1)} %all-to-all-done.own), channel_id=1, source_target_pairs={{0,32},{16,48},{32,0},{48,16},{1,33},{17,49},{33,1},{49,17},{2,34}... | collective-permute-start | bytes 1327112 | tf_op jit(solution)/shard_map/ppermute | solution.py:18
  76.3 1.6 copy-start
  79.1 3.0 %copy-start.1 = (f32[28,2304]{1,0:T(8,128)}, f32[28,2304]{1,0:T(8,128)S(1)}, u32[]{:S(2)}) copy-start(f32[28,2304]{1,0:T(8,128)S(1)} %get-tuple-element.32.tokens) | copy-start | bytes 774148
  95.3 10.3 %collective-permute-start.7 = (bf16[224,2304]{1,0:T(8,128)(2,1)S(1)}, bf16[224,2304]{1,0:T(8,128)(2,1)S(1)}, u32[]{:S(2)}, u32[]{:S(2)}) collective-permute-start(bf16[224,2304]{1,0:T(8,128)(2,1)S(1)} %get-tuple-element.31), channel_id=1, source_target_pairs={{0,1},{1,0},{2,3},{3,2},{4,5},{5,4},{6,7},{7,6},{8,9},{9,8},{10,11... | collective-permute-start | bytes 3096584 | tf_op jit(solution)/shard_map/ppermute | solution.py:18
  104.1 31.8 %copy-start.2 = (f32[28,2304]{1,0:T(8,128)S(1)}, f32[28,2304]{1,0:T(8,128)}, u32[]{:S(2)}) copy-start(f32[28,2304]{1,0:T(8,128)} %copy-done.1) | copy-start | bytes 774148
  104.2 31.8 %copy-start.5 = (f32[2304]{0:T(1024)S(1)}, f32[2304]{0:T(1024)}, u32[]{:S(2)}) copy-start(f32[2304]{0:T(1024)} %gain.3) | copy-start | bytes 27652
  129.7 5.8 %collective-permute-start.9 = (bf16[28,2304]{1,0:T(8,128)(2,1)S(1)}, bf16[28,2304]{1,0:T(8,128)(2,1)S(1)}, u32[]{:S(2)}, u32[]{:S(2)}) collective-permute-start(bf16[28,2304]{1,0:T(8,128)(2,1)S(1)} %slice), channel_id=1, source_target_pairs={{0,3},{3,4},{4,7},{7,8},{8,11},{11,12},{12,15},{1,2},{2,5},{5,6},{... | collective-permute-start | bytes 387080
  163.3 4.5 %collective-permute-start.8 = (bf16[8,504,128]{2,1,0:T(8,128)(2,1)S(1)}, bf16[8,504,128]{2,1,0:T(8,128)(2,1)S(1)}, u32[]{:S(2)}, u32[]{:S(2)}) collective-permute-start(bf16[8,504,128]{2,1,0:T(8,128)(2,1)S(1)} %bitcast.9), channel_id=1, source_target_pairs={{0,1},{1,0},{2,3},{3,2},{4,5},{5,4},{6,7},{7,6},{8,9},{9,8},{10,11... | collective-permute-start | bytes 3096584 | tf_op jit(solution)/shard_map/ppermute | solution.py:18

commit v7 on v6

--- a/solution.py
+++ b/solution.py
@@ -42,16 +42,23 @@
     return shift(block, "x", -1), shift(block, "x", 1)
 
 
-def halves_body(left, right, low, high):
-    half = low.shape[0]
-    low[...] = left[:half]
-    high[...] = right[half:]
-
-
-def second_round(right, left):
-    part = jax.ShapeDtypeStruct((left.shape[0] // 2, *left.shape[1:]), BF16)
-    low, high = local_call(halves_body, [part, part], n_in=2, limit=4)(left, right)
-    return shift(low, "x", 1), shift(high, "x", -1)
+def choose_body(core_ref, right, left, out):
+    @pl.when(core_ref[0] == 0)
+    def _():
+        out[...] = right[...]
+
+    @pl.when(core_ref[0] == 1)
+    def _():
+        out[...] = left[...]
+
+
+def second_round(core, right, left):
+    onward = local_call(
+        choose_body, jax.ShapeDtypeStruct(left.shape, BF16), n_scalars=1, n_in=2, limit=4
+    )(core, right, left)
+    n = lax.axis_size("x")
+    pairs = [(2 * i + k, 2 * ((i + 2 * k - 1) % n) + k) for i in range(n) for k in range(2)]
+    return lax.ppermute(onward, ("x", "c"), pairs)
 
 
 def norm_body(half_ref, y_ref, tokens, gain, out, own, window):
@@ -79,14 +86,12 @@
 def interleave(x, blocks, whole):
     for offset, block in enumerate(blocks):
         at = lax.rem(x + offset, len(blocks))
-        for first, piece in block:
-            for z in range(piece.shape[0]):
-                whole[first + z, at] = piece[z]
-
-
-def hidden_body(x_ref, normed, own, right, left, low, high, hidden, whole):
-    far = ((0, low), (low.shape[0], high))
-    interleave(x_ref[0], (((0, own),), ((0, right),), far, ((0, left),)), whole)
+        for z in range(block.shape[0]):
+            whole[z, at] = block[z]
+
+
+def hidden_body(x_ref, normed, own, right, left, far, hidden, whole):
+    interleave(x_ref[0], (own, right, far, left), whole)
     planes, across, rows, columns = whole.shape
     weight = whole[...].reshape(planes * across * rows, columns)
     width = columns // 2
@@ -101,7 +106,7 @@
 
 
 def partial_body(x_ref, half_ref, hidden, own, right, left, far, send, whole):
-    interleave(x_ref[0], [((0, block),) for block in (own, right, far, left)], whole)
+    interleave(x_ref[0], (own, right, far, left), whole)
     send[...] = half_product(hidden, 1 - half_ref[0], whole)
 
 
@@ -170,8 +175,8 @@
 def per_device(tokens, norm_gain, gate_weight, up_weight, down_weight, branch_gain):
     x1, y1, c1 = (lax.axis_index(a).astype(jnp.int32)[None] for a in ("x", "y", "c"))
     own_half = lax.rem(c1 + y1, 2)
-    gate_weight, x1, y1, own_half, other_half = lax.optimization_barrier(
-        (gate_weight, x1, y1, own_half, 1 - own_half)
+    gate_weight, x1, y1, c1, own_half, other_half = lax.optimization_barrier(
+        (gate_weight, x1, y1, c1, own_half, 1 - own_half)
     )
     n_x, n_y, n_z = (lax.axis_size(a) for a in ("x", "y", "z"))
     count, width = tokens.shape
@@ -187,21 +192,23 @@
         copies_body, jax.ShapeDtypeStruct((n_z, piece, units), BF16), n_in=1, limit=2
     )(after(down_weight.T, both_z))
     down_z = lax.all_to_all(copies, "z", 0, 0, tiled=True)
-    far = second_round(*near)
+    far = second_round(c1, *near)
     down_z = after(down_z, *near)
-    down = (*first_round(down_z), shift(down_z, "x", 2))
+    down_near = first_round(down_z)
     normed, own_tokens = local_call(
         norm_body,
         [jax.ShapeDtypeStruct((count, width), BF16), jax.ShapeDtypeStruct((rows, width), F32)],
         [VMEM((48, width), F32)],
         2, 2, 8,
     )(own_half, y1, after(tokens, down_z), norm_gain)
+    *down_near, normed = lax.optimization_barrier((*down_near, normed))
     hidden = local_call(
         hidden_body,
         jax.ShapeDtypeStruct((count, units), BF16),
         [VMEM((n_z, n_x, piece, 2 * units), BF16)],
-        1, 6,
-    )(x1, normed, both_z, *near, *far)
+        1, 5,
+    )(x1, normed, both_z, *near, far)
+    down = (*down_near, second_round(c1, *down_near))
     send, whole = local_call(
         partial_body,
         [

time: 170 us -> 164 us (0.965)
  starting transfers between devices: 36.1 us -> 31.9 us
  Pallas kernels: 10.9 us -> 8.92 us
  waiting for transfers between devices: 32 us -> 33.8 us
    ppermute x0 -> x2, waiting for transfers between devices: none -> 14.1 us  [second_round(): return lax.ppermute(onward, ('x', 'c'), pairs)]
    ppermute x9 -> x6, waiting for transfers between devices: 30.6 us -> 18.2 us  [shift(): return lax.ppermute(value, axis, [(i, (i + by) % n) for i in range(n)])]
    ppermute x9 -> x6, starting transfers between devices: 30.1 us -> 21.1 us  [shift(): return lax.ppermute(value, axis, [(i, (i + by) % n) for i in range(n)])]
    ppermute x0 -> x2, starting transfers between devices: none -> 4.75 us  [second_round(): return lax.ppermute(onward, ('x', 'c'), pairs)]
    unnamed x16 -> x12, local copies, waits for them, and re-layouts: 4.11 us -> 2.53 us
  transfers between devices with their start and end apart: 11 -> 10, of which waited for: 7 -> 9; matrix products, arithmetic and copies ran while one was open for 1% -> 1% of each run, Pallas kernels for 4% -> 3%
where the time goes in v7:
time: 164 us; the launch traced here: 163 us
  blocking collectives  84.3 us (51%)
  waiting for transfers between devices  33.8 us (21%)
  starting transfers between devices  31.9 us (19%)
  Pallas kernels  8.92 us (5%)
  local copies, waits for them, and re-layouts  2.53 us (2%)
    all_gather x1, blocking collectives, per_device(): both_z = lax.all_gather(own_both, 'z')  33.3 us
    all_gather x1, blocking collectives, per_device(): mine = lax.all_gather(done, ('y', 'c'), axis_index_groups=alternating(n_y))  27.2 us
    unnamed x1, blocking collectives  23.8 us
    ppermute x6, starting transfers between devices, shift(): return lax.ppermute(value, axis, [(i, (i + by) % n) for i in range(n)])  21.1 us
    ppermute x6, waiting for transfers between devices, shift(): return lax.ppermute(value, axis, [(i, (i + by) % n) for i in range(n)])  18.2 us
    ppermute x2, waiting for transfers between devices, second_round(): return lax.ppermute(onward, ('x', 'c'), pairs)  14.1 us
    ppermute x2, starting transfers between devices, second_round(): return lax.ppermute(onward, ('x', 'c'), pairs)  4.75 us
    all_to_all x1, starting transfers between devices, per_device(): down_z = lax.all_to_all(copies, 'z', 0, 0, tiled=True)  3.58 us
  transfers between devices with their start and end apart: 10, of which 9 were waited for; matrix products, arithmetic and copies ran while one was open for 1% of the time, Pallas kernels for 3%

profile of v7, /device:TPU:1, one launch (start us, length us, event | category | flops | bytes accessed | tf_op | source)
XLA Modules:
  0.0 163.0 jit_solution(8978860020771121332)
XLA Ops:
  0.8 33.3 %all-gather = bf16[576,768]{1,0:T(8,128)(2,1)S(1)} all-gather(bf16[48,768]{1,0:T(8,128)(2,1)S(1)} %pad_maximum_fusion), channel_id=2, replica_groups=mesh['z'=12,'x'=4,'y'=8,'c'=2] {'z'}, dimensions={0}, use_global_device_ids=true | all-gather | bytes 958464 | tf_op jit(solution)/shard_map/all_gather | solution.py:189
  35.7 3.6 %all-to-all-start = ((bf16[12,48,384]{2,1,0:T(8,128)(2,1)}), bf16[12,48,384]{2,1,0:T(8,128)(2,1)S(1)}, u32[]{:S(2)}, u32[]{:S(2)}) async-start(bf16[12,48,384]{2,1,0:T(8,128)(2,1)} %shard_map.64), calls=%async_computation | async-start | bytes 884736 | tf_op jit(solution)/shard_map/all_to_all | solution.py:194
  39.3 3.1 %collective-permute-start.1 = (bf16[12,48,768]{2,1,0:T(8,128)(2,1)S(1)}, bf16[12,48,768]{2,1,0:T(8,128)(2,1)S(1)}, u32[]{:S(2)}, u32[]{:S(2)}) collective-permute-start(bf16[12,48,768]{2,1,0:T(8,128)(2,1)S(1)} %bitcast.11), channel_id=1, source_target_pairs={{0,16},{16,32},{32,48},{48,0},{1,17},{17,33},{33,49},{49,1},{2,18}... | collective-permute-start | bytes 2654216 | tf_op jit(solution)/shard_map/ppermute | solution.py:18
  42.4 3.4 %collective-permute-start = (bf16[12,48,768]{2,1,0:T(8,128)(2,1)S(1)}, bf16[12,48,768]{2,1,0:T(8,128)(2,1)S(1)}, u32[]{:S(2)}, u32[]{:S(2)}) collective-permute-start(bf16[12,48,768]{2,1,0:T(8,128)(2,1)S(1)} %bitcast.12), channel_id=1, source_target_pairs={{0,48},{16,0},{32,16},{48,32},{1,49},{17,1},{33,17},{49,33},{2,50}... | collective-permute-start | bytes 2654216 | tf_op jit(solution)/shard_map/ppermute | solution.py:18
  45.8 11.6 %collective-permute-done.1.left = bf16[12,48,768]{2,1,0:T(8,128)(2,1)S(1)} collective-permute-done((bf16[12,48,768]{2,1,0:T(8,128)(2,1)S(1)}, bf16[12,48,768]{2,1,0:T(8,128)(2,1)S(1)}, u32[]{:S(2)}, u32[]{:S(2)}) %collective-permute-start.1) | collective-permute-done | bytes 884768 | tf_op jit(solution)/shard_map/ppermute | solution.py:18
  57.4 1.6 %collective-permute-done.right = bf16[12,48,768]{2,1,0:T(8,128)(2,1)S(1)} collective-permute-done((bf16[12,48,768]{2,1,0:T(8,128)(2,1)S(1)}, bf16[12,48,768]{2,1,0:T(8,128)(2,1)S(1)}, u32[]{:S(2)}, u32[]{:S(2)}) %collective-permute-start) | collective-permute-done | bytes 884768 | tf_op jit(solution)/shard_map/ppermute | solution.py:18
  59.1 3.2 %collective-permute-start.3 = (bf16[12,48,384]{2,1,0:T(8,128)(2,1)S(1)}, bf16[12,48,384]{2,1,0:T(8,128)(2,1)S(1)}, u32[]{:S(2)}, u32[]{:S(2)}) collective-permute-start(bf16[12,48,384]{2,1,0:T(8,128)(2,1)S(1)} %all-to-all-done.own), channel_id=1, source_target_pairs={{0,16},{16,32},{32,48},{48,0},{1,17},{17,33},{33,49},{49,1},{2,18}... | collective-permute-start | bytes 1327112 | tf_op jit(solution)/shard_map/ppermute | solution.py:18
  62.3 3.4 %collective-permute-start.2 = (bf16[12,48,384]{2,1,0:T(8,128)(2,1)S(1)}, bf16[12,48,384]{2,1,0:T(8,128)(2,1)S(1)}, u32[]{:S(2)}, u32[]{:S(2)}) collective-permute-start(bf16[12,48,384]{2,1,0:T(8,128)(2,1)S(1)} %all-to-all-done.own), channel_id=1, source_target_pairs={{0,48},{16,0},{32,16},{48,32},{1,49},{17,1},{33,17},{49,33},{2,50}... | collective-permute-start | bytes 1327112 | tf_op jit(solution)/shard_map/ppermute | solution.py:18
  65.8 1.9 %collective-permute-start.4 = (bf16[12,48,768]{2,1,0:T(8,128)(2,1)S(1)}, bf16[12,48,768]{2,1,0:T(8,128)(2,1)S(1)}, u32[]{:S(2)}, u32[]{:S(2)}) collective-permute-start(bf16[12,48,768]{2,1,0:T(8,128)(2,1)S(1)} %shard_map.66), channel_id=1, source_target_pairs={{0,48},{1,17},{16,0},{17,33},{32,16},{33,49},{48,32},{49,1},{2,50}... | collective-permute-start | bytes 2654216 | tf_op jit(solution)/shard_map/ppermute | solution.py:61
  69.5 1.9 %collective-permute-done.2.right = bf16[12,48,384]{2,1,0:T(8,128)(2,1)S(1)} collective-permute-done((bf16[12,48,384]{2,1,0:T(8,128)(2,1)S(1)}, bf16[12,48,384]{2,1,0:T(8,128)(2,1)S(1)}, u32[]{:S(2)}, u32[]{:S(2)}) %collective-permute-start.2) | collective-permute-done | bytes 442400 | tf_op jit(solution)/shard_map/ppermute | solution.py:18
  71.4 2.8 %collective-permute-start.5 = (bf16[12,48,384]{2,1,0:T(8,128)(2,1)S(1)}, bf16[12,48,384]{2,1,0:T(8,128)(2,1)S(1)}, u32[]{:S(2)}, u32[]{:S(2)}) collective-permute-start(bf16[12,48,384]{2,1,0:T(8,128)(2,1)S(1)} %shard_map.68), channel_id=1, source_target_pairs={{0,48},{1,17},{16,0},{17,33},{32,16},{33,49},{48,32},{49,1},{2,50}... | collective-permute-start | bytes 1327112 | tf_op jit(solution)/shard_map/ppermute | solution.py:61
  74.2 11.3 %collective-permute-done.4.far = bf16[12,48,768]{2,1,0:T(8,128)(2,1)S(1)} collective-permute-done((bf16[12,48,768]{2,1,0:T(8,128)(2,1)S(1)}, bf16[12,48,768]{2,1,0:T(8,128)(2,1)S(1)}, u32[]{:S(2)}, u32[]{:S(2)}) %collective-permute-start.4) | collective-permute-done | bytes 884768 | tf_op jit(solution)/shard_map/ppermute | solution.py:61
  85.5 1.9 %shard_map.67.hidden = bf16[448,384]{1,0:T(8,128)(2,1)S(1)} custom-call(s32[1]{0:T(128)} %bitcast.x_ref, bf16[448,2304]{1,0:T(8,128)(2,1)S(1)} %get-tuple-element.30.normed, bf16[12,48,768]{2,1,0:T(8,128)(2,1)S(1)} %bitcast.13, bf16[12,48,768]{2,1,0:T(8,128)(2,1)S(1)} %collective-permute-done.right, bf16[12,48,768]{2,1,0:T(8,128)(2,1)S(1)} %collective-permute-done.1.left, ...), custom_call_target="tpu_custom_call" | custom-call | tf_op jit(solution)/shard_map/pallas_call | solution.py:205
  87.4 2.8 %collective-permute-done.5.far = bf16[12,48,384]{2,1,0:T(8,128)(2,1)S(1)} collective-permute-done((bf16[12,48,384]{2,1,0:T(8,128)(2,1)S(1)}, bf16[12,48,384]{2,1,0:T(8,128)(2,1)S(1)}, u32[]{:S(2)}, u32[]{:S(2)}) %collective-permute-start.5) | collective-permute-done | bytes 442400 | tf_op jit(solution)/shard_map/ppermute | solution.py:61
  91.3 6.0 %collective-permute-start.6 = (bf16[224,2304]{1,0:T(8,128)(2,1)S(1)}, bf16[224,2304]{1,0:T(8,128)(2,1)S(1)}, u32[]{:S(2)}, u32[]{:S(2)}) collective-permute-start(bf16[224,2304]{1,0:T(8,128)(2,1)S(1)} %get-tuple-element.35), channel_id=1, source_target_pairs={{0,1},{1,0},{2,3},{3,2},{4,5},{5,4},{6,7},{7,6},{8,9},{9,8},{10,11... | collective-permute-start | bytes 3096584 | tf_op jit(solution)/shard_map/ppermute | solution.py:18
  98.1 1.4 collective-permute-done.6.theirs
  99.8 23.8 %fusion = bf16[32,2304]{1,0:T(8,128)(2,1)S(1)} fusion(bf16[224,2304]{1,0:T(8,128)(2,1)S(1)} %shard_map.71), kind=kCustom, calls=%all-reduce-scatter | all-reduce-scatter fusion | flops 589825 | bytes 1183744
  123.6 2.4 %collective-permute-start.8 = (bf16[28,2304]{1,0:T(8,128)(2,1)S(1)}, bf16[28,2304]{1,0:T(8,128)(2,1)S(1)}, u32[]{:S(2)}, u32[]{:S(2)}) collective-permute-start(bf16[28,2304]{1,0:T(8,128)(2,1)S(1)} %slice), channel_id=1, source_target_pairs={{0,3},{3,4},{4,7},{7,8},{8,11},{11,12},{12,15},{1,2},{2,5},{5,6},{... | collective-permute-start | bytes 387080
  126.1 1.3 dynamic-slice.4
  128.0 1.4 collective-permute-done.8
  130.0 27.2 %all-gather.1 = bf16[4032,128]{1,0:T(8,128)(2,1)S(1)} all-gather(bf16[504,128]{1,0:T(8,128)(2,1)S(1)} %shard_map.72), channel_id=3, replica_groups={{0,3,4,7,8,11,12,15},{1,2,5,6,9,10,13,14},{16,19,20,23,24,27,28,31},{17..., dimensions={0}, use_global_device_ids=true | all-gather | bytes 1161216 | tf_op jit(solution)/shard_map/all_gather | solution.py:237
  157.2 2.0 %collective-permute-start.7 = (bf16[8,504,128]{2,1,0:T(8,128)(2,1)S(1)}, bf16[8,504,128]{2,1,0:T(8,128)(2,1)S(1)}, u32[]{:S(2)}, u32[]{:S(2)}) collective-permute-start(bf16[8,504,128]{2,1,0:T(8,128)(2,1)S(1)} %bitcast.9), channel_id=1, source_target_pairs={{0,1},{1,0},{2,3},{3,2},{4,5},{5,4},{6,7},{7,6},{8,9},{9,8},{10,11... | collective-permute-start | bytes 3096584 | tf_op jit(solution)/shard_map/ppermute | solution.py:18
  159.2 1.3 shard_map.73.refs_0_
  161.7 1.3 shard_map.74
  (23 shorter events, 8.0 us)
Async XLA Ops:
  0.8 66.9 %copy-start.2 = (f32[2304]{0:T(1024)S(1)}, f32[2304]{0:T(1024)}, u32[]{:S(2)}) copy-start(f32[2304]{0:T(1024)} %gain.2) | copy-start | bytes 27652
  34.1 0.8 copy-start.1
  35.7 23.4 %all-to-all-start = ((bf16[12,48,384]{2,1,0:T(8,128)(2,1)}), bf16[12,48,384]{2,1,0:T(8,128)(2,1)S(1)}, u32[]{:S(2)}, u32[]{:S(2)}) async-start(bf16[12,48,384]{2,1,0:T(8,128)(2,1)} %shard_map.64), calls=%async_computation | async-start | bytes 884736 | tf_op jit(solution)/shard_map/all_to_all | solution.py:194
  39.3 18.2 %collective-permute-start.1 = (bf16[12,48,768]{2,1,0:T(8,128)(2,1)S(1)}, bf16[12,48,768]{2,1,0:T(8,128)(2,1)S(1)}, u32[]{:S(2)}, u32[]{:S(2)}) collective-permute-start(bf16[12,48,768]{2,1,0:T(8,128)(2,1)S(1)} %bitcast.11), channel_id=1, source_target_pairs={{0,16},{16,32},{32,48},{48,0},{1,17},{17,33},{33,49},{49,1},{2,18}... | collective-permute-start | bytes 2654216 | tf_op jit(solution)/shard_map/ppermute | solution.py:18
  42.4 16.7 %collective-permute-start = (bf16[12,48,768]{2,1,0:T(8,128)(2,1)S(1)}, bf16[12,48,768]{2,1,0:T(8,128)(2,1)S(1)}, u32[]{:S(2)}, u32[]{:S(2)}) collective-permute-start(bf16[12,48,768]{2,1,0:T(8,128)(2,1)S(1)} %bitcast.12), channel_id=1, source_target_pairs={{0,48},{16,0},{32,16},{48,32},{1,49},{17,1},{33,17},{49,33},{2,50}... | collective-permute-start | bytes 2654216 | tf_op jit(solution)/shard_map/ppermute | solution.py:18
  59.1 8.7 %copy-start = (bf16[448,2304]{1,0:T(8,128)(2,1)S(1)}, bf16[448,2304]{1,0:T(8,128)(2,1)}, u32[]{:S(2)}) copy-start(bf16[448,2304]{1,0:T(8,128)(2,1)} %tokens) | copy-start | bytes 6193156
  59.1 10.4 %collective-permute-start.3 = (bf16[12,48,384]{2,1,0:T(8,128)(2,1)S(1)}, bf16[12,48,384]{2,1,0:T(8,128)(2,1)S(1)}, u32[]{:S(2)}, u32[]{:S(2)}) collective-permute-start(bf16[12,48,384]{2,1,0:T(8,128)(2,1)S(1)} %all-to-all-done.own), channel_id=1, source_target_pairs={{0,16},{16,32},{32,48},{48,0},{1,17},{17,33},{33,49},{49,1},{2,18}... | collective-permute-start | bytes 1327112 | tf_op jit(solution)/shard_map/ppermute | solution.py:18
  62.3 9.0 %collective-permute-start.2 = (bf16[12,48,384]{2,1,0:T(8,128)(2,1)S(1)}, bf16[12,48,384]{2,1,0:T(8,128)(2,1)S(1)}, u32[]{:S(2)}, u32[]{:S(2)}) collective-permute-start(bf16[12,48,384]{2,1,0:T(8,128)(2,1)S(1)} %all-to-all-done.own), channel_id=1, source_target_pairs={{0,48},{16,0},{32,16},{48,32},{1,49},{17,1},{33,17},{49,33},{2,50}... | collective-permute-start | bytes 1327112 | tf_op jit(solution)/shard_map/ppermute | solution.py:18
  65.8 19.7 %collective-permute-start.4 = (bf16[12,48,768]{2,1,0:T(8,128)(2,1)S(1)}, bf16[12,48,768]{2,1,0:T(8,128)(2,1)S(1)}, u32[]{:S(2)}, u32[]{:S(2)}) collective-permute-start(bf16[12,48,768]{2,1,0:T(8,128)(2,1)S(1)} %shard_map.66), channel_id=1, source_target_pairs={{0,48},{1,17},{16,0},{17,33},{32,16},{33,49},{48,32},{49,1},{2,50}... | collective-permute-start | bytes 2654216 | tf_op jit(solution)/shard_map/ppermute | solution.py:61
  71.4 18.9 %collective-permute-start.5 = (bf16[12,48,384]{2,1,0:T(8,128)(2,1)S(1)}, bf16[12,48,384]{2,1,0:T(8,128)(2,1)S(1)}, u32[]{:S(2)}, u32[]{:S(2)}) collective-permute-start(bf16[12,48,384]{2,1,0:T(8,128)(2,1)S(1)} %shard_map.68), channel_id=1, source_target_pairs={{0,48},{1,17},{16,0},{17,33},{32,16},{33,49},{48,32},{49,1},{2,50}... | collective-permute-start | bytes 1327112 | tf_op jit(solution)/shard_map/ppermute | solution.py:61
  91.3 8.2 %collective-permute-start.6 = (bf16[224,2304]{1,0:T(8,128)(2,1)S(1)}, bf16[224,2304]{1,0:T(8,128)(2,1)S(1)}, u32[]{:S(2)}, u32[]{:S(2)}) collective-permute-start(bf16[224,2304]{1,0:T(8,128)(2,1)S(1)} %get-tuple-element.35), channel_id=1, source_target_pairs={{0,1},{1,0},{2,3},{3,2},{4,5},{5,4},{6,7},{7,6},{8,9},{9,8},{10,11... | collective-permute-start | bytes 3096584 | tf_op jit(solution)/shard_map/ppermute | solution.py:18
  98.1 31.8 %copy-start.3 = (f32[2304]{0:T(1024)S(1)}, f32[2304]{0:T(1024)}, u32[]{:S(2)}) copy-start(f32[2304]{0:T(1024)} %gain.3) | copy-start | bytes 27652
  123.6 5.8 %collective-permute-start.8 = (bf16[28,2304]{1,0:T(8,128)(2,1)S(1)}, bf16[28,2304]{1,0:T(8,128)(2,1)S(1)}, u32[]{:S(2)}, u32[]{:S(2)}) collective-permute-start(bf16[28,2304]{1,0:T(8,128)(2,1)S(1)} %slice), channel_id=1, source_target_pairs={{0,3},{3,4},{4,7},{7,8},{8,11},{11,12},{12,15},{1,2},{2,5},{5,6},{... | collective-permute-start | bytes 387080
  157.2 4.5 %collective-permute-start.7 = (bf16[8,504,128]{2,1,0:T(8,128)(2,1)S(1)}, bf16[8,504,128]{2,1,0:T(8,128)(2,1)S(1)}, u32[]{:S(2)}, u32[]{:S(2)}) collective-permute-start(bf16[8,504,128]{2,1,0:T(8,128)(2,1)S(1)} %bitcast.9), channel_id=1, source_target_pairs={{0,1},{1,0},{2,3},{3,2},{4,5},{5,4},{6,7},{7,6},{8,9},{9,8},{10,11... | collective-permute-start | bytes 3096584 | tf_op jit(solution)/shard_map/ppermute | solution.py:18
